TPU v7x, 256 devices: a whole 4x4x8 slice. The times are simulated.
256 devices in a mesh: kv: 32 (over z, x), tp: 8 (over y, core).
Axes of the slice: x: 4, y: 4, z: 8, core: 2. Of those that a mesh axis runs over, the one named last changes fastest.
Arguments:
- tokens: bfloat16 [512, 2048], P(None, 'kv'), may hold values from -16 to 16
- norm_gain: bfloat16 [2048], P('kv'), may hold values from 0.099609375 to 1.8984375
- w_query: bfloat16 [2048, 1024], P('kv', 'tp'), may hold values from -0.125 to 0.125
- w_key: bfloat16 [2048, 1024], P('kv', 'tp'), may hold values from -0.125 to 0.125
- w_value: bfloat16 [2048, 2048], P('kv', 'tp'), may hold values from -0.125 to 0.125
- w_gate: bfloat16 [2048, 2048], P('kv', 'tp'), may hold values from -0.125 to 0.125
- w_decay: bfloat16 [2048, 1024], P('kv', 'tp'), may hold values from -0.5 to 0.5
- log_decay: float32 [512, 1024], P('kv', 'tp'), may hold values from -1.5 to 0
- state: float32 [512, 8, 128, 256], P('kv', 'tp'), may hold values from -6 to 6
- out_gain: float32 [256], replicated, may hold values from 0.1 to 1.9
- w_out: bfloat16 [2048, 2048], P('tp', 'kv'), may hold values from -0.125 to 0.125
- mixer_gain: bfloat16 [2048], P('kv'), may hold values from 0.099609375 to 1.8984375
- w_ffgate: bfloat16 [2048, 6144], P('kv', 'tp'), may hold values from -0.125 to 0.125
- w_ffup: bfloat16 [2048, 6144], P('kv', 'tp'), may hold values from -0.125 to 0.125
- w_down: bfloat16 [6144, 2048], P('tp', 'kv'), may hold values from -0.078125 to 0.078125
Outputs:
- result: bfloat16 [512, 2048], P(None, 'kv')
- new_state: float32 [512, 8, 128, 256], P('kv', 'tp')
All inputs are finite; a program needn't handle non-finite values.
Results may differ from a plain program's by a relative error of at most 0.028.
Values may be sent and summed in bfloat16 or wider, within the bound.
A program may use at most 64 MiB of HBM per device.

v0:
```python
import jax
import jax.numpy as jnp
from jax import lax
from jax.sharding import PartitionSpec as P

D = 2048
DK = 128
DV = 256


eps = 1e-06
gate_norm = 16.0


def copy_for_each(array, axis):
    copies = jnp.broadcast_to(array, (lax.axis_size(axis), *array.shape))
    return lax.all_to_all(copies, axis, split_axis=0, concat_axis=0, tiled=True)


def of_everyone(array, axis):
    return copy_for_each(array, axis).sum(axis=0)


def in_blocks(array, dim, count):
    shape = array.shape
    blocks = array.reshape(*shape[:dim], count, shape[dim] // count, *shape[dim + 1 :])
    return jnp.moveaxis(blocks, dim, 0)


def sum_at_owner(array, axis, dim):
    count = lax.axis_size(axis)
    blocks = lax.all_to_all(in_blocks(array, dim, count), axis, 0, 0, tiled=True)
    return jnp.sum(blocks.astype(jnp.float32), axis=0)


def in_order(blocks, dim):
    shape = list(blocks.shape[1:])
    shape[dim] *= blocks.shape[0]
    return jnp.moveaxis(blocks, 0, dim).reshape(shape)


def collect(array, axis, dim):
    blocks = copy_for_each(array, axis)
    return in_order(blocks, dim)


def of_everyone_2(array, axis):
    everything = copy_for_each(array, axis)
    return jnp.sum(everything.astype(jnp.float32), axis=0)


def prepare(resid, gain):
    wide = resid.astype(jnp.float32)
    scaled = (wide * gain.astype(jnp.float32)).astype(jnp.bfloat16)
    return (scaled, jnp.sum(wide * wide, axis=1))


def project(scaled, weights):
    return jnp.concatenate(
        [jnp.dot(scaled, weight, preferred_element_type=jnp.float32) for weight in weights], axis=1
    )


def activate(terms, sums, width):
    terms = terms * lax.rsqrt(sums / D + eps)[:, None]
    return (jax.nn.silu(terms[:, :width]) * terms[:, width:]).astype(jnp.bfloat16)


def body(
    tokens,
    norm_gain,
    w_query,
    w_key,
    w_value,
    w_gate,
    w_decay,
    log_decay,
    state,
    out_gain,
    w_out,
    mixer_gain,
    w_ffgate,
    w_ffup,
    w_down,
):
    seq_dev = state.shape[0]
    heads = state.shape[1]
    key_width = w_query.shape[1]
    value_width = w_value.shape[1]
    scaled, squares = prepare(tokens, norm_gain)
    attn_weights = (w_query, w_key, w_value, w_gate, w_decay)
    sums_all = of_everyone(squares, "kv")
    terms = sum_at_owner(
        (lambda start, count: project(scaled, attn_weights))(
            jnp.int32(0), seq_dev * lax.axis_size("kv")
        ).astype(jnp.bfloat16),
        "kv",
        0,
    )
    sums = lax.dynamic_slice_in_dim(sums_all, lax.axis_index("kv") * seq_dev, seq_dev, 0)
    terms = terms * lax.rsqrt(sums / D + eps)[:, None]
    query = terms[:, :key_width].reshape(seq_dev, heads, DK) * DK ** (-0.5)
    keys = terms[:, key_width : 2 * key_width].reshape(seq_dev, heads, DK)
    values = terms[:, 2 * key_width : 2 * key_width + value_width].reshape(seq_dev, heads, DV)
    gate = terms[:, 2 * key_width + value_width : 2 * key_width + 2 * value_width]
    decay_pre = terms[:, 2 * key_width + 2 * value_width :]
    log_a = jax.nn.log_sigmoid(decay_pre) / gate_norm + log_decay
    new_state = (
        state * jnp.exp(log_a).reshape(seq_dev, heads, DK)[..., None]
        + keys[..., None] * values[:, :, None, :]
    )
    attended = jnp.einsum("bhk,bhkv->bhv", query, new_state)
    normed = (
        attended * lax.rsqrt(jnp.mean(attended * attended, axis=2, keepdims=True) + eps) * out_gain
    )
    mixed = (normed.reshape(seq_dev, value_width) * jax.nn.silu(gate)).astype(jnp.bfloat16)
    partial_out = jnp.dot(collect(mixed, "kv", 0), w_out, preferred_element_type=jnp.float32)
    attn_sum = of_everyone_2(partial_out.astype(jnp.bfloat16), "tp").astype(jnp.float32)
    middle = (tokens.astype(jnp.float32) + attn_sum).astype(jnp.bfloat16)
    scaled2, squares2 = prepare(middle, mixer_gain)
    ff_weights = (w_ffgate, w_ffup)
    width = w_ffgate.shape[1]
    sums_all2 = of_everyone(squares2, "kv")
    terms2 = sum_at_owner(
        (lambda start, count: project(scaled2, ff_weights))(
            jnp.int32(0), seq_dev * lax.axis_size("kv")
        ).astype(jnp.bfloat16),
        "kv",
        0,
    )
    sums2 = lax.dynamic_slice_in_dim(sums_all2, lax.axis_index("kv") * seq_dev, seq_dev, 0)
    hidden = activate(terms2, sums2, width)
    partial_down = jnp.dot(collect(hidden, "kv", 0), w_down, preferred_element_type=jnp.float32)
    down_total = of_everyone_2(partial_down.astype(jnp.bfloat16), "tp").astype(jnp.float32)
    result = (middle.astype(jnp.float32) + down_total).astype(jnp.bfloat16)
    return (result, new_state)


def solution(mesh):
    return jax.shard_map(
        body,
        mesh=mesh,
        in_specs=(
            P(None, "kv"),
            P("kv"),
            P("kv", "tp"),
            P("kv", "tp"),
            P("kv", "tp"),
            P("kv", "tp"),
            P("kv", "tp"),
            P("kv", "tp"),
            P("kv", "tp", None, None),
            P(),
            P("tp", "kv"),
            P("kv"),
            P("kv", "tp"),
            P("kv", "tp"),
            P("tp", "kv"),
        ),
        out_specs=(P(None, "kv"), P("kv", "tp", None, None)),
        check_vma=False,
    )
```

profile of v0, /device:TPU:1, one launch (start us, length us, event | category | flops | bytes accessed | tf_op | source)
XLA Modules:
  0.0 192.5 jit_solution(6379742123364959818)
XLA Ops:
  0.6 0.9 fusion.3
  1.6 0.7 broadcast_in_dim.24
  2.2 11.9 %all-to-all-start.1 = ((f32[32,1,512]{2,1,0:T(1,128)}), f32[32,1,512]{2,1,0:T(1,128)S(1)}, u32[]{:S(2)}, u32[]{:S(2)}) async-start(f32[32,1,512]{2,1,0:T(1,128)} %broadcast_in_dim.24), calls=%async_computation.1 | async-start | bytes 131072 | tf_op jit(solution)/shard_map/all_to_all | solution.py:17
  14.1 0.7 convert_element_type.55
  14.7 1.1 convolution_convert_fusion.5
  15.9 1.1 convolution_convert_fusion.4
  17.0 1.1 convolution_convert_fusion.6
  18.1 1.2 convolution_convert_fusion.3
  19.3 1.2 convolution_convert_fusion.2
  20.7 0.9 copy-done.3
  21.6 1.3 all-to-all-done.1
  22.9 7.9 %all-to-all-start = ((bf16[32,16,896]{2,1,0:T(8,128)(2,1)}), bf16[32,16,896]{2,1,0:T(8,128)(2,1)S(1)}, u32[]{:S(2)}, u32[]{:S(2)}) async-start(bf16[32,16,896]{2,1,0:T(8,128)(2,1)} %copy-done.3), calls=%async_computation | async-start | bytes 1835008 | tf_op jit(solution)/shard_map/all_to_all | solution.py:32
  31.0 23.1 %all-to-all-done = bf16[32,16,896]{2,1,0:T(8,128)(2,1)S(1)} async-done(((bf16[32,16,896]{2,1,0:T(8,128)(2,1)}), bf16[32,16,896]{2,1,0:T(8,128)(2,1)S(1)}, u32[]{:S(2)}, u32[]{:S(2)}) %all-to-all-start) | async-done | bytes 917536 | tf_op jit(solution)/shard_map/all_to_all | solution.py:32
  54.3 0.9 fusion.26
  55.5 16.5 %all_to_all.42 = bf16[32,16,256]{2,1,0:T(8,128)(2,1)S(1)} all-to-all(bf16[32,16,256]{2,1,0:T(8,128)(2,1)S(1)} %broadcast_in_dim.25), channel_id=1, replica_groups=mesh['kv'=32,'tp'=8] {'kv'}, dimensions={0} | all-to-all | bytes 524288 | tf_op jit(solution)/shard_map/all_to_all | solution.py:17
  72.2 0.8 broadcast_in_dim.26
  73.1 8.2 %all-to-all-start.3 = ((bf16[8,512,64]{1,2,0:T(8,128)(2,1)}), bf16[8,512,64]{1,2,0:T(8,128)(2,1)S(1)}, u32[]{:S(2)}, u32[]{:S(2)}) async-start(bf16[8,512,64]{1,2,0:T(8,128)(2,1)} %broadcast_in_dim.26), calls=%async_computation.3 | async-start | bytes 1048576 | tf_op jit(solution)/shard_map/all_to_all | solution.py:17
  81.3 9.3 %all-to-all-done.3 = bf16[8,512,64]{1,2,0:T(8,128)(2,1)S(1)} async-done(((bf16[8,512,64]{1,2,0:T(8,128)(2,1)}), bf16[8,512,64]{1,2,0:T(8,128)(2,1)S(1)}, u32[]{:S(2)}, u32[]{:S(2)}) %all-to-all-start.3) | async-done | bytes 524320 | tf_op jit(solution)/shard_map/all_to_all | solution.py:17
  90.8 0.7 broadcast_in_dim.27
  91.5 3.9 %all-to-all-start.5 = ((f32[32,1,512]{2,1,0:T(1,128)}), f32[32,1,512]{2,1,0:T(1,128)S(1)}, u32[]{:S(2)}, u32[]{:S(2)}) async-start(f32[32,1,512]{2,1,0:T(1,128)} %broadcast_in_dim.27), calls=%async_computation.5 | async-start | bytes 131072 | tf_op jit(solution)/shard_map/all_to_all | solution.py:17
  95.8 0.5 convolution_convert_fusion.1
  96.3 1.3 pad_maximum_fusion
  97.6 6.6 %all-to-all-done.5 = f32[32,1,512]{2,1,0:T(1,128)S(1)} async-done(((f32[32,1,512]{2,1,0:T(1,128)}), f32[32,1,512]{2,1,0:T(1,128)S(1)}, u32[]{:S(2)}, u32[]{:S(2)}) %all-to-all-start.5) | async-done | bytes 65568 | tf_op jit(solution)/shard_map/all_to_all | solution.py:17
  104.2 4.7 %all-to-all-start.4 = ((bf16[32,16,1536]{2,1,0:T(8,128)(2,1)}), bf16[32,16,1536]{2,1,0:T(8,128)(2,1)}, u32[]{:S(2)}, u32[]{:S(2)}) async-start(bf16[32,16,1536]{2,1,0:T(8,128)(2,1)} %pad_maximum_fusion), calls=%async_computation.4 | async-start | bytes 3145728 | tf_op jit(solution)/shard_map/all_to_all | solution.py:32
  109.1 35.7 %all-to-all-done.4 = bf16[32,16,1536]{2,1,0:T(8,128)(2,1)} async-done(((bf16[32,16,1536]{2,1,0:T(8,128)(2,1)}), bf16[32,16,1536]{2,1,0:T(8,128)(2,1)}, u32[]{:S(2)}, u32[]{:S(2)}) %all-to-all-start.4) | async-done | bytes 1572896 | tf_op jit(solution)/shard_map/all_to_all | solution.py:32
  144.8 1.6 convert_reduce_fusion
  146.6 26.8 %all_to_all.43 = bf16[32,16,768]{2,1,0:T(8,128)(2,1)S(1)} all-to-all(bf16[32,16,768]{2,1,0:T(8,128)(2,1)S(1)} %broadcast_in_dim.28), channel_id=1, replica_groups=mesh['kv'=32,'tp'=8] {'kv'}, dimensions={0} | all-to-all | bytes 1572864 | tf_op jit(solution)/shard_map/all_to_all | solution.py:17
  173.8 0.8 broadcast_in_dim.29
  174.6 7.8 %all-to-all-start.7 = ((bf16[8,512,64]{1,2,0:T(8,128)(2,1)}), bf16[8,512,64]{1,2,0:T(8,128)(2,1)S(1)}, u32[]{:S(2)}, u32[]{:S(2)}) async-start(bf16[8,512,64]{1,2,0:T(8,128)(2,1)} %broadcast_in_dim.29), calls=%async_computation.7 | async-start | bytes 1048576 | tf_op jit(solution)/shard_map/all_to_all | solution.py:17
  182.4 1.7 multiply_add_fusion
  184.1 7.7 %all-to-all-done.7 = bf16[8,512,64]{1,2,0:T(8,128)(2,1)S(1)} async-done(((bf16[8,512,64]{1,2,0:T(8,128)(2,1)}), bf16[8,512,64]{1,2,0:T(8,128)(2,1)S(1)}, u32[]{:S(2)}, u32[]{:S(2)}) %all-to-all-start.7) | async-done | bytes 524320 | tf_op jit(solution)/shard_map/all_to_all | solution.py:17
  191.9 0.6 fusion.7
  (46 shorter events, 2.3 us)
Async XLA Ops:
  0.6 94.7 %copy-start = (bf16[64,768]{1,0:T(8,128)(2,1)S(1)}, bf16[64,768]{1,0:T(8,128)(2,1)}, u32[]{:S(2)}) copy-start(bf16[64,768]{1,0:T(8,128)(2,1)} %param.28) | copy-start | bytes 294916
  2.2 20.7 %all-to-all-start.1 = ((f32[32,1,512]{2,1,0:T(1,128)}), f32[32,1,512]{2,1,0:T(1,128)S(1)}, u32[]{:S(2)}, u32[]{:S(2)}) async-start(f32[32,1,512]{2,1,0:T(1,128)} %broadcast_in_dim.24), calls=%async_computation.1 | async-start | bytes 131072 | tf_op jit(solution)/shard_map/all_to_all | solution.py:17
  20.5 33.8 %copy-start.7 = (f32[16,128]{1,0:T(8,128)S(1)}, f32[16,128]{1,0:T(8,128)}, u32[]{:S(2)}) copy-start(f32[16,128]{1,0:T(8,128)} %param.22) | copy-start | bytes 24580
  20.6 33.8 %copy-start.1 = (f32[16,1,128,256]{3,2,1,0:T(8,128)S(1)}, f32[16,1,128,256]{3,2,1,0:T(8,128)}, u32[]{:S(2)}) copy-start(f32[16,1,128,256]{3,2,1,0:T(8,128)} %param.23) | copy-start | bytes 6291460
  20.7 0.9 copy-start.3
  22.9 31.2 %all-to-all-start = ((bf16[32,16,896]{2,1,0:T(8,128)(2,1)}), bf16[32,16,896]{2,1,0:T(8,128)(2,1)S(1)}, u32[]{:S(2)}, u32[]{:S(2)}) async-start(bf16[32,16,896]{2,1,0:T(8,128)(2,1)} %copy-done.3), calls=%async_computation | async-start | bytes 1835008 | tf_op jit(solution)/shard_map/all_to_all | solution.py:32
  30.8 24.6 %copy-start.8 = (f32[256]{0:T(256)S(1)}, f32[256]{0:T(256)}, u32[]{:S(2)}) copy-start(f32[256]{0:T(256)} %param.24) | copy-start | bytes 3076
  31.0 41.1 %copy-start.6 = (bf16[256,64]{0,1:T(8,128)(2,1)S(1)}, bf16[256,64]{0,1:T(8,128)(2,1)}, u32[]{:S(2)}) copy-start(bf16[256,64]{0,1:T(8,128)(2,1)} %param.25) | copy-start | bytes 98308
  54.3 27.0 %copy-start.9 = (bf16[64]{0:T(256)(128)(2,1)S(1)}, bf16[64]{0:T(256)(128)(2,1)}, u32[]{:S(2)}) copy-start(bf16[64]{0:T(256)(128)(2,1)} %param.26) | copy-start | bytes 388
  55.3 35.5 %copy-start.2 = (bf16[512,64]{0,1:T(8,128)(2,1)S(1)}, bf16[512,64]{0,1:T(8,128)(2,1)}, u32[]{:S(2)}) copy-start(bf16[512,64]{0,1:T(8,128)(2,1)} %param.15) | copy-start | bytes 196612
  72.0 23.8 %copy-start.4 = (bf16[64,768]{1,0:T(8,128)(2,1)S(1)}, bf16[64,768]{1,0:T(8,128)(2,1)}, u32[]{:S(2)}) copy-start(bf16[64,768]{1,0:T(8,128)(2,1)} %param.27) | copy-start | bytes 294916
  73.1 17.6 %all-to-all-start.3 = ((bf16[8,512,64]{1,2,0:T(8,128)(2,1)}), bf16[8,512,64]{1,2,0:T(8,128)(2,1)S(1)}, u32[]{:S(2)}, u32[]{:S(2)}) async-start(bf16[8,512,64]{1,2,0:T(8,128)(2,1)} %broadcast_in_dim.26), calls=%async_computation.3 | async-start | bytes 1048576 | tf_op jit(solution)/shard_map/all_to_all | solution.py:17
  91.5 12.7 %all-to-all-start.5 = ((f32[32,1,512]{2,1,0:T(1,128)}), f32[32,1,512]{2,1,0:T(1,128)S(1)}, u32[]{:S(2)}, u32[]{:S(2)}) async-start(f32[32,1,512]{2,1,0:T(1,128)} %broadcast_in_dim.27), calls=%async_computation.5 | async-start | bytes 131072 | tf_op jit(solution)/shard_map/all_to_all | solution.py:17
  104.2 40.6 %all-to-all-start.4 = ((bf16[32,16,1536]{2,1,0:T(8,128)(2,1)}), bf16[32,16,1536]{2,1,0:T(8,128)(2,1)}, u32[]{:S(2)}, u32[]{:S(2)}) async-start(bf16[32,16,1536]{2,1,0:T(8,128)(2,1)} %pad_maximum_fusion), calls=%async_computation.4 | async-start | bytes 3145728 | tf_op jit(solution)/shard_map/all_to_all | solution.py:32
  109.1 64.4 %copy-start.5 = (bf16[768,64]{0,1:T(8,128)(2,1)S(1)}, bf16[768,64]{0,1:T(8,128)(2,1)}, u32[]{:S(2)}) copy-start(bf16[768,64]{0,1:T(8,128)(2,1)} %param.29) | copy-start | bytes 294916
  174.6 17.1 %all-to-all-start.7 = ((bf16[8,512,64]{1,2,0:T(8,128)(2,1)}), bf16[8,512,64]{1,2,0:T(8,128)(2,1)S(1)}, u32[]{:S(2)}, u32[]{:S(2)}) async-start(bf16[8,512,64]{1,2,0:T(8,128)(2,1)} %broadcast_in_dim.29), calls=%async_computation.7 | async-start | bytes 1048576 | tf_op jit(solution)/shard_map/all_to_all | solution.py:17
where the time goes:
time: 193 us
  waiting for transfers between devices  83.8 us (43%)
  starting transfers between devices  44.3 us (23%)
  blocking collectives  43.4 us (22%)
  matrix products  8.09 us (4%)
  other arithmetic  7.85 us (4%)
  local copies, waits for them, and re-layouts  4.19 us (2%)
    all_to_all x2, waiting for transfers between devices, sum_at_owner(): lax.all_to_all(in_blocks(array, dim, count), axis, 0, 0, tiled=True)  58.9 us
    all_to_all x2, blocking collectives, copy_for_each(): return lax.all_to_all(copies, axis, split_axis=0, concat_axis=0, tiled=True)  43.4 us
    all_to_all x4, starting transfers between devices, copy_for_each(): return lax.all_to_all(copies, axis, split_axis=0, concat_axis=0, tiled=True)  31.7 us
    all_to_all x4, waiting for transfers between devices, copy_for_each(): return lax.all_to_all(copies, axis, split_axis=0, concat_axis=0, tiled=True)  25 us
    all_to_all x2, starting transfers between devices, sum_at_owner(): lax.all_to_all(in_blocks(array, dim, count), axis, 0, 0, tiled=True)  12.6 us
    dot_general x7, matrix products, project(): jnp.dot(scaled, weight, preferred_element_type=jnp.float32)  6.6 us
  transfers between devices with their start and end apart: 6, of which 6 were waited for; matrix products, arithmetic and copies ran while one was open for 6% of the time, Pallas kernels for 0%

commit v1 on v0

v1 whole, which is shorter than its diff:
```python
import functools

import jax
import jax.numpy as jnp
from jax import lax
from jax.experimental import pallas as pl
from jax.experimental.pallas import tpu as pltpu
from jax.sharding import PartitionSpec as P

MESH = pl.DeviceIdType.MESH
F32 = jnp.float32
BF16 = jnp.bfloat16

D = 2048
DK = 128
DV = 256
EPS = 1e-06
GATE_NORM = 16.0

NX, NY, NZ = 4, 4, 8
NT = 2 * NY
COPIES = 96


def sigmoid(value):
    return 1.0 / (1.0 + jnp.exp(-value))


def halves(low, high):
    return jnp.concatenate([low, high], axis=1)


def as_pair(total):
    high = jnp.broadcast_to(total, (total.shape[0], 128)).astype(BF16).astype(F32)
    low = jnp.broadcast_to(total, (total.shape[0], 128)) - high
    lane = lax.broadcasted_iota(jnp.int32, high.shape, 1)
    return jnp.where(lane < 64, high, low).astype(BF16)


def of_pair(pair):
    return pair[:, 0:1] + pair[:, 64:65]


def packed_products(left, right, lane):
    width = left.shape[1] // 2
    stacked = jnp.concatenate([left[:, :width], left[:, width:]], axis=0)
    total = jnp.dot(stacked, right, preferred_element_type=F32)
    blocks = []
    for j in range(8):
        first = total[0:64, 128 * j : 128 * j + 128]
        second = total[64:128, 128 * j : 128 * j + 128]
        top = first[0:32] + pltpu.roll(second[0:32], 64, 1)
        bottom = pltpu.roll(first[32:64], 64, 1) + second[32:64]
        blocks.append(jnp.where(lane < 64, top, bottom))
    return blocks


def kernel(
    tokens,
    norm_gain,
    w_query,
    w_key,
    w_value,
    w_gate,
    w_decay,
    log_decay,
    state_hbm,
    out_gain,
    w_out,
    mixer_gain,
    w_ffgate,
    w_ffup,
    w_down,
    result,
    state_out,
    state,
    new_state,
    att,
    w_own,
    x_all,
    w_all,
    w_diag,
    part1,
    got1,
    sum1,
    proj,
    mix,
    w_mix,
    part2,
    got2,
    attn_own,
    attn_all,
    tok_own,
    tok_all,
    middle,
    ff_own,
    ff_all,
    part3,
    got3,
    hid,
    part4,
    got4,
    res_own,
    res_all,
    send_sems,
    recv_sems,
    local_sems,
):
    kv = lax.axis_index("kv")
    t = lax.axis_index("tp")
    z, x = lax.div(kv, NX), lax.rem(kv, NX)
    y, core = lax.div(t, 2), lax.rem(t, 2)

    def at_x(d):
        return lax.rem(x + d, NX)

    def at_z(d):
        return lax.rem(z + d, NZ)

    def at_t(d):
        return lax.rem(t + d, NT)

    sent = []
    counter = [0]

    def new_sem(count=1):
        first = counter[0]
        counter[0] += count
        return first

    def send(src, dst, peer, sem=None, recv=None):
        sem = new_sem() if sem is None else sem
        copy = pltpu.make_async_remote_copy(
            src_ref=src,
            dst_ref=dst,
            send_sem=send_sems.at[sem],
            recv_sem=recv_sems.at[sem if recv is None else recv],
            device_id=peer,
            device_id_type=MESH,
        )
        return copy

    def go(copies):
        for copy in copies:
            copy.start()
        sent.extend(copies)
        return copies

    def arrive(copies):
        for copy in copies:
            copy.wait_recv()

    barrier = pltpu.get_barrier_semaphore()

    def greet(peer):
        pl.semaphore_signal(barrier, inc=1, device_id=peer, device_id_type=MESH)

    for d in range(1, NX):
        greet((z * NX + at_x(d), t))
    for d in range(1, NT):
        greet((kv, at_t(d)))
    for d in range(1, NZ):
        greet((at_z(d) * NX + x, t))
        greet((at_z(d) * NX + x, z))

    @pl.when(t != z)
    def _():
        greet((kv, z))

    state_in = pltpu.make_async_copy(state_hbm, state, local_sems.at[0])
    state_in.start()

    square = (64, 64)
    row = lax.broadcasted_iota(jnp.int32, square, 0)
    column = lax.broadcasted_iota(jnp.int32, square, 1)
    gain = jnp.sum(
        jnp.where(row == column, jnp.broadcast_to(norm_gain[...].astype(F32), square), 0.0),
        axis=1,
        keepdims=True,
    )

    def gained(weight):
        return (weight[...].astype(F32) * gain).astype(BF16)

    w_own[0, :, 0:128] = gained(w_query)
    w_own[0, :, 128:256] = gained(w_key)
    w_own[1] = gained(w_value)
    w_own[2] = gained(w_gate)
    w_own[3, :, 0:128] = gained(w_decay)
    w_own[3, :, 128:256] = jnp.zeros((64, 128), BF16)
    x_all[x] = halves(tokens[0:256, :], tokens[256:512, :])
    w_all[x] = w_own[x]

    greetings = (NX - 1) + (NT - 1) + 2 * (NZ - 1)
    pl.semaphore_wait(barrier, greetings + jnp.where(t != z, 1, 0))

    ring_x = [(d, (z * NX + at_x(d), t)) for d in range(1, NX)]
    ring_z = [(d, (at_z(d) * NX + x, t)) for d in range(1, NZ)]
    ring_t = [(d, (kv, at_t(d))) for d in range(1, NT)]
    gather1 = go([send(w_own.at[at_x(d)], w_all.at[x], peer) for d, peer in ring_x])
    gather1 += go([send(x_all.at[x], x_all.at[x], peer) for d, peer in ring_x])

    gains = mixer_gain[...].astype(F32)
    units = halves(
        jnp.transpose(w_ffgate[...].astype(F32), (1, 0)) * gains,
        jnp.transpose(w_ffup[...].astype(F32), (1, 0)) * gains,
    ).astype(BF16)
    for j in range(NZ):
        low, high = slice(96 * j, 96 * j + 48), slice(96 * j + 48, 96 * j + 96)
        ff_own[j, 0] = units[low]
        ff_own[j, 1] = units[high]
        ff_own[j, 2] = halves(w_down[low, :], w_down[high, :])
    lanes_z = pl.ds(pl.multiple_of(z * 128, 128), 128)
    ff_all[:, t, :, lanes_z] = ff_own[z]
    ff_blocks = go(
        [send(ff_own.at[at_z(d)], ff_all.at[:, t, :, lanes_z], peer) for d, peer in ring_z]
    )
    w_mix[:, lanes_z] = halves(w_out[0:128, :], w_out[128:256, :])
    tok_own[...] = halves(tokens[pl.ds(64 * t, 32), :], tokens[pl.ds(64 * t + 32, 32), :])
    tok_all[z] = tok_own[...]
    w_diag[...] = jnp.zeros(w_diag.shape, BF16)

    arrive(gather1)
    lane256 = lax.broadcasted_iota(jnp.int32, (256, 128), 1)
    total = jnp.zeros((256, 512), F32)
    top = jnp.zeros((256, 128), F32)
    bottom = jnp.zeros((256, 128), F32)
    for j in range(NX):
        w_diag[j, 0:64, 0:256] = w_all[j]
        w_diag[j, 64:128, 256:512] = w_all[j]
    for j in range(NX):
        block = x_all[j]
        total += jnp.dot(block, w_diag[j], preferred_element_type=F32)
        wide = block.astype(F32)
        wide = wide * wide
        top += jnp.where(lane256 < 64, wide, 0.0)
        bottom += jnp.where(lane256 < 64, 0.0, wide)
    has_sums = x == NX - 1
    for j in range(NZ):
        rows = slice(64 * (j % 4), 64 * (j % 4) + 64)
        first = 256 * (j // 4)
        part1[j, :, 0:128] = total[rows, first : first + 128].astype(BF16)
        squares = as_pair(jnp.sum((top if j < 4 else bottom)[rows], axis=1, keepdims=True))
        values = total[rows, first + 128 : first + 256]
        part1[j, :, 128:256] = jnp.where(has_sums, squares.astype(F32), values).astype(BF16)
    got1[z] = part1[z]
    scatter1 = go([send(part1.at[at_z(d)], got1.at[z], peer) for d, peer in ring_z])
    mix_blocks = go(
        [send(w_mix.at[:, lanes_z], w_mix.at[:, lanes_z], peer) for d, peer in ring_z]
    )
    tok_blocks = go([send(tok_own, tok_all.at[z], peer) for d, peer in ring_z])

    arrive(ff_blocks)
    partner = (kv, t + 1 - 2 * core)
    ff_y = go(
        [
            send(ff_all.at[:, t], ff_all.at[:, t], (kv, lax.rem(y + d, NY) * 2 + core))
            for d in range(1, NY)
        ]
    )
    ff_core = go([send(ff_all.at[:, t], ff_all.at[:, t], partner)])

    arrive(scatter1)
    total = got1[0].astype(F32)
    for j in range(1, NZ):
        total += got1[j].astype(F32)
    squares = as_pair(of_pair(total[:, 128:256]))
    for j in range(NX):
        rows = slice(16 * j, 16 * j + 16)
        sum1[j, :, 0:128] = total[rows, 0:128].astype(BF16)
        sum1[j, :, 128:256] = jnp.where(
            has_sums, squares[rows].astype(F32), total[rows, 128:256]
        ).astype(BF16)
    proj[x] = sum1[x]
    exchange1 = go([send(sum1.at[at_x(d)], proj.at[x], peer) for d, peer in ring_x])
    state_in.wait()
    arrive(exchange1)

    inv = lax.rsqrt(of_pair(proj[3, :, 128:256].astype(F32)) / D + EPS)
    query = proj[0, :, 0:128].astype(F32) * (inv * DK ** (-0.5))
    keys = proj[0, :, 128:256].astype(F32) * inv
    values = proj[1].astype(F32) * inv
    gate = proj[2].astype(F32) * inv
    decay_pre = proj[3, :, 0:128].astype(F32) * inv
    log_sigmoid = jnp.minimum(decay_pre, 0.0) - jnp.log1p(jnp.exp(-jnp.abs(decay_pre)))
    decay = jnp.exp(log_sigmoid / GATE_NORM + log_decay[...])
    columns = jnp.transpose(
        jnp.concatenate([query, keys, decay, jnp.zeros((80, 128), F32)], axis=0), (1, 0)
    )
    for b in range(16):
        q_col = columns[:, b : b + 1]
        k_col = columns[:, 16 + b : 17 + b]
        a_col = columns[:, 32 + b : 33 + b]
        new = state[b] * a_col + k_col * values[b : b + 1, :]
        new_state[b] = new
        att[b : b + 1, :] = jnp.sum(new * q_col, axis=0, keepdims=True)
    attended = att[...]
    normed = (
        attended
        * lax.rsqrt(jnp.mean(attended * attended, axis=1, keepdims=True) + EPS)
        * out_gain[...]
    )
    mix[x] = (normed * (gate * sigmoid(gate))).astype(BF16)
    gather2 = go([send(mix.at[x], mix.at[x], peer) for d, peer in ring_x])
    state_back = pltpu.make_async_copy(new_state, state_out, local_sems.at[1])
    state_back.start()

    lane32 = lax.broadcasted_iota(jnp.int32, (32, 128), 1)
    arrive(mix_blocks)
    arrive(gather2)
    mixed = mix[...].reshape(64, DV)
    for j, block in enumerate(packed_products(mixed, w_mix[...], lane32)):
        part2[j] = block.astype(BF16)
    got2[t] = part2[t]
    scatter2 = go([send(part2.at[at_t(d)], got2.at[t], peer) for d, peer in ring_t])
    arrive(scatter2)
    total = got2[0].astype(F32)
    for j in range(1, NT):
        total += got2[j].astype(F32)
    attn_own[...] = total.astype(BF16)

    first_send, first_recv = new_sem(NT), 0
    first_recv = first_send
    spread = [
        send(
            attn_own,
            attn_all.at[t],
            (at_z(d) * NX + x, z),
            sem=first_send + d,
            recv=first_recv + t,
        )
        for d in range(NZ)
    ]
    diagonal = t == z

    @pl.when(diagonal)
    def _():
        attn_all[t] = attn_own[...]

    @pl.when(jnp.logical_not(diagonal))
    def _():
        spread[0].start()

    go(spread[1:])

    arrive(ff_y)
    for d in range(1, NY):
        other = lax.rem(y + d, NY) * 2 + core
        ff_core += go([send(ff_all.at[:, other], ff_all.at[:, other], partner)])

    arrive(tok_blocks)
    for j in range(NT):
        copy = pltpu.make_async_remote_copy(
            src_ref=attn_own,
            dst_ref=attn_all.at[j],
            send_sem=send_sems.at[first_send],
            recv_sem=recv_sems.at[first_recv + j],
            device_id=(kv, t),
            device_id_type=MESH,
        )

        @pl.when(jnp.logical_or(t != z, j != t))
        def _(copy=copy):
            copy.wait_recv()

    top = jnp.zeros((32, 128), F32)
    bottom = jnp.zeros((32, 128), F32)
    pieces = []
    for j in range(NZ):
        block = (tok_all[j].astype(F32) + attn_all[j].astype(F32)).astype(BF16)
        middle[j] = block
        wide = block.astype(F32)
        low = jnp.where(lane32 < 64, wide, 0.0)
        high = jnp.where(lane32 < 64, 0.0, wide)
        top += low * low
        bottom += high * high
        pieces.append(
            jnp.concatenate(
                [low, pltpu.roll(high, 64, 1), pltpu.roll(low, 64, 1), high], axis=0
            ).astype(BF16)
        )
    left = jnp.concatenate(pieces, axis=1)
    squares = as_pair(
        jnp.concatenate(
            [jnp.sum(top, axis=1, keepdims=True), jnp.sum(bottom, axis=1, keepdims=True)], axis=0
        )
    )
    arrive(ff_core)
    weights = ff_all[0:2].reshape(NT * 96, 1024)
    terms = lax.dot_general(
        left, weights, (((1,), (1,)), ((), ())), preferred_element_type=F32
    )
    for j in range(NX):
        rows = slice(16 * j, 16 * j + 16)
        part3[j, :, 0:768] = terms[rows].astype(BF16)
        part3[j, :, 768:1536] = terms[64 + 16 * j : 80 + 16 * j].astype(BF16)
        part3[j, :, 1536:1664] = squares[rows]
    got3[x] = part3[x]
    scatter3 = go([send(part3.at[at_x(d)], got3.at[x], peer) for d, peer in ring_x])
    arrive(scatter3)
    total = got3[0].astype(F32)
    for j in range(1, NX):
        total += got3[j].astype(F32)
    inv = lax.rsqrt(of_pair(total[:, 1536:1664]) / D + EPS)
    gate = total[:, 0:768] * inv
    hid[x] = (gate * sigmoid(gate) * (total[:, 768:1536] * inv)).astype(BF16)
    gather3 = go([send(hid.at[x], hid.at[x], peer) for d, peer in ring_x])
    arrive(gather3)

    hidden = hid[...].reshape(64, 768)
    weights = ff_all[2].reshape(NT * 48, 1024)
    for j, block in enumerate(packed_products(hidden, weights, lane32)):
        part4[j] = block.astype(BF16)
    got4[z] = part4[z]
    scatter4 = go([send(part4.at[at_z(d)], got4.at[z], peer) for d, peer in ring_z])
    arrive(scatter4)
    total = got4[0].astype(F32)
    for j in range(1, NZ):
        total += got4[j].astype(F32)
    res_own[...] = (middle[z].astype(F32) + total).astype(BF16)
    res_all[t] = res_own[...]
    gather4 = go([send(res_own, res_all.at[t], peer) for d, peer in ring_t])
    arrive(gather4)
    for j in range(NT):
        block = res_all[j]
        result[64 * j : 64 * j + 32, :] = block[:, 0:64]
        result[64 * j + 32 : 64 * j + 64, :] = block[:, 64:128]

    for copy in sent:
        copy.wait_send()

    @pl.when(jnp.logical_not(diagonal))
    def _():
        spread[0].wait_send()

    state_back.wait()


def body(
    tokens,
    norm_gain,
    w_query,
    w_key,
    w_value,
    w_gate,
    w_decay,
    log_decay,
    state,
    out_gain,
    w_out,
    mixer_gain,
    w_ffgate,
    w_ffup,
    w_down,
):
    vmem = pl.BlockSpec(memory_space=pltpu.VMEM)
    hbm = pl.BlockSpec(memory_space=pl.ANY)
    shape = state.shape
    result, new_state = pl.pallas_call(
        kernel,
        out_shape=(
            jax.ShapeDtypeStruct(tokens.shape, BF16),
            jax.ShapeDtypeStruct((shape[0], DK, DV), F32),
        ),
        in_specs=[vmem] * 8 + [hbm] + [vmem] * 6,
        out_specs=(vmem, hbm),
        scratch_shapes=[
            pltpu.VMEM((16, DK, DV), F32),
            pltpu.VMEM((16, DK, DV), F32),
            pltpu.VMEM((16, DV), F32),
            pltpu.VMEM((NX, 64, 256), BF16),
            pltpu.VMEM((NX, 256, 128), BF16),
            pltpu.VMEM((NX, 64, 256), BF16),
            pltpu.VMEM((NX, 128, 512), BF16),
            pltpu.VMEM((NZ, 64, 256), BF16),
            pltpu.VMEM((NZ, 64, 256), BF16),
            pltpu.VMEM((NX, 16, 256), BF16),
            pltpu.VMEM((NX, 16, 256), BF16),
            pltpu.VMEM((NX, 16, 256), BF16),
            pltpu.VMEM((128, 1024), BF16),
            pltpu.VMEM((NT, 32, 128), BF16),
            pltpu.VMEM((NT, 32, 128), BF16),
            pltpu.VMEM((32, 128), BF16),
            pltpu.VMEM((NT, 32, 128), BF16),
            pltpu.VMEM((32, 128), BF16),
            pltpu.VMEM((NZ, 32, 128), BF16),
            pltpu.VMEM((NZ, 32, 128), BF16),
            pltpu.VMEM((NZ, 3, 48, 128), BF16),
            pltpu.VMEM((3, NT, 48, 1024), BF16),
            pltpu.VMEM((NX, 16, 1664), BF16),
            pltpu.VMEM((NX, 16, 1664), BF16),
            pltpu.VMEM((NX, 16, 768), BF16),
            pltpu.VMEM((NZ, 32, 128), BF16),
            pltpu.VMEM((NZ, 32, 128), BF16),
            pltpu.VMEM((32, 128), BF16),
            pltpu.VMEM((NT, 32, 128), BF16),
            pltpu.SemaphoreType.DMA((COPIES,)),
            pltpu.SemaphoreType.DMA((COPIES,)),
            pltpu.SemaphoreType.DMA((2,)),
        ],
        compiler_params=pltpu.CompilerParams(
            collective_id=0, has_side_effects=True, vmem_limit_bytes=40 * 1024 * 1024
        ),
    )(
        tokens,
        norm_gain.reshape(1, 64),
        w_query,
        w_key,
        w_value,
        w_gate,
        w_decay,
        log_decay,
        state.reshape(shape[0], DK, DV),
        out_gain.reshape(1, DV),
        w_out,
        mixer_gain.reshape(1, 64),
        w_ffgate,
        w_ffup,
        w_down,
    )
    return (result, new_state.reshape(shape))


def solution(mesh):
    return jax.shard_map(
        body,
        mesh=mesh,
        in_specs=(
            P(None, "kv"),
            P("kv"),
            P("kv", "tp"),
            P("kv", "tp"),
            P("kv", "tp"),
            P("kv", "tp"),
            P("kv", "tp"),
            P("kv", "tp"),
            P("kv", "tp", None, None),
            P(),
            P("tp", "kv"),
            P("kv"),
            P("kv", "tp"),
            P("kv", "tp"),
            P("tp", "kv"),
        ),
        out_specs=(P(None, "kv"), P("kv", "tp", None, None)),
        check_vma=False,
    )
```

time: 193 us -> 82.3 us (0.43)
  waiting for transfers between devices: 83.8 us -> 0 us
  Pallas kernels: 0 us -> 66.2 us
  starting transfers between devices: 44.3 us -> 0 us
  blocking collectives: 43.4 us -> 0 us
  local copies, waits for them, and re-layouts: 4.19 us -> 14.7 us
  matrix products: 8.09 us -> 0 us
  other arithmetic: 7.85 us -> 0 us
    all_to_all x6 -> x0, waiting for transfers between devices: 83.8 us -> none  [the longest x2 58.9 us: sum_at_owner(): lax.all_to_all(in_blocks(array, dim, count), axis, 0, 0, tiled=True)]
    pallas_call x0 -> x1, Pallas kernels: none -> 66.2 us  [body(): pl.pallas_call(kernel, out_shape=(jax.ShapeDtypeStruct(tokens.shape, BF16...]
    all_to_all x6 -> x0, starting transfers between devices: 44.3 us -> none  [the longest x4 31.7 us: copy_for_each(): return lax.all_to_all(copies, axis, split_axis=0, concat_axis=0, tiled=True)]
    all_to_all x2 -> x0, blocking collectives: 43.4 us -> none  [copy_for_each(): return lax.all_to_all(copies, axis, split_axis=0, concat_axis=0, tiled=True)]
    unnamed x24 -> x29, local copies, waits for them, and re-layouts: 1.06 us -> 14.7 us
    dot_general x10 -> x0, matrix products: 8.09 us -> none  [the longest x7 6.6 us: project(): jnp.dot(scaled, weight, preferred_element_type=jnp.float32)]
    reduce_sum x9 -> x0, other arithmetic: 3.11 us -> none  [the longest x2 1.77 us: sum_at_owner(): return jnp.sum(blocks.astype(jnp.float32), axis=0)]
    broadcast_in_dim x6 -> x0, local copies, waits for them, and re-layouts: 3.09 us -> none  [copy_for_each(): copies = jnp.broadcast_to(array, (lax.axis_size(axis), *array.shape))]
  transfers between devices with their start and end apart: 6 -> 0, of which waited for: 6 -> 0; matrix products, arithmetic and copies ran while one was open for 6% -> 0% of each run, Pallas kernels for 0% -> 0%
where the time goes in v1:
time: 82.3 us; the launch traced here: 81.6 us
  Pallas kernels  66.2 us (80%)
  local copies, waits for them, and re-layouts  14.7 us (18%)
    pallas_call x1, Pallas kernels, body(): pl.pallas_call(kernel, out_shape=(jax.ShapeDtypeStruct(tokens.shape, BF16...  66.2 us
    unnamed x29, local copies, waits for them, and re-layouts  14.7 us

profile of v1, /device:TPU:1, one launch (start us, length us, event | category | flops | bytes accessed | tf_op | source)
XLA Modules:
  0.0 81.6 jit_solution(15591708523397525700)
XLA Ops:
  0.6 0.9 %copy.18.w_out = bf16[256,64]{1,0:T(8,128)(2,1)S(1)} copy(bf16[256,64]{0,1:T(8,128)(2,1)} %param.25) | data formatting | bytes 65536 | tf_op args[10]
  1.5 1.0 %copy.17.tokens = bf16[512,64]{1,0:T(8,128)(2,1)S(1)} copy(bf16[512,64]{0,1:T(8,128)(2,1)} %param.15) | data formatting | bytes 131072 | tf_op args[0]
  2.5 1.1 %copy.19.w_down = bf16[768,64]{1,0:T(8,128)(2,1)S(1)} copy(bf16[768,64]{0,1:T(8,128)(2,1)} %param.29) | data formatting | bytes 196608 | tf_op args[14]
  3.5 0.0 copy-start
  3.5 1.6 %copy-done = f32[16,1,128,256]{3,2,1,0:T(8,128)S(1)} copy-done((f32[16,1,128,256]{3,2,1,0:T(8,128)S(1)}, f32[16,1,128,256]{3,2,1,0:T(8,128)}, u32[]{:S(2)}) %copy-start) | copy-done | bytes 2097176
  5.1 0.0 copy-start.1
  5.1 0.9 %copy-done.1 = bf16[64,768]{1,0:T(8,128)(2,1)S(1)} copy-done((bf16[64,768]{1,0:T(8,128)(2,1)S(1)}, bf16[64,768]{1,0:T(8,128)(2,1)}, u32[]{:S(2)}) %copy-start.1) | copy-done | bytes 98328
  6.0 0.0 copy-start.2
  6.0 0.9 %copy-done.2 = bf16[64,768]{1,0:T(8,128)(2,1)S(1)} copy-done((bf16[64,768]{1,0:T(8,128)(2,1)S(1)}, bf16[64,768]{1,0:T(8,128)(2,1)}, u32[]{:S(2)}) %copy-start.2) | copy-done | bytes 98328
  6.9 0.0 copy-start.3
  6.9 0.8 copy-done.3
  7.7 0.0 copy-start.4
  7.7 0.8 copy-done.4
  8.4 0.0 copy-start.5
  8.4 0.7 copy-done.5
  9.2 0.0 copy-start.6
  9.2 0.7 copy-done.6
  9.9 0.0 copy-start.7
  9.9 0.7 copy-done.7
  10.6 0.0 copy-start.8
  10.6 0.7 copy-done.8
  11.3 0.0 copy-start.9
  11.3 0.7 copy-done.9
  12.0 0.0 copy-start.10
  12.0 0.7 copy-done.10
  12.6 0.0 copy-start.11
  12.6 0.7 copy-done.11
  13.3 66.2 %shard_map.158 = (bf16[512,64]{1,0:T(8,128)(2,1)S(1)}, f32[16,128,256]{2,1,0:T(8,128)S(1)}) custom-call(bf16[512,64]{1,0:T(8,128)(2,1)S(1)} %copy.17.tokens, bf16[1,64]{1,0:T(2,128)(2,1)S(1)} %bitcast.10, bf16[64,128]{1,0:T(8,128)(2,1)S(1)} %copy-done.5, bf16[64,128]{1,0:T(8,128)(2,1)S(1)} %copy-done.6, bf16[64,256]{1,0:T(8,128)(2,1)S(1)} %copy-done.3, ...), custom_call_target="tpu_custom_call" | custom-call | tf_op jit(solution)/shard_map/pallas_call | solution.py:459
  79.5 0.7 copy.20
  80.3 1.3 %copy.23 = f32[16,1,128,256]{3,2,1,0:T(8,128)} copy(f32[16,1,128,256]{3,2,1,0:T(8,128)S(1)} %bitcast.8) | data formatting | bytes 4194304
Async XLA Ops:
  3.5 1.6 %copy-start = (f32[16,1,128,256]{3,2,1,0:T(8,128)S(1)}, f32[16,1,128,256]{3,2,1,0:T(8,128)}, u32[]{:S(2)}) copy-start(f32[16,1,128,256]{3,2,1,0:T(8,128)} %param.23) | copy-start | bytes 6291460
  5.1 0.9 %copy-start.1 = (bf16[64,768]{1,0:T(8,128)(2,1)S(1)}, bf16[64,768]{1,0:T(8,128)(2,1)}, u32[]{:S(2)}) copy-start(bf16[64,768]{1,0:T(8,128)(2,1)} %w_ffgate.1) | copy-start | bytes 294916
  6.0 0.9 %copy-start.2 = (bf16[64,768]{1,0:T(8,128)(2,1)S(1)}, bf16[64,768]{1,0:T(8,128)(2,1)}, u32[]{:S(2)}) copy-start(bf16[64,768]{1,0:T(8,128)(2,1)} %w_ffup.1) | copy-start | bytes 294916
  6.9 0.8 copy-start.3
  7.7 0.8 copy-start.4
  8.4 0.7 copy-start.5
  9.2 0.7 copy-start.6
  9.9 0.7 copy-start.7
  10.6 0.7 copy-start.8
  11.3 0.7 copy-start.9
  12.0 0.7 copy-start.10
  12.6 0.7 copy-start.11

commit v2 on v1

--- a/solution.py
+++ b/solution.py
@@ -20,6 +20,9 @@
 NX, NY, NZ = 4, 4, 8
 NT = 2 * NY
 COPIES = 96
+STATE = 8
+FIRST = [0, 1, 2, 3, 4, 5, 6]
+LATER = [12, 13, 14, 10, 11, 7, 9, STATE]
 
 
 def sigmoid(value):
@@ -55,57 +58,59 @@
     return blocks
 
 
-def kernel(
-    tokens,
-    norm_gain,
-    w_query,
-    w_key,
-    w_value,
-    w_gate,
-    w_decay,
-    log_decay,
-    state_hbm,
-    out_gain,
-    w_out,
-    mixer_gain,
-    w_ffgate,
-    w_ffup,
-    w_down,
-    result,
-    state_out,
-    state,
-    new_state,
-    att,
-    w_own,
-    x_all,
-    w_all,
-    w_diag,
-    part1,
-    got1,
-    sum1,
-    proj,
-    mix,
-    w_mix,
-    part2,
-    got2,
-    attn_own,
-    attn_all,
-    tok_own,
-    tok_all,
-    middle,
-    ff_own,
-    ff_all,
-    part3,
-    got3,
-    hid,
-    part4,
-    got4,
-    res_own,
-    res_all,
-    send_sems,
-    recv_sems,
-    local_sems,
-):
+def kernel(*refs):
+    inputs, (res_out, state_out), refs = refs[:15], refs[15:17], refs[17:]
+    held, refs = refs[:15], refs[15:]
+    (
+        tokens,
+        norm_gain,
+        w_query,
+        w_key,
+        w_value,
+        w_gate,
+        w_decay,
+        log_decay,
+        state,
+        out_gain,
+        w_out,
+        mixer_gain,
+        w_ffgate,
+        w_ffup,
+        w_down,
+    ) = held
+    (
+        new_state,
+        att,
+        w_own,
+        x_all,
+        w_all,
+        w_diag,
+        part1,
+        got1,
+        sum1,
+        proj,
+        mix,
+        w_mix,
+        part2,
+        got2,
+        attn_own,
+        attn_all,
+        tok_own,
+        tok_all,
+        middle,
+        ff_own,
+        ff_all,
+        part3,
+        got3,
+        hid,
+        part4,
+        got4,
+        res_own,
+        res_all,
+        send_sems,
+        recv_sems,
+        local_sems,
+    ) = refs
     kv = lax.axis_index("kv")
     t = lax.axis_index("tp")
     z, x = lax.div(kv, NX), lax.rem(kv, NX)
@@ -167,9 +172,19 @@
     def _():
         greet((kv, z))
 
-    state_in = pltpu.make_async_copy(state_hbm, state, local_sems.at[0])
-    state_in.start()
-
+    loads = [
+        pltpu.make_async_copy(src, dst, local_sems.at[i])
+        for i, (src, dst) in enumerate(zip(inputs, held))
+    ]
+    for i in FIRST + LATER:
+        loads[i].start()
+
+    def load(*numbers):
+        for i in numbers:
+            loads[i].wait()
+
+    with jax.named_scope("wait_first"):
+        load(*FIRST)
     square = (64, 64)
     row = lax.broadcasted_iota(jnp.int32, square, 0)
     column = lax.broadcasted_iota(jnp.int32, square, 1)
@@ -188,11 +203,13 @@
     w_own[2] = gained(w_gate)
     w_own[3, :, 0:128] = gained(w_decay)
     w_own[3, :, 128:256] = jnp.zeros((64, 128), BF16)
-    x_all[x] = halves(tokens[0:256, :], tokens[256:512, :])
+    own = jnp.concatenate([tokens[:, 0:256], tokens[:, 256:512]], axis=0).astype(F32)
+    x_all[x] = jnp.transpose(own, (1, 0)).astype(BF16)
     w_all[x] = w_own[x]
 
     greetings = (NX - 1) + (NT - 1) + 2 * (NZ - 1)
-    pl.semaphore_wait(barrier, greetings + jnp.where(t != z, 1, 0))
+    with jax.named_scope("wait_barrier"):
+        pl.semaphore_wait(barrier, greetings + jnp.where(t != z, 1, 0))
 
     ring_x = [(d, (z * NX + at_x(d), t)) for d in range(1, NX)]
     ring_z = [(d, (at_z(d) * NX + x, t)) for d in range(1, NZ)]
@@ -200,27 +217,38 @@
     gather1 = go([send(w_own.at[at_x(d)], w_all.at[x], peer) for d, peer in ring_x])
     gather1 += go([send(x_all.at[x], x_all.at[x], peer) for d, peer in ring_x])
 
+    with jax.named_scope("wait_later"):
+        load(*[i for i in LATER if i != STATE])
     gains = mixer_gain[...].astype(F32)
-    units = halves(
-        jnp.transpose(w_ffgate[...].astype(F32), (1, 0)) * gains,
-        jnp.transpose(w_ffup[...].astype(F32), (1, 0)) * gains,
-    ).astype(BF16)
+    units = jnp.transpose(
+        jnp.concatenate([w_ffgate[...], w_ffup[...]], axis=0).astype(F32), (1, 0)
+    )
+    units = (units * jnp.concatenate([gains, gains], axis=1)).astype(BF16)
+    down = w_down[...].astype(F32)
+    down = jnp.concatenate([down, pltpu.roll(down, 768 - 48, 1)], axis=0)
+    down = jnp.transpose(down, (1, 0)).astype(BF16)
     for j in range(NZ):
         low, high = slice(96 * j, 96 * j + 48), slice(96 * j + 48, 96 * j + 96)
         ff_own[j, 0] = units[low]
         ff_own[j, 1] = units[high]
-        ff_own[j, 2] = halves(w_down[low, :], w_down[high, :])
+        ff_own[j, 2] = down[low]
     lanes_z = pl.ds(pl.multiple_of(z * 128, 128), 128)
     ff_all[:, t, :, lanes_z] = ff_own[z]
     ff_blocks = go(
         [send(ff_own.at[at_z(d)], ff_all.at[:, t, :, lanes_z], peer) for d, peer in ring_z]
     )
-    w_mix[:, lanes_z] = halves(w_out[0:128, :], w_out[128:256, :])
-    tok_own[...] = halves(tokens[pl.ds(64 * t, 32), :], tokens[pl.ds(64 * t + 32, 32), :])
+    out_rows = jnp.concatenate([w_out[:, 0:128], w_out[:, 128:256]], axis=0).astype(F32)
+    w_mix[:, lanes_z] = jnp.transpose(out_rows, (1, 0)).astype(BF16)
+    lane32 = lax.broadcasted_iota(jnp.int32, (32, 128), 1)
+    rows = pl.multiple_of(64 * lax.rem(t, 4), 64)
+    own = x_all[x, pl.ds(rows, 64), :].astype(F32)
+    own = jnp.where(t < 4, own, pltpu.roll(own, 64, 1))
+    tok_own[...] = jnp.where(lane32 < 64, own[0:32], pltpu.roll(own[32:64], 64, 1)).astype(BF16)
     tok_all[z] = tok_own[...]
     w_diag[...] = jnp.zeros(w_diag.shape, BF16)
 
-    arrive(gather1)
+    with jax.named_scope("wait_gather1"):
+        arrive(gather1)
     lane256 = lax.broadcasted_iota(jnp.int32, (256, 128), 1)
     total = jnp.zeros((256, 512), F32)
     top = jnp.zeros((256, 128), F32)
@@ -250,7 +278,8 @@
     )
     tok_blocks = go([send(tok_own, tok_all.at[z], peer) for d, peer in ring_z])
 
-    arrive(ff_blocks)
+    with jax.named_scope("wait_ff_blocks"):
+        arrive(ff_blocks)
     partner = (kv, t + 1 - 2 * core)
     ff_y = go(
         [
@@ -260,7 +289,8 @@
     )
     ff_core = go([send(ff_all.at[:, t], ff_all.at[:, t], partner)])
 
-    arrive(scatter1)
+    with jax.named_scope("wait_scatter1"):
+        arrive(scatter1)
     total = got1[0].astype(F32)
     for j in range(1, NZ):
         total += got1[j].astype(F32)
@@ -273,8 +303,9 @@
         ).astype(BF16)
     proj[x] = sum1[x]
     exchange1 = go([send(sum1.at[at_x(d)], proj.at[x], peer) for d, peer in ring_x])
-    state_in.wait()
-    arrive(exchange1)
+    load(STATE)
+    with jax.named_scope("wait_exchange1"):
+        arrive(exchange1)
 
     inv = lax.rsqrt(of_pair(proj[3, :, 128:256].astype(F32)) / D + EPS)
     query = proj[0, :, 0:128].astype(F32) * (inv * DK ** (-0.5))
@@ -302,18 +333,20 @@
     )
     mix[x] = (normed * (gate * sigmoid(gate))).astype(BF16)
     gather2 = go([send(mix.at[x], mix.at[x], peer) for d, peer in ring_x])
-    state_back = pltpu.make_async_copy(new_state, state_out, local_sems.at[1])
+    state_back = pltpu.make_async_copy(new_state, state_out, local_sems.at[15])
     state_back.start()
 
-    lane32 = lax.broadcasted_iota(jnp.int32, (32, 128), 1)
-    arrive(mix_blocks)
-    arrive(gather2)
+    with jax.named_scope("wait_mix_blocks"):
+        arrive(mix_blocks)
+    with jax.named_scope("wait_gather2"):
+        arrive(gather2)
     mixed = mix[...].reshape(64, DV)
     for j, block in enumerate(packed_products(mixed, w_mix[...], lane32)):
         part2[j] = block.astype(BF16)
     got2[t] = part2[t]
     scatter2 = go([send(part2.at[at_t(d)], got2.at[t], peer) for d, peer in ring_t])
-    arrive(scatter2)
+    with jax.named_scope("wait_scatter2"):
+        arrive(scatter2)
     total = got2[0].astype(F32)
     for j in range(1, NT):
         total += got2[j].astype(F32)
@@ -343,13 +376,15 @@
 
     go(spread[1:])
 
-    arrive(ff_y)
+    with jax.named_scope("wait_ff_y"):
+        arrive(ff_y)
     for d in range(1, NY):
         other = lax.rem(y + d, NY) * 2 + core
         ff_core += go([send(ff_all.at[:, other], ff_all.at[:, other], partner)])
 
-    arrive(tok_blocks)
-    for j in range(NT):
+    with jax.named_scope("wait_tok_blocks"):
+        arrive(tok_blocks)
+    def wait_spread(j):
         copy = pltpu.make_async_remote_copy(
             src_ref=attn_own,
             dst_ref=attn_all.at[j],
@@ -362,6 +397,10 @@
         @pl.when(jnp.logical_or(t != z, j != t))
         def _(copy=copy):
             copy.wait_recv()
+
+    with jax.named_scope("wait_spread"):
+        for j in range(NT):
+            wait_spread(j)
 
     top = jnp.zeros((32, 128), F32)
     bottom = jnp.zeros((32, 128), F32)
@@ -385,7 +424,8 @@
             [jnp.sum(top, axis=1, keepdims=True), jnp.sum(bottom, axis=1, keepdims=True)], axis=0
         )
     )
-    arrive(ff_core)
+    with jax.named_scope("wait_ff_core"):
+        arrive(ff_core)
     weights = ff_all[0:2].reshape(NT * 96, 1024)
     terms = lax.dot_general(
         left, weights, (((1,), (1,)), ((), ())), preferred_element_type=F32
@@ -397,7 +437,8 @@
         part3[j, :, 1536:1664] = squares[rows]
     got3[x] = part3[x]
     scatter3 = go([send(part3.at[at_x(d)], got3.at[x], peer) for d, peer in ring_x])
-    arrive(scatter3)
+    with jax.named_scope("wait_scatter3"):
+        arrive(scatter3)
     total = got3[0].astype(F32)
     for j in range(1, NX):
         total += got3[j].astype(F32)
@@ -405,7 +446,8 @@
     gate = total[:, 0:768] * inv
     hid[x] = (gate * sigmoid(gate) * (total[:, 768:1536] * inv)).astype(BF16)
     gather3 = go([send(hid.at[x], hid.at[x], peer) for d, peer in ring_x])
-    arrive(gather3)
+    with jax.named_scope("wait_gather3"):
+        arrive(gather3)
 
     hidden = hid[...].reshape(64, 768)
     weights = ff_all[2].reshape(NT * 48, 1024)
@@ -413,19 +455,18 @@
         part4[j] = block.astype(BF16)
     got4[z] = part4[z]
     scatter4 = go([send(part4.at[at_z(d)], got4.at[z], peer) for d, peer in ring_z])
-    arrive(scatter4)
+    with jax.named_scope("wait_scatter4"):
+        arrive(scatter4)
     total = got4[0].astype(F32)
     for j in range(1, NZ):
         total += got4[j].astype(F32)
     res_own[...] = (middle[z].astype(F32) + total).astype(BF16)
     res_all[t] = res_own[...]
     gather4 = go([send(res_own, res_all.at[t], peer) for d, peer in ring_t])
-    arrive(gather4)
-    for j in range(NT):
-        block = res_all[j]
-        result[64 * j : 64 * j + 32, :] = block[:, 0:64]
-        result[64 * j + 32 : 64 * j + 64, :] = block[:, 64:128]
-
+    with jax.named_scope("wait_gather4"):
+        arrive(gather4)
+    res_back = pltpu.make_async_copy(res_all, res_out, local_sems.at[16])
+    res_back.start()
     for copy in sent:
         copy.wait_send()
 
@@ -434,6 +475,16 @@
         spread[0].wait_send()
 
     state_back.wait()
+    res_back.wait()
+
+
+def finish(res_all, state_in, result, state_out):
+    rows = []
+    for j in range(NT):
+        block = res_all[j].astype(F32)
+        rows += [block, pltpu.roll(block, 64, 1)]
+    rows = jnp.concatenate(rows, axis=0)
+    result[...] = jnp.transpose(rows, (1, 0))[0:64].astype(BF16)
 
 
 def body(
@@ -454,18 +505,35 @@
     w_down,
 ):
     vmem = pl.BlockSpec(memory_space=pltpu.VMEM)
-    hbm = pl.BlockSpec(memory_space=pl.ANY)
+    hbm = pl.BlockSpec(memory_space=pltpu.HBM)
     shape = state.shape
-    result, new_state = pl.pallas_call(
+    arguments = (
+        tokens.T,
+        norm_gain.reshape(1, 64),
+        w_query,
+        w_key,
+        w_value,
+        w_gate,
+        w_decay,
+        log_decay,
+        state.reshape(shape[0], DK, DV),
+        out_gain.reshape(1, DV),
+        w_out.T,
+        mixer_gain.reshape(1, 64),
+        w_ffgate,
+        w_ffup,
+        w_down.T,
+    )
+    blocks, new_state = pl.pallas_call(
         kernel,
         out_shape=(
-            jax.ShapeDtypeStruct(tokens.shape, BF16),
+            jax.ShapeDtypeStruct((NT, 32, 128), BF16),
             jax.ShapeDtypeStruct((shape[0], DK, DV), F32),
         ),
-        in_specs=[vmem] * 8 + [hbm] + [vmem] * 6,
-        out_specs=(vmem, hbm),
-        scratch_shapes=[
-            pltpu.VMEM((16, DK, DV), F32),
+        in_specs=[hbm] * 15,
+        out_specs=(hbm, hbm),
+        scratch_shapes=[pltpu.VMEM(value.shape, value.dtype) for value in arguments]
+        + [
             pltpu.VMEM((16, DK, DV), F32),
             pltpu.VMEM((16, DV), F32),
             pltpu.VMEM((NX, 64, 256), BF16),
@@ -496,29 +564,23 @@
             pltpu.VMEM((NT, 32, 128), BF16),
             pltpu.SemaphoreType.DMA((COPIES,)),
             pltpu.SemaphoreType.DMA((COPIES,)),
-            pltpu.SemaphoreType.DMA((2,)),
+            pltpu.SemaphoreType.DMA((17,)),
         ],
         compiler_params=pltpu.CompilerParams(
-            collective_id=0, has_side_effects=True, vmem_limit_bytes=40 * 1024 * 1024
+            collective_id=0, has_side_effects=True, vmem_limit_bytes=67043328
         ),
-    )(
-        tokens,
-        norm_gain.reshape(1, 64),
-        w_query,
-        w_key,
-        w_value,
-        w_gate,
-        w_decay,
-        log_decay,
-        state.reshape(shape[0], DK, DV),
-        out_gain.reshape(1, DV),
-        w_out,
-        mixer_gain.reshape(1, 64),
-        w_ffgate,
-        w_ffup,
-        w_down,
-    )
-    return (result, new_state.reshape(shape))
+    )(*arguments)
+    result, new_state = pl.pallas_call(
+        finish,
+        out_shape=(
+            jax.ShapeDtypeStruct((64, 512), BF16),
+            jax.ShapeDtypeStruct((shape[0], DK, DV), F32),
+        ),
+        in_specs=[vmem, hbm],
+        out_specs=(vmem, hbm),
+        input_output_aliases={1: 1},
+    )(blocks, new_state)
+    return (result.T, new_state.reshape(shape))
 
 
 def solution(mesh):

time: 82.3 us -> 72.4 us (0.88)
  local copies, waits for them, and re-layouts: 14.7 us -> 3.09 us
  Pallas kernels: 66.2 us -> 68.5 us
    unnamed x29 -> x1, local copies, waits for them, and re-layouts: 14.7 us -> 3.09 us
    pallas_call x1 -> x2, Pallas kernels: 66.2 us -> 68.5 us  [the longest x1 66.9 us: body(): pl.pallas_call(kernel, out_shape=(jax.ShapeDtypeStruct((NT, 32, 128), BF1...]
where the time goes in v2:
time: 72.4 us; the launch traced here: 72.3 us
  Pallas kernels  68.5 us (95%)
  local copies, waits for them, and re-layouts  3.09 us (4%)
    pallas_call x1, Pallas kernels, body(): pl.pallas_call(kernel, out_shape=(jax.ShapeDtypeStruct((NT, 32, 128), BF1...  66.9 us
    unnamed x1, local copies, waits for them, and re-layouts  3.09 us
    pallas_call x1, Pallas kernels, body(): pl.pallas_call(finish, out_shape=(jax.ShapeDtypeStruct((64, 512), BF16),...  1.63 us

profile of v2, /device:TPU:1, one launch (start us, length us, event | category | flops | bytes accessed | tf_op | source)
XLA Modules:
  0.0 72.3 jit_solution(7041708067353739175)
XLA Ops:
  0.6 66.9 %shard_map.158 = (bf16[8,32,128]{2,1,0:T(8,128)(2,1)}, f32[16,128,256]{2,1,0:T(8,128)}) custom-call(bf16[64,512]{1,0:T(8,128)(2,1)} %bitcast.14, bf16[1,64]{1,0:T(2,128)(2,1)} %bitcast.17, bf16[64,128]{1,0:T(8,128)(2,1)} %refs_2_.1, bf16[64,128]{1,0:T(8,128)(2,1)} %refs_3_.1, bf16[64,256]{1,0:T(8,128)(2,1)} %refs_4_.1, bf16[64,256]{1,0:T(8,128)(2,1)} %refs_5_.1, ...), custom_call_target="tpu_custom_call" | custom-call | tf_op jit(solution)/shard_map/pallas_call | solution.py:527
  67.5 1.6 %shard_map.159 = (bf16[64,512]{1,0:T(8,128)(2,1)}, f32[16,128,256]{2,1,0:T(8,128)}) custom-call(bf16[8,32,128]{2,1,0:T(8,128)(2,1)} %get-tuple-element.6.res_all, f32[16,128,256]{2,1,0:T(8,128)} %get-tuple-element.7.state_in), custom_call_target="tpu_custom_call", output_to_operand_aliasing={{1}: (1, {})} | custom-call | tf_op jit(solution)/shard_map/pallas_call | solution.py:573
  69.2 3.1 %copy.21 = f32[16,1,128,256]{3,2,1,0:T(8,128)} copy(f32[16,1,128,256]{3,2,1,0:T(8,128)} %bitcast.11) | data formatting | bytes 4194304

commit v3 on v2

--- a/solution.py
+++ b/solution.py
@@ -19,8 +19,12 @@
 
 NX, NY, NZ = 4, 4, 8
 NT = 2 * NY
-COPIES = 96
+COPIES = 136
 STATE = 8
+FAR_X = [2, 1, 3]
+FAR_Z = [4, 3, 5, 2, 6, 1, 7]
+FAR_T = [4, 5, 2, 3, 6, 7, 1]
+PLANE = [(dz, dx) for dz in FAR_Z + [0] for dx in FAR_X + [0] if (dz, dx) != (0, 0)]
 FIRST = [0, 1, 2, 3, 4, 5, 6]
 LATER = [12, 13, 14, 10, 11, 7, 9, STATE]
 
@@ -87,8 +91,6 @@
         w_diag,
         part1,
         got1,
-        sum1,
-        proj,
         mix,
         w_mix,
         part2,
@@ -160,12 +162,11 @@
     def greet(peer):
         pl.semaphore_signal(barrier, inc=1, device_id=peer, device_id_type=MESH)
 
-    for d in range(1, NX):
-        greet((z * NX + at_x(d), t))
-    for d in range(1, NT):
+    for dz, dx in PLANE:
+        greet((at_z(dz) * NX + at_x(dx), t))
+    for d in FAR_T:
         greet((kv, at_t(d)))
-    for d in range(1, NZ):
-        greet((at_z(d) * NX + x, t))
+    for d in FAR_Z:
         greet((at_z(d) * NX + x, z))
 
     @pl.when(t != z)
@@ -207,13 +208,13 @@
     x_all[x] = jnp.transpose(own, (1, 0)).astype(BF16)
     w_all[x] = w_own[x]
 
-    greetings = (NX - 1) + (NT - 1) + 2 * (NZ - 1)
+    greetings = len(PLANE) + len(FAR_T) + len(FAR_Z)
     with jax.named_scope("wait_barrier"):
         pl.semaphore_wait(barrier, greetings + jnp.where(t != z, 1, 0))
 
-    ring_x = [(d, (z * NX + at_x(d), t)) for d in range(1, NX)]
-    ring_z = [(d, (at_z(d) * NX + x, t)) for d in range(1, NZ)]
-    ring_t = [(d, (kv, at_t(d))) for d in range(1, NT)]
+    ring_x = [(d, (z * NX + at_x(d), t)) for d in FAR_X]
+    ring_z = [(d, (at_z(d) * NX + x, t)) for d in FAR_Z]
+    ring_t = [(d, (kv, at_t(d))) for d in FAR_T]
     gather1 = go([send(w_own.at[at_x(d)], w_all.at[x], peer) for d, peer in ring_x])
     gather1 += go([send(x_all.at[x], x_all.at[x], peer) for d, peer in ring_x])
 
@@ -245,6 +246,7 @@
     own = jnp.where(t < 4, own, pltpu.roll(own, 64, 1))
     tok_own[...] = jnp.where(lane32 < 64, own[0:32], pltpu.roll(own[32:64], 64, 1)).astype(BF16)
     tok_all[z] = tok_own[...]
+    tok_blocks = go([send(tok_own, tok_all.at[z], peer) for d, peer in ring_z])
     w_diag[...] = jnp.zeros(w_diag.shape, BF16)
 
     with jax.named_scope("wait_gather1"):
@@ -265,18 +267,28 @@
         bottom += jnp.where(lane256 < 64, 0.0, wide)
     has_sums = x == NX - 1
     for j in range(NZ):
-        rows = slice(64 * (j % 4), 64 * (j % 4) + 64)
-        first = 256 * (j // 4)
-        part1[j, :, 0:128] = total[rows, first : first + 128].astype(BF16)
-        squares = as_pair(jnp.sum((top if j < 4 else bottom)[rows], axis=1, keepdims=True))
-        values = total[rows, first + 128 : first + 256]
-        part1[j, :, 128:256] = jnp.where(has_sums, squares.astype(F32), values).astype(BF16)
-    got1[z] = part1[z]
-    scatter1 = go([send(part1.at[at_z(d)], got1.at[z], peer) for d, peer in ring_z])
+        squares = as_pair(
+            jnp.sum((top if j < 4 else bottom)[64 * (j % 4) : 64 * (j % 4) + 64], axis=1, keepdims=True)
+        )
+        for k in range(NX):
+            rows = slice(64 * (j % 4) + 16 * k, 64 * (j % 4) + 16 * k + 16)
+            first = 256 * (j // 4)
+            part1[j, k, :, 0:128] = total[rows, first : first + 128].astype(BF16)
+            part1[j, k, :, 128:256] = jnp.where(
+                has_sums,
+                squares[16 * k : 16 * k + 16].astype(F32),
+                total[rows, first + 128 : first + 256],
+            ).astype(BF16)
+    got1[x, z] = part1[z, x]
+    scatter1 = go(
+        [
+            send(part1.at[at_z(dz), at_x(dx)], got1.at[x, z], (at_z(dz) * NX + at_x(dx), t))
+            for dz, dx in PLANE
+        ]
+    )
     mix_blocks = go(
         [send(w_mix.at[:, lanes_z], w_mix.at[:, lanes_z], peer) for d, peer in ring_z]
     )
-    tok_blocks = go([send(tok_own, tok_all.at[z], peer) for d, peer in ring_z])
 
     with jax.named_scope("wait_ff_blocks"):
         arrive(ff_blocks)
@@ -291,28 +303,20 @@
 
     with jax.named_scope("wait_scatter1"):
         arrive(scatter1)
-    total = got1[0].astype(F32)
-    for j in range(1, NZ):
-        total += got1[j].astype(F32)
-    squares = as_pair(of_pair(total[:, 128:256]))
+    proj = []
     for j in range(NX):
-        rows = slice(16 * j, 16 * j + 16)
-        sum1[j, :, 0:128] = total[rows, 0:128].astype(BF16)
-        sum1[j, :, 128:256] = jnp.where(
-            has_sums, squares[rows].astype(F32), total[rows, 128:256]
-        ).astype(BF16)
-    proj[x] = sum1[x]
-    exchange1 = go([send(sum1.at[at_x(d)], proj.at[x], peer) for d, peer in ring_x])
+        total = got1[j, 0].astype(F32)
+        for k in range(1, NZ):
+            total += got1[j, k].astype(F32)
+        proj.append(total)
     load(STATE)
-    with jax.named_scope("wait_exchange1"):
-        arrive(exchange1)
-
-    inv = lax.rsqrt(of_pair(proj[3, :, 128:256].astype(F32)) / D + EPS)
-    query = proj[0, :, 0:128].astype(F32) * (inv * DK ** (-0.5))
-    keys = proj[0, :, 128:256].astype(F32) * inv
-    values = proj[1].astype(F32) * inv
-    gate = proj[2].astype(F32) * inv
-    decay_pre = proj[3, :, 0:128].astype(F32) * inv
+
+    inv = lax.rsqrt(of_pair(proj[3][:, 128:256]) / D + EPS)
+    query = proj[0][:, 0:128] * (inv * DK ** (-0.5))
+    keys = proj[0][:, 128:256] * inv
+    values = proj[1] * inv
+    gate = proj[2] * inv
+    decay_pre = proj[3][:, 0:128] * inv
     log_sigmoid = jnp.minimum(decay_pre, 0.0) - jnp.log1p(jnp.exp(-jnp.abs(decay_pre)))
     decay = jnp.exp(log_sigmoid / GATE_NORM + log_decay[...])
     columns = jnp.transpose(
@@ -467,24 +471,41 @@
         arrive(gather4)
     res_back = pltpu.make_async_copy(res_all, res_out, local_sems.at[16])
     res_back.start()
-    for copy in sent:
-        copy.wait_send()
+    with jax.named_scope("wait_sends"):
+        for copy in sent:
+            copy.wait_send()
 
     @pl.when(jnp.logical_not(diagonal))
     def _():
         spread[0].wait_send()
 
-    state_back.wait()
-    res_back.wait()
-
-
-def finish(res_all, state_in, result, state_out):
+    with jax.named_scope("wait_state_back"):
+        state_back.wait()
+    with jax.named_scope("wait_res_back"):
+        res_back.wait()
+
+
+def finish(blocks_in, state_in, result_out, state_out, blocks, state, result, sems):
+    first = pltpu.make_async_copy(blocks_in, blocks, sems.at[32])
+    first.start()
+    count = state.shape[0]
+    for i in range(count):
+        pltpu.make_async_copy(state_in.at[i], state.at[i], sems.at[i]).start()
+    first.wait()
     rows = []
     for j in range(NT):
-        block = res_all[j].astype(F32)
+        block = blocks[j].astype(F32)
         rows += [block, pltpu.roll(block, 64, 1)]
     rows = jnp.concatenate(rows, axis=0)
     result[...] = jnp.transpose(rows, (1, 0))[0:64].astype(BF16)
+    last = pltpu.make_async_copy(result, result_out, sems.at[33])
+    last.start()
+    for i in range(count):
+        pltpu.make_async_copy(state_in.at[i], state.at[i], sems.at[i]).wait()
+        pltpu.make_async_copy(state.at[i], state_out.at[i], sems.at[16 + i]).start()
+    for i in range(count):
+        pltpu.make_async_copy(state.at[i], state_out.at[i], sems.at[16 + i]).wait()
+    last.wait()
 
 
 def body(
@@ -504,7 +525,6 @@
     w_ffup,
     w_down,
 ):
-    vmem = pl.BlockSpec(memory_space=pltpu.VMEM)
     hbm = pl.BlockSpec(memory_space=pltpu.HBM)
     shape = state.shape
     arguments = (
@@ -540,10 +560,8 @@
             pltpu.VMEM((NX, 256, 128), BF16),
             pltpu.VMEM((NX, 64, 256), BF16),
             pltpu.VMEM((NX, 128, 512), BF16),
-            pltpu.VMEM((NZ, 64, 256), BF16),
-            pltpu.VMEM((NZ, 64, 256), BF16),
-            pltpu.VMEM((NX, 16, 256), BF16),
-            pltpu.VMEM((NX, 16, 256), BF16),
+            pltpu.VMEM((NZ, NX, 16, 256), BF16),
+            pltpu.VMEM((NX, NZ, 16, 256), BF16),
             pltpu.VMEM((NX, 16, 256), BF16),
             pltpu.VMEM((128, 1024), BF16),
             pltpu.VMEM((NT, 32, 128), BF16),
@@ -576,9 +594,15 @@
             jax.ShapeDtypeStruct((64, 512), BF16),
             jax.ShapeDtypeStruct((shape[0], DK, DV), F32),
         ),
-        in_specs=[vmem, hbm],
-        out_specs=(vmem, hbm),
-        input_output_aliases={1: 1},
+        in_specs=[hbm, hbm],
+        out_specs=(hbm, hbm),
+        scratch_shapes=[
+            pltpu.VMEM((NT, 32, 128), BF16),
+            pltpu.VMEM((shape[0], DK, DV), F32),
+            pltpu.VMEM((64, 512), BF16),
+            pltpu.SemaphoreType.DMA((34,)),
+        ],
+        compiler_params=pltpu.CompilerParams(vmem_limit_bytes=67043328),
     )(blocks, new_state)
     return (result.T, new_state.reshape(shape))
 

time: 72.4 us -> 67 us (0.925)
  local copies, waits for them, and re-layouts: 3.09 us -> 0 us
  Pallas kernels: 68.5 us -> 66.2 us
    pallas_call x1, Pallas kernels: 66.9 us -> 63.6 us  [body(): pl.pallas_call(kernel, out_shape=(jax.ShapeDtypeStruct((NT, 32, 128), BF1...]
    unnamed x1 -> x0, local copies, waits for them, and re-layouts: 3.09 us -> none
    pallas_call x1, Pallas kernels: 1.63 us -> 2.62 us  [body(): pl.pallas_call(finish, out_shape=(jax.ShapeDtypeStruct((64, 512), BF16),...]
where the time goes in v3:
time: 67 us; the launch traced here: 66.9 us
  Pallas kernels  66.2 us (99%)
    pallas_call x1, Pallas kernels, body(): pl.pallas_call(kernel, out_shape=(jax.ShapeDtypeStruct((NT, 32, 128), BF1...  63.6 us
    pallas_call x1, Pallas kernels, body(): pl.pallas_call(finish, out_shape=(jax.ShapeDtypeStruct((64, 512), BF16),...  2.62 us

profile of v3, /device:TPU:1, one launch (start us, length us, event | category | flops | bytes accessed | tf_op | source)
XLA Modules:
  0.0 66.9 jit_solution(18139312547298110104)
XLA Ops:
  0.6 63.6 %shard_map.158 = (bf16[8,32,128]{2,1,0:T(8,128)(2,1)}, f32[16,128,256]{2,1,0:T(8,128)}) custom-call(bf16[64,512]{1,0:T(8,128)(2,1)} %bitcast.13, bf16[1,64]{1,0:T(2,128)(2,1)} %bitcast.16, bf16[64,128]{1,0:T(8,128)(2,1)} %refs_2_.1, bf16[64,128]{1,0:T(8,128)(2,1)} %refs_3_.1, bf16[64,256]{1,0:T(8,128)(2,1)} %refs_4_.1, bf16[64,256]{1,0:T(8,128)(2,1)} %refs_5_.1, ...), custom_call_target="tpu_custom_call" | custom-call | tf_op jit(solution)/shard_map/pallas_call | solution.py:547
  64.3 2.6 %shard_map.159 = (bf16[64,512]{1,0:T(8,128)(2,1)}, f32[16,128,256]{2,1,0:T(8,128)}) custom-call(bf16[8,32,128]{2,1,0:T(8,128)(2,1)} %get-tuple-element.6.blocks_in, f32[16,128,256]{2,1,0:T(8,128)} %get-tuple-element.7.state_in), custom_call_target="tpu_custom_call" | custom-call | tf_op jit(solution)/shard_map/pallas_call | solution.py:591

commit v4 on v3

--- a/solution.py
+++ b/solution.py
@@ -19,14 +19,14 @@
 
 NX, NY, NZ = 4, 4, 8
 NT = 2 * NY
-COPIES = 136
-STATE = 8
+COPIES = 21
 FAR_X = [2, 1, 3]
+FAR_Y = [2, 1, 3]
 FAR_Z = [4, 3, 5, 2, 6, 1, 7]
 FAR_T = [4, 5, 2, 3, 6, 7, 1]
 PLANE = [(dz, dx) for dz in FAR_Z + [0] for dx in FAR_X + [0] if (dz, dx) != (0, 0)]
-FIRST = [0, 1, 2, 3, 4, 5, 6]
-LATER = [12, 13, 14, 10, 11, 7, 9, STATE]
+LOADS = [(0, 0), (1, 1), (2, 0), (3, 0), (4, 0), (5, 0), (6, 0)]
+LOADS += [(10, 3), (12, 2), (13, 2), (14, 2), (11, 4), (7, 5), (9, 6), (8, 7)]
 
 
 def sigmoid(value):
@@ -127,35 +127,34 @@
     def at_t(d):
         return lax.rem(t + d, NT)
 
-    sent = []
     counter = [0]
-
-    def new_sem(count=1):
-        first = counter[0]
-        counter[0] += count
-        return first
-
-    def send(src, dst, peer, sem=None, recv=None):
-        sem = new_sem() if sem is None else sem
-        copy = pltpu.make_async_remote_copy(
-            src_ref=src,
-            dst_ref=dst,
-            send_sem=send_sems.at[sem],
-            recv_sem=recv_sems.at[sem if recv is None else recv],
-            device_id=peer,
-            device_id_type=MESH,
-        )
-        return copy
-
-    def go(copies):
-        for copy in copies:
-            copy.start()
-        sent.extend(copies)
-        return copies
-
-    def arrive(copies):
-        for copy in copies:
-            copy.wait_recv()
+    unsent = []
+
+    class Exchange:
+        def __init__(self, size):
+            self.number = counter[0]
+            self.size = size
+            counter[0] += 1
+            unsent.append(self)
+
+        def send(self, src, dst, peer):
+            pltpu.make_async_remote_copy(
+                src_ref=src,
+                dst_ref=dst,
+                send_sem=send_sems.at[self.number],
+                recv_sem=recv_sems.at[self.number],
+                device_id=peer,
+                device_id_type=MESH,
+            ).start()
+
+        def wait(self, sems, size):
+            pltpu.make_async_copy(size, size, sems.at[self.number]).wait()
+
+        def arrive(self):
+            self.wait(recv_sems, self.size)
+
+        def leave(self):
+            self.wait(send_sems, self.size)
 
     barrier = pltpu.get_barrier_semaphore()
 
@@ -173,19 +172,15 @@
     def _():
         greet((kv, z))
 
-    loads = [
-        pltpu.make_async_copy(src, dst, local_sems.at[i])
-        for i, (src, dst) in enumerate(zip(inputs, held))
-    ]
-    for i in FIRST + LATER:
-        loads[i].start()
-
-    def load(*numbers):
-        for i in numbers:
-            loads[i].wait()
+    for i, sem in LOADS:
+        pltpu.make_async_copy(inputs[i], held[i], local_sems.at[sem]).start()
+
+    def loaded(sem, size):
+        pltpu.make_async_copy(size, size, local_sems.at[sem]).wait()
 
     with jax.named_scope("wait_first"):
-        load(*FIRST)
+        loaded(0, part1.at[0:22])
+        loaded(1, norm_gain)
     square = (64, 64)
     row = lax.broadcasted_iota(jnp.int32, square, 0)
     column = lax.broadcasted_iota(jnp.int32, square, 1)
@@ -212,14 +207,48 @@
     with jax.named_scope("wait_barrier"):
         pl.semaphore_wait(barrier, greetings + jnp.where(t != z, 1, 0))
 
+    tile_z = w_mix.at[:, 0:128]
+
+    def lanes_of(block):
+        return pl.ds(pl.multiple_of(block * 128, 128), 128)
+
     ring_x = [(d, (z * NX + at_x(d), t)) for d in FAR_X]
     ring_z = [(d, (at_z(d) * NX + x, t)) for d in FAR_Z]
     ring_t = [(d, (kv, at_t(d))) for d in FAR_T]
-    gather1 = go([send(w_own.at[at_x(d)], w_all.at[x], peer) for d, peer in ring_x])
-    gather1 += go([send(x_all.at[x], x_all.at[x], peer) for d, peer in ring_x])
+    gather_w, gather_x = Exchange(w_all.at[0:3]), Exchange(x_all.at[0:3])
+    for d, peer in ring_x:
+        gather_w.send(w_own.at[at_x(d)], w_all.at[x], peer)
+    for d, peer in ring_x:
+        gather_x.send(x_all.at[x], x_all.at[x], peer)
 
     with jax.named_scope("wait_later"):
-        load(*[i for i in LATER if i != STATE])
+        loaded(3, w_out)
+    out_rows = jnp.concatenate([w_out[:, 0:128], w_out[:, 128:256]], axis=0).astype(F32)
+    w_mix[:, lanes_of(z)] = jnp.transpose(out_rows, (1, 0)).astype(BF16)
+    mix_steps = []
+
+    def mix_step(step):
+        if step > 1:
+            for exchange in mix_steps[-1]:
+                exchange.arrive()
+        exchanges = []
+        for way in (1, -1):
+            if step <= (4 if way > 0 else 3):
+                lanes = lanes_of(at_z(NZ - way * (step - 1)))
+                exchange = Exchange(tile_z)
+                exchange.send(
+                    w_mix.at[:, lanes], w_mix.at[:, lanes], (at_z(NZ + way) * NX + x, t)
+                )
+                exchanges.append(exchange)
+        mix_steps.append(exchanges)
+
+    mix_step(1)
+
+    with jax.named_scope("wait_later"):
+        loaded(2, ff_all.at[0, 0:3])
+        loaded(4, mixer_gain)
+        loaded(5, log_decay)
+        loaded(6, out_gain)
     gains = mixer_gain[...].astype(F32)
     units = jnp.transpose(
         jnp.concatenate([w_ffgate[...], w_ffup[...]], axis=0).astype(F32), (1, 0)
@@ -233,24 +262,23 @@
         ff_own[j, 0] = units[low]
         ff_own[j, 1] = units[high]
         ff_own[j, 2] = down[low]
-    lanes_z = pl.ds(pl.multiple_of(z * 128, 128), 128)
+    lanes_z = lanes_of(z)
     ff_all[:, t, :, lanes_z] = ff_own[z]
-    ff_blocks = go(
-        [send(ff_own.at[at_z(d)], ff_all.at[:, t, :, lanes_z], peer) for d, peer in ring_z]
-    )
-    out_rows = jnp.concatenate([w_out[:, 0:128], w_out[:, 128:256]], axis=0).astype(F32)
-    w_mix[:, lanes_z] = jnp.transpose(out_rows, (1, 0)).astype(BF16)
+    ff_blocks = Exchange(ff_own.at[0:7])
+    for d, peer in ring_z:
+        ff_blocks.send(ff_own.at[at_z(d)], ff_all.at[:, t, :, lanes_z], peer)
     lane32 = lax.broadcasted_iota(jnp.int32, (32, 128), 1)
     rows = pl.multiple_of(64 * lax.rem(t, 4), 64)
     own = x_all[x, pl.ds(rows, 64), :].astype(F32)
     own = jnp.where(t < 4, own, pltpu.roll(own, 64, 1))
     tok_own[...] = jnp.where(lane32 < 64, own[0:32], pltpu.roll(own[32:64], 64, 1)).astype(BF16)
     tok_all[z] = tok_own[...]
-    tok_blocks = go([send(tok_own, tok_all.at[z], peer) for d, peer in ring_z])
     w_diag[...] = jnp.zeros(w_diag.shape, BF16)
 
     with jax.named_scope("wait_gather1"):
-        arrive(gather1)
+        gather_w.arrive()
+        gather_x.arrive()
+    mix_step(2)
     lane256 = lax.broadcasted_iota(jnp.int32, (256, 128), 1)
     total = jnp.zeros((256, 512), F32)
     top = jnp.zeros((256, 128), F32)
@@ -273,43 +301,40 @@
         for k in range(NX):
             rows = slice(64 * (j % 4) + 16 * k, 64 * (j % 4) + 16 * k + 16)
             first = 256 * (j // 4)
-            part1[j, k, :, 0:128] = total[rows, first : first + 128].astype(BF16)
-            part1[j, k, :, 128:256] = jnp.where(
+            part1[NX * j + k, :, 0:128] = total[rows, first : first + 128].astype(BF16)
+            part1[NX * j + k, :, 128:256] = jnp.where(
                 has_sums,
                 squares[16 * k : 16 * k + 16].astype(F32),
                 total[rows, first + 128 : first + 256],
             ).astype(BF16)
-    got1[x, z] = part1[z, x]
-    scatter1 = go(
-        [
-            send(part1.at[at_z(dz), at_x(dx)], got1.at[x, z], (at_z(dz) * NX + at_x(dx), t))
-            for dz, dx in PLANE
-        ]
-    )
-    mix_blocks = go(
-        [send(w_mix.at[:, lanes_z], w_mix.at[:, lanes_z], peer) for d, peer in ring_z]
-    )
+    got1[x * NZ + z] = part1[kv]
+    scatter1 = Exchange(got1.at[0:31])
+    for dz, dx in PLANE:
+        peer = at_z(dz) * NX + at_x(dx)
+        scatter1.send(part1.at[peer], got1.at[x * NZ + z], (peer, t))
+    tok_blocks = Exchange(tok_all.at[0:7])
+    for d, peer in ring_z:
+        tok_blocks.send(tok_own, tok_all.at[z], peer)
 
     with jax.named_scope("wait_ff_blocks"):
-        arrive(ff_blocks)
+        ff_blocks.arrive()
     partner = (kv, t + 1 - 2 * core)
-    ff_y = go(
-        [
-            send(ff_all.at[:, t], ff_all.at[:, t], (kv, lax.rem(y + d, NY) * 2 + core))
-            for d in range(1, NY)
-        ]
-    )
-    ff_core = go([send(ff_all.at[:, t], ff_all.at[:, t], partner)])
+    ff_y, ff_core = Exchange(ff_all.at[:, 0:3]), Exchange(ff_all.at[:, 0:4])
+    for d in FAR_Y:
+        ff_y.send(ff_all.at[:, t], ff_all.at[:, t], (kv, lax.rem(y + d, NY) * 2 + core))
+    ff_core.send(ff_all.at[:, t], ff_all.at[:, t], partner)
+    mix_step(3)
 
     with jax.named_scope("wait_scatter1"):
-        arrive(scatter1)
+        scatter1.arrive()
+    mix_step(4)
     proj = []
     for j in range(NX):
-        total = got1[j, 0].astype(F32)
+        total = got1[NZ * j].astype(F32)
         for k in range(1, NZ):
-            total += got1[j, k].astype(F32)
+            total += got1[NZ * j + k].astype(F32)
         proj.append(total)
-    load(STATE)
+    loaded(7, state)
 
     inv = lax.rsqrt(of_pair(proj[3][:, 128:256]) / D + EPS)
     query = proj[0][:, 0:128] * (inv * DK ** (-0.5))
@@ -336,75 +361,63 @@
         * out_gain[...]
     )
     mix[x] = (normed * (gate * sigmoid(gate))).astype(BF16)
-    gather2 = go([send(mix.at[x], mix.at[x], peer) for d, peer in ring_x])
-    state_back = pltpu.make_async_copy(new_state, state_out, local_sems.at[15])
+    gather2 = Exchange(mix.at[0:3])
+    for d, peer in ring_x:
+        gather2.send(mix.at[x], mix.at[x], peer)
+    state_back = pltpu.make_async_copy(new_state, state_out, local_sems.at[8])
     state_back.start()
 
     with jax.named_scope("wait_mix_blocks"):
-        arrive(mix_blocks)
+        for exchange in mix_steps[-1]:
+            exchange.arrive()
     with jax.named_scope("wait_gather2"):
-        arrive(gather2)
+        gather2.arrive()
     mixed = mix[...].reshape(64, DV)
     for j, block in enumerate(packed_products(mixed, w_mix[...], lane32)):
         part2[j] = block.astype(BF16)
     got2[t] = part2[t]
-    scatter2 = go([send(part2.at[at_t(d)], got2.at[t], peer) for d, peer in ring_t])
+    scatter2 = Exchange(got2.at[0:7])
+    for d, peer in ring_t:
+        scatter2.send(part2.at[at_t(d)], got2.at[t], peer)
     with jax.named_scope("wait_scatter2"):
-        arrive(scatter2)
+        scatter2.arrive()
     total = got2[0].astype(F32)
     for j in range(1, NT):
         total += got2[j].astype(F32)
     attn_own[...] = total.astype(BF16)
 
-    first_send, first_recv = new_sem(NT), 0
-    first_recv = first_send
-    spread = [
-        send(
-            attn_own,
-            attn_all.at[t],
-            (at_z(d) * NX + x, z),
-            sem=first_send + d,
-            recv=first_recv + t,
-        )
-        for d in range(NZ)
-    ]
+    spread = Exchange(attn_all)
     diagonal = t == z
+    for d in FAR_Z:
+        spread.send(attn_own, attn_all.at[t], (at_z(d) * NX + x, z))
+
+    @pl.when(jnp.logical_not(diagonal))
+    def _():
+        spread.send(attn_own, attn_all.at[t], (kv, z))
 
     @pl.when(diagonal)
     def _():
         attn_all[t] = attn_own[...]
 
-    @pl.when(jnp.logical_not(diagonal))
-    def _():
-        spread[0].start()
-
-    go(spread[1:])
+    def spread_wait(sems):
+        @pl.when(diagonal)
+        def _():
+            spread.wait(sems, attn_all.at[0:7])
+
+        @pl.when(jnp.logical_not(diagonal))
+        def _():
+            spread.wait(sems, attn_all)
 
     with jax.named_scope("wait_ff_y"):
-        arrive(ff_y)
+        ff_y.arrive()
     for d in range(1, NY):
         other = lax.rem(y + d, NY) * 2 + core
-        ff_core += go([send(ff_all.at[:, other], ff_all.at[:, other], partner)])
+        ff_core.send(ff_all.at[:, other], ff_all.at[:, other], partner)
 
     with jax.named_scope("wait_tok_blocks"):
-        arrive(tok_blocks)
-    def wait_spread(j):
-        copy = pltpu.make_async_remote_copy(
-            src_ref=attn_own,
-            dst_ref=attn_all.at[j],
-            send_sem=send_sems.at[first_send],
-            recv_sem=recv_sems.at[first_recv + j],
-            device_id=(kv, t),
-            device_id_type=MESH,
-        )
-
-        @pl.when(jnp.logical_or(t != z, j != t))
-        def _(copy=copy):
-            copy.wait_recv()
-
+        tok_blocks.arrive()
     with jax.named_scope("wait_spread"):
-        for j in range(NT):
-            wait_spread(j)
+        spread_wait(recv_sems)
 
     top = jnp.zeros((32, 128), F32)
     bottom = jnp.zeros((32, 128), F32)
@@ -429,7 +442,7 @@
         )
     )
     with jax.named_scope("wait_ff_core"):
-        arrive(ff_core)
+        ff_core.arrive()
     weights = ff_all[0:2].reshape(NT * 96, 1024)
     terms = lax.dot_general(
         left, weights, (((1,), (1,)), ((), ())), preferred_element_type=F32
@@ -440,45 +453,51 @@
         part3[j, :, 768:1536] = terms[64 + 16 * j : 80 + 16 * j].astype(BF16)
         part3[j, :, 1536:1664] = squares[rows]
     got3[x] = part3[x]
-    scatter3 = go([send(part3.at[at_x(d)], got3.at[x], peer) for d, peer in ring_x])
+    scatter3 = Exchange(got3.at[0:3])
+    for d, peer in ring_x:
+        scatter3.send(part3.at[at_x(d)], got3.at[x], peer)
     with jax.named_scope("wait_scatter3"):
-        arrive(scatter3)
+        scatter3.arrive()
     total = got3[0].astype(F32)
     for j in range(1, NX):
         total += got3[j].astype(F32)
     inv = lax.rsqrt(of_pair(total[:, 1536:1664]) / D + EPS)
     gate = total[:, 0:768] * inv
     hid[x] = (gate * sigmoid(gate) * (total[:, 768:1536] * inv)).astype(BF16)
-    gather3 = go([send(hid.at[x], hid.at[x], peer) for d, peer in ring_x])
+    gather3 = Exchange(hid.at[0:3])
+    for d, peer in ring_x:
+        gather3.send(hid.at[x], hid.at[x], peer)
     with jax.named_scope("wait_gather3"):
-        arrive(gather3)
+        gather3.arrive()
 
     hidden = hid[...].reshape(64, 768)
     weights = ff_all[2].reshape(NT * 48, 1024)
     for j, block in enumerate(packed_products(hidden, weights, lane32)):
         part4[j] = block.astype(BF16)
     got4[z] = part4[z]
-    scatter4 = go([send(part4.at[at_z(d)], got4.at[z], peer) for d, peer in ring_z])
+    scatter4 = Exchange(got4.at[0:7])
+    for d, peer in ring_z:
+        scatter4.send(part4.at[at_z(d)], got4.at[z], peer)
     with jax.named_scope("wait_scatter4"):
-        arrive(scatter4)
+        scatter4.arrive()
     total = got4[0].astype(F32)
     for j in range(1, NZ):
         total += got4[j].astype(F32)
     res_own[...] = (middle[z].astype(F32) + total).astype(BF16)
     res_all[t] = res_own[...]
-    gather4 = go([send(res_own, res_all.at[t], peer) for d, peer in ring_t])
+    gather4 = Exchange(res_all.at[0:7])
+    for d, peer in ring_t:
+        gather4.send(res_own, res_all.at[t], peer)
     with jax.named_scope("wait_gather4"):
-        arrive(gather4)
-    res_back = pltpu.make_async_copy(res_all, res_out, local_sems.at[16])
+        gather4.arrive()
+    res_back = pltpu.make_async_copy(res_all, res_out, local_sems.at[9])
     res_back.start()
     with jax.named_scope("wait_sends"):
-        for copy in sent:
-            copy.wait_send()
-
-    @pl.when(jnp.logical_not(diagonal))
-    def _():
-        spread[0].wait_send()
-
+        for exchange in unsent:
+            if exchange is spread:
+                spread_wait(send_sems)
+            else:
+                exchange.leave()
     with jax.named_scope("wait_state_back"):
         state_back.wait()
     with jax.named_scope("wait_res_back"):
@@ -486,11 +505,13 @@
 
 
 def finish(blocks_in, state_in, result_out, state_out, blocks, state, result, sems):
-    first = pltpu.make_async_copy(blocks_in, blocks, sems.at[32])
+    first = pltpu.make_async_copy(blocks_in, blocks, sems.at[0])
+    last = pltpu.make_async_copy(result, result_out, sems.at[1])
+    everything = pltpu.make_async_copy(state, state, sems.at[2])
+    parts = [pl.ds(2 * i, 2) for i in range(8)]
     first.start()
-    count = state.shape[0]
-    for i in range(count):
-        pltpu.make_async_copy(state_in.at[i], state.at[i], sems.at[i]).start()
+    for i, part in enumerate(parts):
+        pltpu.make_async_copy(state_in.at[part], state.at[part], sems.at[3 + i]).start()
     first.wait()
     rows = []
     for j in range(NT):
@@ -498,13 +519,11 @@
         rows += [block, pltpu.roll(block, 64, 1)]
     rows = jnp.concatenate(rows, axis=0)
     result[...] = jnp.transpose(rows, (1, 0))[0:64].astype(BF16)
-    last = pltpu.make_async_copy(result, result_out, sems.at[33])
     last.start()
-    for i in range(count):
-        pltpu.make_async_copy(state_in.at[i], state.at[i], sems.at[i]).wait()
-        pltpu.make_async_copy(state.at[i], state_out.at[i], sems.at[16 + i]).start()
-    for i in range(count):
-        pltpu.make_async_copy(state.at[i], state_out.at[i], sems.at[16 + i]).wait()
+    for i, part in enumerate(parts):
+        pltpu.make_async_copy(state_in.at[part], state.at[part], sems.at[3 + i]).wait()
+        pltpu.make_async_copy(state.at[part], state_out.at[part], sems.at[2]).start()
+    everything.wait()
     last.wait()
 
 
@@ -560,8 +579,8 @@
             pltpu.VMEM((NX, 256, 128), BF16),
             pltpu.VMEM((NX, 64, 256), BF16),
             pltpu.VMEM((NX, 128, 512), BF16),
-            pltpu.VMEM((NZ, NX, 16, 256), BF16),
-            pltpu.VMEM((NX, NZ, 16, 256), BF16),
+            pltpu.VMEM((NZ * NX, 16, 256), BF16),
+            pltpu.VMEM((NX * NZ, 16, 256), BF16),
             pltpu.VMEM((NX, 16, 256), BF16),
             pltpu.VMEM((128, 1024), BF16),
             pltpu.VMEM((NT, 32, 128), BF16),
@@ -582,7 +601,7 @@
             pltpu.VMEM((NT, 32, 128), BF16),
             pltpu.SemaphoreType.DMA((COPIES,)),
             pltpu.SemaphoreType.DMA((COPIES,)),
-            pltpu.SemaphoreType.DMA((17,)),
+            pltpu.SemaphoreType.DMA((10,)),
         ],
         compiler_params=pltpu.CompilerParams(
             collective_id=0, has_side_effects=True, vmem_limit_bytes=67043328
@@ -600,7 +619,7 @@
             pltpu.VMEM((NT, 32, 128), BF16),
             pltpu.VMEM((shape[0], DK, DV), F32),
             pltpu.VMEM((64, 512), BF16),
-            pltpu.SemaphoreType.DMA((34,)),
+            pltpu.SemaphoreType.DMA((11,)),
         ],
         compiler_params=pltpu.CompilerParams(vmem_limit_bytes=67043328),
     )(blocks, new_state)

time: 67 us -> 65 us (0.970)
  Pallas kernels: 66.2 us -> 64.2 us
    pallas_call x1, Pallas kernels: 63.6 us -> 61.8 us  [body(): pl.pallas_call(kernel, out_shape=(jax.ShapeDtypeStruct((NT, 32, 128), BF1...]
where the time goes in v4:
time: 65 us; the launch traced here: 64.8 us
  Pallas kernels  64.2 us (99%)
    pallas_call x1, Pallas kernels, body(): pl.pallas_call(kernel, out_shape=(jax.ShapeDtypeStruct((NT, 32, 128), BF1...  61.8 us
    pallas_call x1, Pallas kernels, body(): pl.pallas_call(finish, out_shape=(jax.ShapeDtypeStruct((64, 512), BF16),...  2.42 us

profile of v4, /device:TPU:1, one launch (start us, length us, event | category | flops | bytes accessed | tf_op | source)
XLA Modules:
  0.0 64.8 jit_solution(15868851831512608673)
XLA Ops:
  0.6 61.8 %shard_map.158 = (bf16[8,32,128]{2,1,0:T(8,128)(2,1)}, f32[16,128,256]{2,1,0:T(8,128)}) custom-call(bf16[64,512]{1,0:T(8,128)(2,1)} %bitcast.13, bf16[1,64]{1,0:T(2,128)(2,1)} %bitcast.16, bf16[64,128]{1,0:T(8,128)(2,1)} %refs_2_.1, bf16[64,128]{1,0:T(8,128)(2,1)} %refs_3_.1, bf16[64,256]{1,0:T(8,128)(2,1)} %refs_4_.1, bf16[64,256]{1,0:T(8,128)(2,1)} %refs_5_.1, ...), custom_call_target="tpu_custom_call" | custom-call | tf_op jit(solution)/shard_map/pallas_call | solution.py:566
  62.4 2.4 %shard_map.159 = (bf16[64,512]{1,0:T(8,128)(2,1)}, f32[16,128,256]{2,1,0:T(8,128)}) custom-call(bf16[8,32,128]{2,1,0:T(8,128)(2,1)} %get-tuple-element.6.blocks_in, f32[16,128,256]{2,1,0:T(8,128)} %get-tuple-element.7.state_in), custom_call_target="tpu_custom_call" | custom-call | tf_op jit(solution)/shard_map/pallas_call | solution.py:610

commit v5 on v4

--- a/solution.py
+++ b/solution.py
@@ -19,7 +19,7 @@
 
 NX, NY, NZ = 4, 4, 8
 NT = 2 * NY
-COPIES = 21
+COPIES = 24
 FAR_X = [2, 1, 3]
 FAR_Y = [2, 1, 3]
 FAR_Z = [4, 3, 5, 2, 6, 1, 7]
@@ -63,7 +63,7 @@
 
 
 def kernel(*refs):
-    inputs, (res_out, state_out), refs = refs[:15], refs[15:17], refs[17:]
+    inputs, (result, new_state), refs = refs[:15], refs[15:17], refs[17:]
     held, refs = refs[:15], refs[15:]
     (
         tokens,
@@ -83,7 +83,6 @@
         w_down,
     ) = held
     (
-        new_state,
         att,
         w_own,
         x_all,
@@ -100,8 +99,10 @@
         tok_own,
         tok_all,
         middle,
-        ff_own,
-        ff_all,
+        up_own,
+        up_all,
+        down_own,
+        down_all,
         part3,
         got3,
         hid,
@@ -156,6 +157,9 @@
         def leave(self):
             self.wait(send_sems, self.size)
 
+    for i, sem in LOADS:
+        pltpu.make_async_copy(inputs[i], held[i], local_sems.at[sem]).start()
+
     barrier = pltpu.get_barrier_semaphore()
 
     def greet(peer):
@@ -171,9 +175,6 @@
     @pl.when(t != z)
     def _():
         greet((kv, z))
-
-    for i, sem in LOADS:
-        pltpu.make_async_copy(inputs[i], held[i], local_sems.at[sem]).start()
 
     def loaded(sem, size):
         pltpu.make_async_copy(size, size, local_sems.at[sem]).wait()
@@ -245,7 +246,7 @@
     mix_step(1)
 
     with jax.named_scope("wait_later"):
-        loaded(2, ff_all.at[0, 0:3])
+        loaded(2, up_all.at[0, 0:3])
         loaded(4, mixer_gain)
         loaded(5, log_decay)
         loaded(6, out_gain)
@@ -258,15 +259,15 @@
     down = jnp.concatenate([down, pltpu.roll(down, 768 - 48, 1)], axis=0)
     down = jnp.transpose(down, (1, 0)).astype(BF16)
     for j in range(NZ):
-        low, high = slice(96 * j, 96 * j + 48), slice(96 * j + 48, 96 * j + 96)
-        ff_own[j, 0] = units[low]
-        ff_own[j, 1] = units[high]
-        ff_own[j, 2] = down[low]
+        up_own[j, 0] = units[96 * j : 96 * j + 48]
+        up_own[j, 1] = units[96 * j + 48 : 96 * j + 96]
+        down_own[j] = down[96 * j : 96 * j + 48]
     lanes_z = lanes_of(z)
-    ff_all[:, t, :, lanes_z] = ff_own[z]
-    ff_blocks = Exchange(ff_own.at[0:7])
+    up_all[:, t, :, lanes_z] = up_own[z]
+    down_all[t, :, lanes_z] = down_own[z]
+    up_blocks = Exchange(up_own.at[0:7])
     for d, peer in ring_z:
-        ff_blocks.send(ff_own.at[at_z(d)], ff_all.at[:, t, :, lanes_z], peer)
+        up_blocks.send(up_own.at[at_z(d)], up_all.at[:, t, :, lanes_z], peer)
     lane32 = lax.broadcasted_iota(jnp.int32, (32, 128), 1)
     rows = pl.multiple_of(64 * lax.rem(t, 4), 64)
     own = x_all[x, pl.ds(rows, 64), :].astype(F32)
@@ -312,17 +313,24 @@
     for dz, dx in PLANE:
         peer = at_z(dz) * NX + at_x(dx)
         scatter1.send(part1.at[peer], got1.at[x * NZ + z], (peer, t))
+    down_blocks = Exchange(down_own.at[0:7])
+    for d, peer in ring_z:
+        down_blocks.send(down_own.at[at_z(d)], down_all.at[t, :, lanes_z], peer)
     tok_blocks = Exchange(tok_all.at[0:7])
     for d, peer in ring_z:
         tok_blocks.send(tok_own, tok_all.at[z], peer)
 
-    with jax.named_scope("wait_ff_blocks"):
-        ff_blocks.arrive()
+    with jax.named_scope("wait_up_blocks"):
+        up_blocks.arrive()
     partner = (kv, t + 1 - 2 * core)
-    ff_y, ff_core = Exchange(ff_all.at[:, 0:3]), Exchange(ff_all.at[:, 0:4])
+
+    def along_y(d):
+        return lax.rem(y + d, NY) * 2 + core
+
+    up_y, up_core = Exchange(up_all.at[:, 0:3]), Exchange(up_all.at[:, 0:4])
     for d in FAR_Y:
-        ff_y.send(ff_all.at[:, t], ff_all.at[:, t], (kv, lax.rem(y + d, NY) * 2 + core))
-    ff_core.send(ff_all.at[:, t], ff_all.at[:, t], partner)
+        up_y.send(up_all.at[:, t], up_all.at[:, t], (kv, along_y(d)))
+    up_core.send(up_all.at[:, t], up_all.at[:, t], partner)
     mix_step(3)
 
     with jax.named_scope("wait_scatter1"):
@@ -364,8 +372,6 @@
     gather2 = Exchange(mix.at[0:3])
     for d, peer in ring_x:
         gather2.send(mix.at[x], mix.at[x], peer)
-    state_back = pltpu.make_async_copy(new_state, state_out, local_sems.at[8])
-    state_back.start()
 
     with jax.named_scope("wait_mix_blocks"):
         for exchange in mix_steps[-1]:
@@ -408,11 +414,17 @@
         def _():
             spread.wait(sems, attn_all)
 
-    with jax.named_scope("wait_ff_y"):
-        ff_y.arrive()
+    with jax.named_scope("wait_down_blocks"):
+        down_blocks.arrive()
+    down_y, down_core = Exchange(down_all.at[0:3]), Exchange(down_all.at[0:4])
+    for d in FAR_Y:
+        down_y.send(down_all.at[t], down_all.at[t], (kv, along_y(d)))
+    with jax.named_scope("wait_up_y"):
+        up_y.arrive()
     for d in range(1, NY):
-        other = lax.rem(y + d, NY) * 2 + core
-        ff_core.send(ff_all.at[:, other], ff_all.at[:, other], partner)
+        other = along_y(d)
+        up_core.send(up_all.at[:, other], up_all.at[:, other], partner)
+    down_core.send(down_all.at[t], down_all.at[t], partner)
 
     with jax.named_scope("wait_tok_blocks"):
         tok_blocks.arrive()
@@ -441,9 +453,9 @@
             [jnp.sum(top, axis=1, keepdims=True), jnp.sum(bottom, axis=1, keepdims=True)], axis=0
         )
     )
-    with jax.named_scope("wait_ff_core"):
-        ff_core.arrive()
-    weights = ff_all[0:2].reshape(NT * 96, 1024)
+    with jax.named_scope("wait_up_core"):
+        up_core.arrive()
+    weights = up_all[...].reshape(NT * 96, 1024)
     terms = lax.dot_general(
         left, weights, (((1,), (1,)), ((), ())), preferred_element_type=F32
     )
@@ -456,6 +468,11 @@
     scatter3 = Exchange(got3.at[0:3])
     for d, peer in ring_x:
         scatter3.send(part3.at[at_x(d)], got3.at[x], peer)
+    with jax.named_scope("wait_down_y"):
+        down_y.arrive()
+    for d in range(1, NY):
+        other = along_y(d)
+        down_core.send(down_all.at[other], down_all.at[other], partner)
     with jax.named_scope("wait_scatter3"):
         scatter3.arrive()
     total = got3[0].astype(F32)
@@ -467,11 +484,13 @@
     gather3 = Exchange(hid.at[0:3])
     for d, peer in ring_x:
         gather3.send(hid.at[x], hid.at[x], peer)
+    with jax.named_scope("wait_down_core"):
+        down_core.arrive()
     with jax.named_scope("wait_gather3"):
         gather3.arrive()
 
     hidden = hid[...].reshape(64, 768)
-    weights = ff_all[2].reshape(NT * 48, 1024)
+    weights = down_all[...].reshape(NT * 48, 1024)
     for j, block in enumerate(packed_products(hidden, weights, lane32)):
         part4[j] = block.astype(BF16)
     got4[z] = part4[z]
@@ -490,41 +509,28 @@
         gather4.send(res_own, res_all.at[t], peer)
     with jax.named_scope("wait_gather4"):
         gather4.arrive()
-    res_back = pltpu.make_async_copy(res_all, res_out, local_sems.at[9])
-    res_back.start()
+    rows = []
+    for j in range(NT):
+        block = res_all[j].astype(F32)
+        rows += [block, pltpu.roll(block, 64, 1)]
+    rows = jnp.concatenate(rows, axis=0)
+    result[...] = jnp.transpose(rows, (1, 0))[0:64].astype(BF16)
     with jax.named_scope("wait_sends"):
         for exchange in unsent:
             if exchange is spread:
                 spread_wait(send_sems)
             else:
                 exchange.leave()
-    with jax.named_scope("wait_state_back"):
-        state_back.wait()
-    with jax.named_scope("wait_res_back"):
-        res_back.wait()
-
-
-def finish(blocks_in, state_in, result_out, state_out, blocks, state, result, sems):
-    first = pltpu.make_async_copy(blocks_in, blocks, sems.at[0])
-    last = pltpu.make_async_copy(result, result_out, sems.at[1])
-    everything = pltpu.make_async_copy(state, state, sems.at[2])
+
+def finish(result_in, state_in, result_out, state_out, sems):
+    result = pltpu.make_async_copy(result_in, result_out, sems.at[0])
+    states = pltpu.make_async_copy(state_in, state_out, sems.at[1])
     parts = [pl.ds(2 * i, 2) for i in range(8)]
-    first.start()
-    for i, part in enumerate(parts):
-        pltpu.make_async_copy(state_in.at[part], state.at[part], sems.at[3 + i]).start()
-    first.wait()
-    rows = []
-    for j in range(NT):
-        block = blocks[j].astype(F32)
-        rows += [block, pltpu.roll(block, 64, 1)]
-    rows = jnp.concatenate(rows, axis=0)
-    result[...] = jnp.transpose(rows, (1, 0))[0:64].astype(BF16)
-    last.start()
-    for i, part in enumerate(parts):
-        pltpu.make_async_copy(state_in.at[part], state.at[part], sems.at[3 + i]).wait()
-        pltpu.make_async_copy(state.at[part], state_out.at[part], sems.at[2]).start()
-    everything.wait()
-    last.wait()
+    result.start()
+    for part in parts:
+        pltpu.make_async_copy(state_in.at[part], state_out.at[part], sems.at[1]).start()
+    result.wait()
+    states.wait()
 
 
 def body(
@@ -544,6 +550,7 @@
     w_ffup,
     w_down,
 ):
+    vmem = pl.BlockSpec(memory_space=pltpu.VMEM)
     hbm = pl.BlockSpec(memory_space=pltpu.HBM)
     shape = state.shape
     arguments = (
@@ -563,17 +570,17 @@
         w_ffup,
         w_down.T,
     )
-    blocks, new_state = pl.pallas_call(
+    arguments = [pltpu.with_memory_space_constraint(value, pltpu.HBM) for value in arguments]
+    result, new_state = pl.pallas_call(
         kernel,
         out_shape=(
-            jax.ShapeDtypeStruct((NT, 32, 128), BF16),
-            jax.ShapeDtypeStruct((shape[0], DK, DV), F32),
+            pltpu.VMEM((64, 512), BF16),
+            pltpu.VMEM((shape[0], DK, DV), F32),
         ),
         in_specs=[hbm] * 15,
-        out_specs=(hbm, hbm),
+        out_specs=(vmem, vmem),
         scratch_shapes=[pltpu.VMEM(value.shape, value.dtype) for value in arguments]
         + [
-            pltpu.VMEM((16, DK, DV), F32),
             pltpu.VMEM((16, DV), F32),
             pltpu.VMEM((NX, 64, 256), BF16),
             pltpu.VMEM((NX, 256, 128), BF16),
@@ -590,8 +597,10 @@
             pltpu.VMEM((32, 128), BF16),
             pltpu.VMEM((NZ, 32, 128), BF16),
             pltpu.VMEM((NZ, 32, 128), BF16),
-            pltpu.VMEM((NZ, 3, 48, 128), BF16),
-            pltpu.VMEM((3, NT, 48, 1024), BF16),
+            pltpu.VMEM((NZ, 2, 48, 128), BF16),
+            pltpu.VMEM((2, NT, 48, 1024), BF16),
+            pltpu.VMEM((NZ, 48, 128), BF16),
+            pltpu.VMEM((NT, 48, 1024), BF16),
             pltpu.VMEM((NX, 16, 1664), BF16),
             pltpu.VMEM((NX, 16, 1664), BF16),
             pltpu.VMEM((NX, 16, 768), BF16),
@@ -601,10 +610,10 @@
             pltpu.VMEM((NT, 32, 128), BF16),
             pltpu.SemaphoreType.DMA((COPIES,)),
             pltpu.SemaphoreType.DMA((COPIES,)),
-            pltpu.SemaphoreType.DMA((10,)),
+            pltpu.SemaphoreType.DMA((8,)),
         ],
         compiler_params=pltpu.CompilerParams(
-            collective_id=0, has_side_effects=True, vmem_limit_bytes=67043328
+            collective_id=0, has_side_effects=True, vmem_limit_bytes=40 * 1024 * 1024
         ),
     )(*arguments)
     result, new_state = pl.pallas_call(
@@ -613,16 +622,11 @@
             jax.ShapeDtypeStruct((64, 512), BF16),
             jax.ShapeDtypeStruct((shape[0], DK, DV), F32),
         ),
-        in_specs=[hbm, hbm],
+        in_specs=[vmem, vmem],
         out_specs=(hbm, hbm),
-        scratch_shapes=[
-            pltpu.VMEM((NT, 32, 128), BF16),
-            pltpu.VMEM((shape[0], DK, DV), F32),
-            pltpu.VMEM((64, 512), BF16),
-            pltpu.SemaphoreType.DMA((11,)),
-        ],
-        compiler_params=pltpu.CompilerParams(vmem_limit_bytes=67043328),
-    )(blocks, new_state)
+        scratch_shapes=[pltpu.SemaphoreType.DMA((2,))],
+        compiler_params=pltpu.CompilerParams(vmem_limit_bytes=8 * 1024 * 1024),
+    )(result, new_state)
     return (result.T, new_state.reshape(shape))
 
 

time: 65 us -> 64.4 us (level)
    pallas_call x1, Pallas kernels: 2.42 us -> 1.34 us  [body(): pl.pallas_call(finish, out_shape=(jax.ShapeDtypeStruct((64, 512), BF16),...]
where the time goes in v5:
time: 64.4 us; the launch traced here: 64.3 us
  Pallas kernels  63.6 us (99%)
    pallas_call x1, Pallas kernels, body(): pl.pallas_call(kernel, out_shape=(pltpu.VMEM((64, 512), BF16), pltpu.VMEM...  62.3 us
    pallas_call x1, Pallas kernels, body(): pl.pallas_call(finish, out_shape=(jax.ShapeDtypeStruct((64, 512), BF16),...  1.34 us

profile of v5, /device:TPU:1, one launch (start us, length us, event | category | flops | bytes accessed | tf_op | source)
XLA Modules:
  0.0 64.3 jit_solution(1092088574859184866)
XLA Ops:
  0.6 62.3 %shard_map.158 = (bf16[64,512]{1,0:T(8,128)(2,1)S(1)}, f32[16,128,256]{2,1,0:T(8,128)S(1)}) custom-call(bf16[64,512]{1,0:T(8,128)(2,1)} %bitcast.13, bf16[1,64]{1,0:T(2,128)(2,1)} %bitcast.16, bf16[64,128]{1,0:T(8,128)(2,1)} %refs_2_.1, bf16[64,128]{1,0:T(8,128)(2,1)} %refs_3_.1, bf16[64,256]{1,0:T(8,128)(2,1)} %refs_4_.1, bf16[64,256]{1,0:T(8,128)(2,1)} %refs_5_.1, ...), custom_call_target="tpu_custom_call" | custom-call | tf_op jit(solution)/shard_map/pallas_call | solution.py:574
  62.9 1.3 %shard_map.159 = (bf16[64,512]{1,0:T(8,128)(2,1)}, f32[16,128,256]{2,1,0:T(8,128)}) custom-call(bf16[64,512]{1,0:T(8,128)(2,1)S(1)} %get-tuple-element.6.result_in, f32[16,128,256]{2,1,0:T(8,128)S(1)} %get-tuple-element.7.state_in), custom_call_target="tpu_custom_call" | custom-call | tf_op jit(solution)/shard_map/pallas_call | solution.py:619

commit v6 on v5

--- a/solution.py
+++ b/solution.py
@@ -19,7 +19,7 @@
 
 NX, NY, NZ = 4, 4, 8
 NT = 2 * NY
-COPIES = 24
+COPIES = 27
 FAR_X = [2, 1, 3]
 FAR_Y = [2, 1, 3]
 FAR_Z = [4, 3, 5, 2, 6, 1, 7]
@@ -48,16 +48,13 @@
     return pair[:, 0:1] + pair[:, 64:65]
 
 
-def packed_products(left, right, lane):
-    width = left.shape[1] // 2
-    stacked = jnp.concatenate([left[:, :width], left[:, width:]], axis=0)
-    total = jnp.dot(stacked, right, preferred_element_type=F32)
+def packed_products(first, second, lane):
     blocks = []
     for j in range(8):
-        first = total[0:64, 128 * j : 128 * j + 128]
-        second = total[64:128, 128 * j : 128 * j + 128]
-        top = first[0:32] + pltpu.roll(second[0:32], 64, 1)
-        bottom = pltpu.roll(first[32:64], 64, 1) + second[32:64]
+        low = first[:, 128 * j : 128 * j + 128]
+        high = second[:, 128 * j : 128 * j + 128]
+        top = low[0:32] + pltpu.roll(high[0:32], 64, 1)
+        bottom = pltpu.roll(low[32:64], 64, 1) + high[32:64]
         blocks.append(jnp.where(lane < 64, top, bottom))
     return blocks
 
@@ -103,8 +100,10 @@
         up_all,
         down_own,
         down_all,
-        part3,
-        got3,
+        part3a,
+        got3a,
+        part3b,
+        got3b,
         hid,
         part4,
         got4,
@@ -201,7 +200,7 @@
     w_own[3, :, 0:128] = gained(w_decay)
     w_own[3, :, 128:256] = jnp.zeros((64, 128), BF16)
     own = jnp.concatenate([tokens[:, 0:256], tokens[:, 256:512]], axis=0).astype(F32)
-    x_all[x] = jnp.transpose(own, (1, 0)).astype(BF16)
+    x_all[x] = jnp.transpose(own, (1, 0)).astype(BF16).reshape(4, 64, 128)
     w_all[x] = w_own[x]
 
     greetings = len(PLANE) + len(FAR_T) + len(FAR_Z)
@@ -216,11 +215,15 @@
     ring_x = [(d, (z * NX + at_x(d), t)) for d in FAR_X]
     ring_z = [(d, (at_z(d) * NX + x, t)) for d in FAR_Z]
     ring_t = [(d, (kv, at_t(d))) for d in FAR_T]
-    gather_w, gather_x = Exchange(w_all.at[0:3]), Exchange(x_all.at[0:3])
+    gather_w = Exchange(w_all.at[0:3])
+    gather_x = [Exchange(x_all.at[0:3, 0:2]) for half in range(2)]
+    halves_z = [[lax.rem(z + d, 4) for d in steps] for steps in ((1, 2), (0, 3))]
     for d, peer in ring_x:
         gather_w.send(w_own.at[at_x(d)], w_all.at[x], peer)
-    for d, peer in ring_x:
-        gather_x.send(x_all.at[x], x_all.at[x], peer)
+    for half in range(2):
+        for d, peer in ring_x:
+            for r in halves_z[half]:
+                gather_x[half].send(x_all.at[x, r], x_all.at[x, r], peer)
 
     with jax.named_scope("wait_later"):
         loaded(3, w_out)
@@ -269,56 +272,56 @@
     for d, peer in ring_z:
         up_blocks.send(up_own.at[at_z(d)], up_all.at[:, t, :, lanes_z], peer)
     lane32 = lax.broadcasted_iota(jnp.int32, (32, 128), 1)
-    rows = pl.multiple_of(64 * lax.rem(t, 4), 64)
-    own = x_all[x, pl.ds(rows, 64), :].astype(F32)
+    own = x_all[x, lax.rem(t, 4)].astype(F32)
     own = jnp.where(t < 4, own, pltpu.roll(own, 64, 1))
     tok_own[...] = jnp.where(lane32 < 64, own[0:32], pltpu.roll(own[32:64], 64, 1)).astype(BF16)
     tok_all[z] = tok_own[...]
     w_diag[...] = jnp.zeros(w_diag.shape, BF16)
 
-    with jax.named_scope("wait_gather1"):
+    with jax.named_scope("wait_mix_step"):
+        mix_step(2)
+
+    with jax.named_scope("wait_gather1_w"):
         gather_w.arrive()
-        gather_x.arrive()
-    mix_step(2)
-    lane256 = lax.broadcasted_iota(jnp.int32, (256, 128), 1)
-    total = jnp.zeros((256, 512), F32)
-    top = jnp.zeros((256, 128), F32)
-    bottom = jnp.zeros((256, 128), F32)
     for j in range(NX):
         w_diag[j, 0:64, 0:256] = w_all[j]
         w_diag[j, 64:128, 256:512] = w_all[j]
-    for j in range(NX):
-        block = x_all[j]
-        total += jnp.dot(block, w_diag[j], preferred_element_type=F32)
-        wide = block.astype(F32)
-        wide = wide * wide
-        top += jnp.where(lane256 < 64, wide, 0.0)
-        bottom += jnp.where(lane256 < 64, 0.0, wide)
+    lane128 = lax.broadcasted_iota(jnp.int32, (128, 128), 1)
     has_sums = x == NX - 1
-    for j in range(NZ):
-        squares = as_pair(
-            jnp.sum((top if j < 4 else bottom)[64 * (j % 4) : 64 * (j % 4) + 64], axis=1, keepdims=True)
-        )
-        for k in range(NX):
-            rows = slice(64 * (j % 4) + 16 * k, 64 * (j % 4) + 16 * k + 16)
-            first = 256 * (j // 4)
-            part1[NX * j + k, :, 0:128] = total[rows, first : first + 128].astype(BF16)
-            part1[NX * j + k, :, 128:256] = jnp.where(
-                has_sums,
-                squares[16 * k : 16 * k + 16].astype(F32),
-                total[rows, first + 128 : first + 256],
-            ).astype(BF16)
+    scatter1 = Exchange(got1.at[0:31])
+    for half, (blocks, steps) in enumerate(zip(halves_z, ([5, 2, 6, 1], [4, 3, 7, 0]))):
+        with jax.named_scope(f"wait_gather1_{half}"):
+            gather_x[half].arrive()
+        total = jnp.zeros((128, 512), F32)
+        sums = [jnp.zeros((128, 128), F32)] * 2
+        for j in range(NX):
+            block = jnp.concatenate([x_all[j, r] for r in blocks], axis=0)
+            total += jnp.dot(block, w_diag[j], preferred_element_type=F32)
+            wide = block.astype(F32)
+            wide = wide * wide
+            sums[0] += jnp.where(lane128 < 64, wide, 0.0)
+            sums[1] += jnp.where(lane128 < 64, 0.0, wide)
+        for i, r in enumerate(blocks):
+            for side in range(2):
+                squares = as_pair(
+                    jnp.sum(sums[side][64 * i : 64 * i + 64], axis=1, keepdims=True)
+                )
+                first = 256 * side
+                for k in range(NX):
+                    rows = slice(64 * i + 16 * k, 64 * i + 16 * k + 16)
+                    owner = NX * (r + 4 * side) + k
+                    part1[owner, :, 0:128] = total[rows, first : first + 128].astype(BF16)
+                    part1[owner, :, 128:256] = jnp.where(
+                        has_sums,
+                        squares[16 * k : 16 * k + 16].astype(F32),
+                        total[rows, first + 128 : first + 256],
+                    ).astype(BF16)
+        for dz in steps:
+            for dx in FAR_X + [0]:
+                if (dz, dx) != (0, 0):
+                    peer = at_z(dz) * NX + at_x(dx)
+                    scatter1.send(part1.at[peer], got1.at[x * NZ + z], (peer, t))
     got1[x * NZ + z] = part1[kv]
-    scatter1 = Exchange(got1.at[0:31])
-    for dz, dx in PLANE:
-        peer = at_z(dz) * NX + at_x(dx)
-        scatter1.send(part1.at[peer], got1.at[x * NZ + z], (peer, t))
-    down_blocks = Exchange(down_own.at[0:7])
-    for d, peer in ring_z:
-        down_blocks.send(down_own.at[at_z(d)], down_all.at[t, :, lanes_z], peer)
-    tok_blocks = Exchange(tok_all.at[0:7])
-    for d, peer in ring_z:
-        tok_blocks.send(tok_own, tok_all.at[z], peer)
 
     with jax.named_scope("wait_up_blocks"):
         up_blocks.arrive()
@@ -353,16 +356,11 @@
     log_sigmoid = jnp.minimum(decay_pre, 0.0) - jnp.log1p(jnp.exp(-jnp.abs(decay_pre)))
     decay = jnp.exp(log_sigmoid / GATE_NORM + log_decay[...])
     columns = jnp.transpose(
-        jnp.concatenate([query, keys, decay, jnp.zeros((80, 128), F32)], axis=0), (1, 0)
+        jnp.concatenate([query * decay, keys, decay, jnp.zeros((80, 128), F32)], axis=0), (1, 0)
     )
     for b in range(16):
-        q_col = columns[:, b : b + 1]
-        k_col = columns[:, 16 + b : 17 + b]
-        a_col = columns[:, 32 + b : 33 + b]
-        new = state[b] * a_col + k_col * values[b : b + 1, :]
-        new_state[b] = new
-        att[b : b + 1, :] = jnp.sum(new * q_col, axis=0, keepdims=True)
-    attended = att[...]
+        att[b : b + 1, :] = jnp.sum(state[b] * columns[:, b : b + 1], axis=0, keepdims=True)
+    attended = att[...] + jnp.sum(query * keys, axis=1, keepdims=True) * values
     normed = (
         attended
         * lax.rsqrt(jnp.mean(attended * attended, axis=1, keepdims=True) + EPS)
@@ -372,6 +370,16 @@
     gather2 = Exchange(mix.at[0:3])
     for d, peer in ring_x:
         gather2.send(mix.at[x], mix.at[x], peer)
+    down_blocks = Exchange(down_own.at[0:7])
+    for d, peer in ring_z:
+        down_blocks.send(down_own.at[at_z(d)], down_all.at[t, :, lanes_z], peer)
+    tok_blocks = Exchange(tok_all.at[0:7])
+    for d, peer in ring_z:
+        tok_blocks.send(tok_own, tok_all.at[z], peer)
+    for b in range(16):
+        k_col = columns[:, 16 + b : 17 + b]
+        a_col = columns[:, 32 + b : 33 + b]
+        new_state[b] = state[b] * a_col + k_col * values[b : b + 1, :]
 
     with jax.named_scope("wait_mix_blocks"):
         for exchange in mix_steps[-1]:
@@ -379,7 +387,9 @@
     with jax.named_scope("wait_gather2"):
         gather2.arrive()
     mixed = mix[...].reshape(64, DV)
-    for j, block in enumerate(packed_products(mixed, w_mix[...], lane32)):
+    stacked = jnp.concatenate([mixed[:, 0:128], mixed[:, 128:256]], axis=0)
+    total = jnp.dot(stacked, w_mix[...], preferred_element_type=F32)
+    for j, block in enumerate(packed_products(total[0:64], total[64:128], lane32)):
         part2[j] = block.astype(BF16)
     got2[t] = part2[t]
     scatter2 = Exchange(got2.at[0:7])
@@ -455,43 +465,55 @@
     )
     with jax.named_scope("wait_up_core"):
         up_core.arrive()
-    weights = up_all[...].reshape(NT * 96, 1024)
-    terms = lax.dot_general(
-        left, weights, (((1,), (1,)), ((), ())), preferred_element_type=F32
-    )
-    for j in range(NX):
-        rows = slice(16 * j, 16 * j + 16)
-        part3[j, :, 0:768] = terms[rows].astype(BF16)
-        part3[j, :, 768:1536] = terms[64 + 16 * j : 80 + 16 * j].astype(BF16)
-        part3[j, :, 1536:1664] = squares[rows]
-    got3[x] = part3[x]
-    scatter3 = Exchange(got3.at[0:3])
-    for d, peer in ring_x:
-        scatter3.send(part3.at[at_x(d)], got3.at[x], peer)
+    parts3, gots3 = (part3a, part3b), (got3a, got3b)
+    scatter3 = [Exchange(got3.at[0:3]) for got3 in gots3]
+    for half, (part3, got3) in enumerate(zip(parts3, gots3)):
+        terms = lax.dot_general(
+            left,
+            up_all[half].reshape(384, 1024),
+            (((1,), (1,)), ((), ())),
+            preferred_element_type=F32,
+        )
+        for j in range(NX):
+            rows = slice(16 * j, 16 * j + 16)
+            part3[j, :, 0:384] = terms[rows].astype(BF16)
+            part3[j, :, 384:768] = terms[64 + 16 * j : 80 + 16 * j].astype(BF16)
+            if half == 0:
+                part3[j, :, 768:896] = squares[rows]
+        got3[x] = part3[x]
+        for d, peer in ring_x:
+            scatter3[half].send(part3.at[at_x(d)], got3.at[x], peer)
     with jax.named_scope("wait_down_y"):
         down_y.arrive()
     for d in range(1, NY):
         other = along_y(d)
         down_core.send(down_all.at[other], down_all.at[other], partner)
-    with jax.named_scope("wait_scatter3"):
-        scatter3.arrive()
-    total = got3[0].astype(F32)
-    for j in range(1, NX):
-        total += got3[j].astype(F32)
-    inv = lax.rsqrt(of_pair(total[:, 1536:1664]) / D + EPS)
-    gate = total[:, 0:768] * inv
-    hid[x] = (gate * sigmoid(gate) * (total[:, 768:1536] * inv)).astype(BF16)
-    gather3 = Exchange(hid.at[0:3])
-    for d, peer in ring_x:
-        gather3.send(hid.at[x], hid.at[x], peer)
+    gather3 = [Exchange(hid.at[half, 0:3]) for half in range(2)]
+    inv = None
+    for half, got3 in enumerate(gots3):
+        with jax.named_scope(f"wait_scatter3_{half}"):
+            scatter3[half].arrive()
+        total = got3[0].astype(F32)
+        for j in range(1, NX):
+            total += got3[j].astype(F32)
+        if half == 0:
+            inv = lax.rsqrt(of_pair(total[:, 768:896]) / D + EPS)
+        gate = total[:, 0:384] * inv
+        hid[half, x] = (gate * sigmoid(gate) * (total[:, 384:768] * inv)).astype(BF16)
+        for d, peer in ring_x:
+            gather3[half].send(hid.at[half, x], hid.at[half, x], peer)
     with jax.named_scope("wait_down_core"):
         down_core.arrive()
-    with jax.named_scope("wait_gather3"):
-        gather3.arrive()
-
-    hidden = hid[...].reshape(64, 768)
+
     weights = down_all[...].reshape(NT * 48, 1024)
-    for j, block in enumerate(packed_products(hidden, weights, lane32)):
+    products = []
+    for half in range(2):
+        with jax.named_scope(f"wait_gather3_{half}"):
+            gather3[half].arrive()
+        products.append(
+            jnp.dot(hid[half].reshape(64, 384), weights, preferred_element_type=F32)
+        )
+    for j, block in enumerate(packed_products(*products, lane32)):
         part4[j] = block.astype(BF16)
     got4[z] = part4[z]
     scatter4 = Exchange(got4.at[0:7])
@@ -583,7 +605,7 @@
         + [
             pltpu.VMEM((16, DV), F32),
             pltpu.VMEM((NX, 64, 256), BF16),
-            pltpu.VMEM((NX, 256, 128), BF16),
+            pltpu.VMEM((NX, 4, 64, 128), BF16),
             pltpu.VMEM((NX, 64, 256), BF16),
             pltpu.VMEM((NX, 128, 512), BF16),
             pltpu.VMEM((NZ * NX, 16, 256), BF16),
@@ -601,9 +623,11 @@
             pltpu.VMEM((2, NT, 48, 1024), BF16),
             pltpu.VMEM((NZ, 48, 128), BF16),
             pltpu.VMEM((NT, 48, 1024), BF16),
-            pltpu.VMEM((NX, 16, 1664), BF16),
-            pltpu.VMEM((NX, 16, 1664), BF16),
+            pltpu.VMEM((NX, 16, 896), BF16),
+            pltpu.VMEM((NX, 16, 896), BF16),
             pltpu.VMEM((NX, 16, 768), BF16),
+            pltpu.VMEM((NX, 16, 768), BF16),
+            pltpu.VMEM((2, NX, 16, 384), BF16),
             pltpu.VMEM((NZ, 32, 128), BF16),
             pltpu.VMEM((NZ, 32, 128), BF16),
             pltpu.VMEM((32, 128), BF16),

time: 64.4 us -> 60.6 us (0.941)
  Pallas kernels: 63.6 us -> 59.8 us
    pallas_call x1, Pallas kernels: 62.3 us -> 58.5 us  [body(): pl.pallas_call(kernel, out_shape=(pltpu.VMEM((64, 512), BF16), pltpu.VMEM...]
where the time goes in v6:
time: 60.6 us; the launch traced here: 60.5 us
  Pallas kernels  59.8 us (99%)
  between operations  0.64 us (1%)
    pallas_call x1, Pallas kernels, body(): pl.pallas_call(kernel, out_shape=(pltpu.VMEM((64, 512), BF16), pltpu.VMEM...  58.5 us
    pallas_call x1, Pallas kernels, body(): pl.pallas_call(finish, out_shape=(jax.ShapeDtypeStruct((64, 512), BF16),...  1.34 us

profile of v6, /device:TPU:1, one launch (start us, length us, event | category | flops | bytes accessed | tf_op | source)
XLA Modules:
  0.0 60.5 jit_solution(16093271453815417632)
XLA Ops:
  0.6 58.5 %shard_map.158 = (bf16[64,512]{1,0:T(8,128)(2,1)S(1)}, f32[16,128,256]{2,1,0:T(8,128)S(1)}) custom-call(bf16[64,512]{1,0:T(8,128)(2,1)} %bitcast.13, bf16[1,64]{1,0:T(2,128)(2,1)} %bitcast.16, bf16[64,128]{1,0:T(8,128)(2,1)} %refs_2_.1, bf16[64,128]{1,0:T(8,128)(2,1)} %refs_3_.1, bf16[64,256]{1,0:T(8,128)(2,1)} %refs_4_.1, bf16[64,256]{1,0:T(8,128)(2,1)} %refs_5_.1, ...), custom_call_target="tpu_custom_call" | custom-call | tf_op jit(solution)/shard_map/pallas_call | solution.py:596
  59.1 1.3 %shard_map.159 = (bf16[64,512]{1,0:T(8,128)(2,1)}, f32[16,128,256]{2,1,0:T(8,128)}) custom-call(bf16[64,512]{1,0:T(8,128)(2,1)S(1)} %get-tuple-element.6.result_in, f32[16,128,256]{2,1,0:T(8,128)S(1)} %get-tuple-element.7.state_in), custom_call_target="tpu_custom_call" | custom-call | tf_op jit(solution)/shard_map/pallas_call | solution.py:643

commit v7 on v6

--- a/solution.py
+++ b/solution.py
@@ -19,11 +19,12 @@
 
 NX, NY, NZ = 4, 4, 8
 NT = 2 * NY
-COPIES = 27
+COPIES = 32
 FAR_X = [2, 1, 3]
 FAR_Y = [2, 1, 3]
 FAR_Z = [4, 3, 5, 2, 6, 1, 7]
 FAR_T = [4, 5, 2, 3, 6, 7, 1]
+X_ORDER = [(0, 4), (2, 6), (3, 7), (1, 5)]
 PLANE = [(dz, dx) for dz in FAR_Z + [0] for dx in FAR_X + [0] if (dz, dx) != (0, 0)]
 LOADS = [(0, 0), (1, 1), (2, 0), (3, 0), (4, 0), (5, 0), (6, 0)]
 LOADS += [(10, 3), (12, 2), (13, 2), (14, 2), (11, 4), (7, 5), (9, 6), (8, 7)]
@@ -216,14 +217,13 @@
     ring_z = [(d, (at_z(d) * NX + x, t)) for d in FAR_Z]
     ring_t = [(d, (kv, at_t(d))) for d in FAR_T]
     gather_w = Exchange(w_all.at[0:3])
-    gather_x = [Exchange(x_all.at[0:3, 0:2]) for half in range(2)]
-    halves_z = [[lax.rem(z + d, 4) for d in steps] for steps in ((1, 2), (0, 3))]
+    gather_x = [Exchange(x_all.at[0:3, 0]) for _ in X_ORDER]
+    x_blocks = [lax.rem(z + steps[0], 4) for steps in X_ORDER]
     for d, peer in ring_x:
         gather_w.send(w_own.at[at_x(d)], w_all.at[x], peer)
-    for half in range(2):
+    for exchange, r in zip(gather_x, x_blocks):
         for d, peer in ring_x:
-            for r in halves_z[half]:
-                gather_x[half].send(x_all.at[x, r], x_all.at[x, r], peer)
+            exchange.send(x_all.at[x, r], x_all.at[x, r], peer)
 
     with jax.named_scope("wait_later"):
         loaded(3, w_out)
@@ -262,15 +262,35 @@
     down = jnp.concatenate([down, pltpu.roll(down, 768 - 48, 1)], axis=0)
     down = jnp.transpose(down, (1, 0)).astype(BF16)
     for j in range(NZ):
-        up_own[j, 0] = units[96 * j : 96 * j + 48]
-        up_own[j, 1] = units[96 * j + 48 : 96 * j + 96]
+        up_own[0, j] = units[96 * j : 96 * j + 48]
+        up_own[1, j] = units[96 * j + 48 : 96 * j + 96]
         down_own[j] = down[96 * j : 96 * j + 48]
     lanes_z = lanes_of(z)
-    up_all[:, t, :, lanes_z] = up_own[z]
+    for half in range(2):
+        up_all[half, t, :, lanes_z] = up_own[half, z]
     down_all[t, :, lanes_z] = down_own[z]
-    up_blocks = Exchange(up_own.at[0:7])
-    for d, peer in ring_z:
-        up_blocks.send(up_own.at[at_z(d)], up_all.at[:, t, :, lanes_z], peer)
+    up_blocks = [Exchange(up_own.at[half, 0:7]) for half in range(2)]
+    up_y = [Exchange(up_all.at[half, 0:3]) for half in range(2)]
+    up_core = [Exchange(up_all.at[half, 0:4]) for half in range(2)]
+    partner = (kv, t + 1 - 2 * core)
+
+    def along_y(d):
+        return lax.rem(y + d, NY) * 2 + core
+
+    def up_along_z(half):
+        for d, peer in ring_z:
+            up_blocks[half].send(
+                up_own.at[half, at_z(d)], up_all.at[half, t, :, lanes_z], peer
+            )
+
+    def up_along_y(half):
+        with jax.named_scope(f"wait_up_blocks_{half}"):
+            up_blocks[half].arrive()
+        for d in FAR_Y:
+            up_y[half].send(up_all.at[half, t], up_all.at[half, t], (kv, along_y(d)))
+        up_core[half].send(up_all.at[half, t], up_all.at[half, t], partner)
+
+    up_along_z(0)
     lane32 = lax.broadcasted_iota(jnp.int32, (32, 128), 1)
     own = x_all[x, lax.rem(t, 4)].astype(F32)
     own = jnp.where(t < 4, own, pltpu.roll(own, 64, 1))
@@ -286,54 +306,39 @@
     for j in range(NX):
         w_diag[j, 0:64, 0:256] = w_all[j]
         w_diag[j, 64:128, 256:512] = w_all[j]
-    lane128 = lax.broadcasted_iota(jnp.int32, (128, 128), 1)
+    lane64 = lax.broadcasted_iota(jnp.int32, (64, 128), 1)
     has_sums = x == NX - 1
     scatter1 = Exchange(got1.at[0:31])
-    for half, (blocks, steps) in enumerate(zip(halves_z, ([5, 2, 6, 1], [4, 3, 7, 0]))):
-        with jax.named_scope(f"wait_gather1_{half}"):
-            gather_x[half].arrive()
-        total = jnp.zeros((128, 512), F32)
-        sums = [jnp.zeros((128, 128), F32)] * 2
+    for number, (r, steps) in enumerate(zip(x_blocks, X_ORDER)):
+        with jax.named_scope(f"wait_gather1_{number}"):
+            gather_x[number].arrive()
+        total = jnp.zeros((64, 512), F32)
+        squares = jnp.zeros((64, 128), F32)
         for j in range(NX):
-            block = jnp.concatenate([x_all[j, r] for r in blocks], axis=0)
+            block = x_all[j, r]
             total += jnp.dot(block, w_diag[j], preferred_element_type=F32)
             wide = block.astype(F32)
-            wide = wide * wide
-            sums[0] += jnp.where(lane128 < 64, wide, 0.0)
-            sums[1] += jnp.where(lane128 < 64, 0.0, wide)
-        for i, r in enumerate(blocks):
-            for side in range(2):
-                squares = as_pair(
-                    jnp.sum(sums[side][64 * i : 64 * i + 64], axis=1, keepdims=True)
-                )
-                first = 256 * side
-                for k in range(NX):
-                    rows = slice(64 * i + 16 * k, 64 * i + 16 * k + 16)
-                    owner = NX * (r + 4 * side) + k
-                    part1[owner, :, 0:128] = total[rows, first : first + 128].astype(BF16)
-                    part1[owner, :, 128:256] = jnp.where(
-                        has_sums,
-                        squares[16 * k : 16 * k + 16].astype(F32),
-                        total[rows, first + 128 : first + 256],
-                    ).astype(BF16)
-        for dz in steps:
+            squares += wide * wide
+        for side in range(2):
+            ours = (lane64 < 64) if side == 0 else (lane64 >= 64)
+            sums = as_pair(jnp.sum(jnp.where(ours, squares, 0.0), axis=1, keepdims=True))
+            first = 256 * side
+            for k in range(NX):
+                rows = slice(16 * k, 16 * k + 16)
+                owner = NX * (r + 4 * side) + k
+                part1[owner, :, 0:128] = total[rows, first : first + 128].astype(BF16)
+                part1[owner, :, 128:256] = jnp.where(
+                    has_sums, sums[rows].astype(F32), total[rows, first + 128 : first + 256]
+                ).astype(BF16)
+        for dz in sorted(steps, key=lambda step: -min(step, NZ - step)):
             for dx in FAR_X + [0]:
                 if (dz, dx) != (0, 0):
                     peer = at_z(dz) * NX + at_x(dx)
                     scatter1.send(part1.at[peer], got1.at[x * NZ + z], (peer, t))
     got1[x * NZ + z] = part1[kv]
 
-    with jax.named_scope("wait_up_blocks"):
-        up_blocks.arrive()
-    partner = (kv, t + 1 - 2 * core)
-
-    def along_y(d):
-        return lax.rem(y + d, NY) * 2 + core
-
-    up_y, up_core = Exchange(up_all.at[:, 0:3]), Exchange(up_all.at[:, 0:4])
-    for d in FAR_Y:
-        up_y.send(up_all.at[:, t], up_all.at[:, t], (kv, along_y(d)))
-    up_core.send(up_all.at[:, t], up_all.at[:, t], partner)
+    up_along_z(1)
+    up_along_y(0)
     mix_step(3)
 
     with jax.named_scope("wait_scatter1"):
@@ -395,6 +400,7 @@
     scatter2 = Exchange(got2.at[0:7])
     for d, peer in ring_t:
         scatter2.send(part2.at[at_t(d)], got2.at[t], peer)
+    up_along_y(1)
     with jax.named_scope("wait_scatter2"):
         scatter2.arrive()
     total = got2[0].astype(F32)
@@ -429,11 +435,12 @@
     down_y, down_core = Exchange(down_all.at[0:3]), Exchange(down_all.at[0:4])
     for d in FAR_Y:
         down_y.send(down_all.at[t], down_all.at[t], (kv, along_y(d)))
-    with jax.named_scope("wait_up_y"):
-        up_y.arrive()
-    for d in range(1, NY):
-        other = along_y(d)
-        up_core.send(up_all.at[:, other], up_all.at[:, other], partner)
+    for half in range(2):
+        with jax.named_scope(f"wait_up_y_{half}"):
+            up_y[half].arrive()
+        for d in range(1, NY):
+            other = along_y(d)
+            up_core[half].send(up_all.at[half, other], up_all.at[half, other], partner)
     down_core.send(down_all.at[t], down_all.at[t], partner)
 
     with jax.named_scope("wait_tok_blocks"):
@@ -463,11 +470,11 @@
             [jnp.sum(top, axis=1, keepdims=True), jnp.sum(bottom, axis=1, keepdims=True)], axis=0
         )
     )
-    with jax.named_scope("wait_up_core"):
-        up_core.arrive()
     parts3, gots3 = (part3a, part3b), (got3a, got3b)
     scatter3 = [Exchange(got3.at[0:3]) for got3 in gots3]
     for half, (part3, got3) in enumerate(zip(parts3, gots3)):
+        with jax.named_scope(f"wait_up_core_{half}"):
+            up_core[half].arrive()
         terms = lax.dot_general(
             left,
             up_all[half].reshape(384, 1024),
@@ -619,7 +626,7 @@
             pltpu.VMEM((32, 128), BF16),
             pltpu.VMEM((NZ, 32, 128), BF16),
             pltpu.VMEM((NZ, 32, 128), BF16),
-            pltpu.VMEM((NZ, 2, 48, 128), BF16),
+            pltpu.VMEM((2, NZ, 48, 128), BF16),
             pltpu.VMEM((2, NT, 48, 1024), BF16),
             pltpu.VMEM((NZ, 48, 128), BF16),
             pltpu.VMEM((NT, 48, 1024), BF16),

time: 60.6 us -> 60.6 us (level)
  no operation moved by 1% of the time
where the time goes in v7:
time: 60.6 us; the launch traced here: 60.5 us
  Pallas kernels  59.9 us (99%)
  between operations  0.64 us (1%)
    pallas_call x1, Pallas kernels, body(): pl.pallas_call(kernel, out_shape=(pltpu.VMEM((64, 512), BF16), pltpu.VMEM...  58.5 us
    pallas_call x1, Pallas kernels, body(): pl.pallas_call(finish, out_shape=(jax.ShapeDtypeStruct((64, 512), BF16),...  1.34 us

profile of v7, /device:TPU:1, one launch (start us, length us, event | category | flops | bytes accessed | tf_op | source)
XLA Modules:
  0.0 60.5 jit_solution(18013885832454192703)
XLA Ops:
  0.6 58.5 %shard_map.158 = (bf16[64,512]{1,0:T(8,128)(2,1)S(1)}, f32[16,128,256]{2,1,0:T(8,128)S(1)}) custom-call(bf16[64,512]{1,0:T(8,128)(2,1)} %bitcast.13, bf16[1,64]{1,0:T(2,128)(2,1)} %bitcast.16, bf16[64,128]{1,0:T(8,128)(2,1)} %refs_2_.1, bf16[64,128]{1,0:T(8,128)(2,1)} %refs_3_.1, bf16[64,256]{1,0:T(8,128)(2,1)} %refs_4_.1, bf16[64,256]{1,0:T(8,128)(2,1)} %refs_5_.1, ...), custom_call_target="tpu_custom_call" | custom-call | tf_op jit(solution)/shard_map/pallas_call | solution.py:603
  59.2 1.3 %shard_map.159 = (bf16[64,512]{1,0:T(8,128)(2,1)}, f32[16,128,256]{2,1,0:T(8,128)}) custom-call(bf16[64,512]{1,0:T(8,128)(2,1)S(1)} %get-tuple-element.6.result_in, f32[16,128,256]{2,1,0:T(8,128)S(1)} %get-tuple-element.7.state_in), custom_call_target="tpu_custom_call" | custom-call | tf_op jit(solution)/shard_map/pallas_call | solution.py:650

commit v8 on v7

--- a/solution.py
+++ b/solution.py
@@ -32,10 +32,6 @@
 
 def sigmoid(value):
     return 1.0 / (1.0 + jnp.exp(-value))
-
-
-def halves(low, high):
-    return jnp.concatenate([low, high], axis=1)
 
 
 def as_pair(total):
@@ -83,6 +79,7 @@
     (
         att,
         w_own,
+        x_own,
         x_all,
         w_all,
         w_diag,
@@ -169,13 +166,6 @@
         greet((at_z(dz) * NX + at_x(dx), t))
     for d in FAR_T:
         greet((kv, at_t(d)))
-    for d in FAR_Z:
-        greet((at_z(d) * NX + x, z))
-
-    @pl.when(t != z)
-    def _():
-        greet((kv, z))
-
     def loaded(sem, size):
         pltpu.make_async_copy(size, size, local_sems.at[sem]).wait()
 
@@ -201,12 +191,13 @@
     w_own[3, :, 0:128] = gained(w_decay)
     w_own[3, :, 128:256] = jnp.zeros((64, 128), BF16)
     own = jnp.concatenate([tokens[:, 0:256], tokens[:, 256:512]], axis=0).astype(F32)
-    x_all[x] = jnp.transpose(own, (1, 0)).astype(BF16).reshape(4, 64, 128)
+    own = jnp.transpose(own, (1, 0))
+    x_own[...] = own.reshape(4, 64, 128)
+    x_all[x] = own.astype(BF16).reshape(4, 64, 128)
     w_all[x] = w_own[x]
 
-    greetings = len(PLANE) + len(FAR_T) + len(FAR_Z)
     with jax.named_scope("wait_barrier"):
-        pl.semaphore_wait(barrier, greetings + jnp.where(t != z, 1, 0))
+        pl.semaphore_wait(barrier, len(PLANE) + len(FAR_T))
 
     tile_z = w_mix.at[:, 0:128]
 
@@ -292,9 +283,8 @@
 
     up_along_z(0)
     lane32 = lax.broadcasted_iota(jnp.int32, (32, 128), 1)
-    own = x_all[x, lax.rem(t, 4)].astype(F32)
-    own = jnp.where(t < 4, own, pltpu.roll(own, 64, 1))
-    tok_own[...] = jnp.where(lane32 < 64, own[0:32], pltpu.roll(own[32:64], 64, 1)).astype(BF16)
+    ours = x_own[:, pl.ds(pl.multiple_of(8 * t, 8), 8), :]
+    tok_own[...] = ours.reshape(32, 128).astype(BF16)
     tok_all[z] = tok_own[...]
     w_diag[...] = jnp.zeros(w_diag.shape, BF16)
 
@@ -337,13 +327,13 @@
                     scatter1.send(part1.at[peer], got1.at[x * NZ + z], (peer, t))
     got1[x * NZ + z] = part1[kv]
 
+    with jax.named_scope("wait_mix_step"):
+        mix_step(3)
     up_along_z(1)
     up_along_y(0)
-    mix_step(3)
 
     with jax.named_scope("wait_scatter1"):
         scatter1.arrive()
-    mix_step(4)
     proj = []
     for j in range(NX):
         total = got1[NZ * j].astype(F32)
@@ -375,6 +365,8 @@
     gather2 = Exchange(mix.at[0:3])
     for d, peer in ring_x:
         gather2.send(mix.at[x], mix.at[x], peer)
+    with jax.named_scope("wait_mix_step"):
+        mix_step(4)
     down_blocks = Exchange(down_own.at[0:7])
     for d, peer in ring_z:
         down_blocks.send(down_own.at[at_z(d)], down_all.at[t, :, lanes_z], peer)
@@ -394,8 +386,23 @@
     mixed = mix[...].reshape(64, DV)
     stacked = jnp.concatenate([mixed[:, 0:128], mixed[:, 128:256]], axis=0)
     total = jnp.dot(stacked, w_mix[...], preferred_element_type=F32)
-    for j, block in enumerate(packed_products(total[0:64], total[64:128], lane32)):
-        part2[j] = block.astype(BF16)
+    lane64 = lax.broadcasted_iota(jnp.int32, (64, 128), 1)
+    pairs = []
+    for p in range(4):
+        low, high = [
+            (total[0:64, first : first + 128], total[64:128, first : first + 128])
+            for first in (256 * p, 256 * p + 128)
+        ]
+        pairs.append(
+            jnp.where(
+                lane64 < 64,
+                low[0] + pltpu.roll(low[1], 64, 1),
+                pltpu.roll(high[0], 64, 1) + high[1],
+            )
+        )
+    for j in range(NT):
+        rows = slice(8 * j, 8 * j + 8)
+        part2[j] = jnp.concatenate([pair[rows] for pair in pairs], axis=0).astype(BF16)
     got2[t] = part2[t]
     scatter2 = Exchange(got2.at[0:7])
     for d, peer in ring_t:
@@ -408,27 +415,10 @@
         total += got2[j].astype(F32)
     attn_own[...] = total.astype(BF16)
 
-    spread = Exchange(attn_all)
-    diagonal = t == z
-    for d in FAR_Z:
-        spread.send(attn_own, attn_all.at[t], (at_z(d) * NX + x, z))
-
-    @pl.when(jnp.logical_not(diagonal))
-    def _():
-        spread.send(attn_own, attn_all.at[t], (kv, z))
-
-    @pl.when(diagonal)
-    def _():
-        attn_all[t] = attn_own[...]
-
-    def spread_wait(sems):
-        @pl.when(diagonal)
-        def _():
-            spread.wait(sems, attn_all.at[0:7])
-
-        @pl.when(jnp.logical_not(diagonal))
-        def _():
-            spread.wait(sems, attn_all)
+    attn_all[z] = attn_own[...]
+    spread = Exchange(attn_all.at[0:7])
+    for d, peer in ring_z:
+        spread.send(attn_own, attn_all.at[z], peer)
 
     with jax.named_scope("wait_down_blocks"):
         down_blocks.arrive()
@@ -446,30 +436,34 @@
     with jax.named_scope("wait_tok_blocks"):
         tok_blocks.arrive()
     with jax.named_scope("wait_spread"):
-        spread_wait(recv_sems)
-
-    top = jnp.zeros((32, 128), F32)
-    bottom = jnp.zeros((32, 128), F32)
+        spread.arrive()
+
+    squares = jnp.zeros((64, 128), F32)
     pieces = []
-    for j in range(NZ):
-        block = (tok_all[j].astype(F32) + attn_all[j].astype(F32)).astype(BF16)
-        middle[j] = block
-        wide = block.astype(F32)
-        low = jnp.where(lane32 < 64, wide, 0.0)
-        high = jnp.where(lane32 < 64, 0.0, wide)
-        top += low * low
-        bottom += high * high
-        pieces.append(
-            jnp.concatenate(
-                [low, pltpu.roll(high, 64, 1), pltpu.roll(low, 64, 1), high], axis=0
-            ).astype(BF16)
+    sums = [attn_all[j].astype(F32) for j in range(NZ)]
+    middles = []
+    for p in range(4):
+        low, high = tok_all[2 * p].astype(F32), tok_all[2 * p + 1].astype(F32)
+        residual = jnp.concatenate(
+            [
+                jnp.where(lane32 < 64, low, pltpu.roll(high, 64, 1)),
+                jnp.where(lane32 < 64, pltpu.roll(low, 64, 1), high),
+            ],
+            axis=0,
         )
+        added = jnp.concatenate([total[8 * p : 8 * p + 8] for total in sums], axis=0)
+        wide = (residual + added).astype(BF16).astype(F32)
+        middles.append(wide)
+        squares += wide * wide
+        turned = pltpu.roll(wide, 64, 1)
+        for here, there in ((wide, turned), (turned, wide)):
+            pieces.append(
+                jnp.concatenate(
+                    [jnp.where(lane64 < 64, here, 0.0), jnp.where(lane64 < 64, 0.0, there)], axis=0
+                ).astype(BF16)
+            )
     left = jnp.concatenate(pieces, axis=1)
-    squares = as_pair(
-        jnp.concatenate(
-            [jnp.sum(top, axis=1, keepdims=True), jnp.sum(bottom, axis=1, keepdims=True)], axis=0
-        )
-    )
+    squares = as_pair(jnp.sum(squares, axis=1, keepdims=True))
     parts3, gots3 = (part3a, part3b), (got3a, got3b)
     scatter3 = [Exchange(got3.at[0:3]) for got3 in gots3]
     for half, (part3, got3) in enumerate(zip(parts3, gots3)):
@@ -490,6 +484,10 @@
         got3[x] = part3[x]
         for d, peer in ring_x:
             scatter3[half].send(part3.at[at_x(d)], got3.at[x], peer)
+    for p, wide in enumerate(middles):
+        turned = pltpu.roll(wide, 64, 1)
+        middle[2 * p] = jnp.where(lane32 < 64, wide[0:32], turned[32:64]).astype(BF16)
+        middle[2 * p + 1] = jnp.where(lane32 < 64, turned[0:32], wide[32:64]).astype(BF16)
     with jax.named_scope("wait_down_y"):
         down_y.arrive()
     for d in range(1, NY):
@@ -538,18 +536,21 @@
         gather4.send(res_own, res_all.at[t], peer)
     with jax.named_scope("wait_gather4"):
         gather4.arrive()
-    rows = []
-    for j in range(NT):
-        block = res_all[j].astype(F32)
-        rows += [block, pltpu.roll(block, 64, 1)]
-    rows = jnp.concatenate(rows, axis=0)
+    blocks = [res_all[j].astype(F32) for j in range(NT)]
+    blocks = [blocks, [pltpu.roll(block, 64, 1) for block in blocks]]
+    rows = jnp.concatenate(
+        [
+            blocks[j // 4][k][8 * (j % 4) : 8 * (j % 4) + 8]
+            for j in range(NZ)
+            for k in range(NT)
+        ],
+        axis=0,
+    )
     result[...] = jnp.transpose(rows, (1, 0))[0:64].astype(BF16)
     with jax.named_scope("wait_sends"):
         for exchange in unsent:
-            if exchange is spread:
-                spread_wait(send_sems)
-            else:
-                exchange.leave()
+            exchange.leave()
+
 
 def finish(result_in, state_in, result_out, state_out, sems):
     result = pltpu.make_async_copy(result_in, result_out, sems.at[0])
@@ -612,6 +613,7 @@
         + [
             pltpu.VMEM((16, DV), F32),
             pltpu.VMEM((NX, 64, 256), BF16),
+            pltpu.VMEM((4, 64, 128), F32),
             pltpu.VMEM((NX, 4, 64, 128), BF16),
             pltpu.VMEM((NX, 64, 256), BF16),
             pltpu.VMEM((NX, 128, 512), BF16),

time: 60.6 us -> 59.2 us (0.977)
  Pallas kernels: 59.9 us -> 58.5 us
    pallas_call x1, Pallas kernels: 58.5 us -> 57.1 us  [body(): pl.pallas_call(kernel, out_shape=(pltpu.VMEM((64, 512), BF16), pltpu.VMEM...]
where the time goes in v8:
time: 59.2 us; the launch traced here: 59.1 us
  Pallas kernels  58.5 us (99%)
  between operations  0.64 us (1%)
    pallas_call x1, Pallas kernels, body(): pl.pallas_call(kernel, out_shape=(pltpu.VMEM((64, 512), BF16), pltpu.VMEM...  57.1 us
    pallas_call x1, Pallas kernels, body(): pl.pallas_call(finish, out_shape=(jax.ShapeDtypeStruct((64, 512), BF16),...  1.34 us

profile of v8, /device:TPU:1, one launch (start us, length us, event | category | flops | bytes accessed | tf_op | source)
XLA Modules:
  0.0 59.1 jit_solution(50998644367037951)
XLA Ops:
  0.6 57.1 %shard_map.158 = (bf16[64,512]{1,0:T(8,128)(2,1)S(1)}, f32[16,128,256]{2,1,0:T(8,128)S(1)}) custom-call(bf16[64,512]{1,0:T(8,128)(2,1)} %bitcast.13, bf16[1,64]{1,0:T(2,128)(2,1)} %bitcast.16, bf16[64,128]{1,0:T(8,128)(2,1)} %refs_2_.1, bf16[64,128]{1,0:T(8,128)(2,1)} %refs_3_.1, bf16[64,256]{1,0:T(8,128)(2,1)} %refs_4_.1, bf16[64,256]{1,0:T(8,128)(2,1)} %refs_5_.1, ...), custom_call_target="tpu_custom_call" | custom-call | tf_op jit(solution)/shard_map/pallas_call | solution.py:604
  57.8 1.3 %shard_map.159 = (bf16[64,512]{1,0:T(8,128)(2,1)}, f32[16,128,256]{2,1,0:T(8,128)}) custom-call(bf16[64,512]{1,0:T(8,128)(2,1)S(1)} %get-tuple-element.6.result_in, f32[16,128,256]{2,1,0:T(8,128)S(1)} %get-tuple-element.7.state_in), custom_call_target="tpu_custom_call" | custom-call | tf_op jit(solution)/shard_map/pallas_call | solution.py:652

commit v9 on v8

--- a/solution.py
+++ b/solution.py
@@ -20,6 +20,7 @@
 NX, NY, NZ = 4, 4, 8
 NT = 2 * NY
 COPIES = 32
+SMALL, UP, DOWN, LAST = range(4)
 FAR_X = [2, 1, 3]
 FAR_Y = [2, 1, 3]
 FAR_Z = [4, 3, 5, 2, 6, 1, 7]
@@ -126,33 +127,24 @@
         return lax.rem(t + d, NT)
 
     counter = [0]
-    unsent = []
 
     class Exchange:
-        def __init__(self, size):
-            self.number = counter[0]
-            self.size = size
+        def __init__(self, size, group=SMALL):
+            self.number, self.group, self.size = counter[0], group, size
             counter[0] += 1
-            unsent.append(self)
 
         def send(self, src, dst, peer):
             pltpu.make_async_remote_copy(
                 src_ref=src,
                 dst_ref=dst,
-                send_sem=send_sems.at[self.number],
+                send_sem=send_sems.at[self.group],
                 recv_sem=recv_sems.at[self.number],
                 device_id=peer,
                 device_id_type=MESH,
             ).start()
 
-        def wait(self, sems, size):
-            pltpu.make_async_copy(size, size, sems.at[self.number]).wait()
-
         def arrive(self):
-            self.wait(recv_sems, self.size)
-
-        def leave(self):
-            self.wait(send_sems, self.size)
+            pltpu.make_async_copy(self.size, self.size, recv_sems.at[self.number]).wait()
 
     for i, sem in LOADS:
         pltpu.make_async_copy(inputs[i], held[i], local_sems.at[sem]).start()
@@ -207,8 +199,8 @@
     ring_x = [(d, (z * NX + at_x(d), t)) for d in FAR_X]
     ring_z = [(d, (at_z(d) * NX + x, t)) for d in FAR_Z]
     ring_t = [(d, (kv, at_t(d))) for d in FAR_T]
-    gather_w = Exchange(w_all.at[0:3])
-    gather_x = [Exchange(x_all.at[0:3, 0]) for _ in X_ORDER]
+    gather_w = Exchange(w_all.at[0:3], DOWN)
+    gather_x = [Exchange(x_all.at[0:3, 0], UP) for _ in X_ORDER]
     x_blocks = [lax.rem(z + steps[0], 4) for steps in X_ORDER]
     for d, peer in ring_x:
         gather_w.send(w_own.at[at_x(d)], w_all.at[x], peer)
@@ -261,8 +253,8 @@
         up_all[half, t, :, lanes_z] = up_own[half, z]
     down_all[t, :, lanes_z] = down_own[z]
     up_blocks = [Exchange(up_own.at[half, 0:7]) for half in range(2)]
-    up_y = [Exchange(up_all.at[half, 0:3]) for half in range(2)]
-    up_core = [Exchange(up_all.at[half, 0:4]) for half in range(2)]
+    up_y = [Exchange(up_all.at[half, 0:3], UP) for half in range(2)]
+    up_core = [Exchange(up_all.at[half, 0:4], UP) for half in range(2)]
     partner = (kv, t + 1 - 2 * core)
 
     def along_y(d):
@@ -300,6 +292,9 @@
     has_sums = x == NX - 1
     scatter1 = Exchange(got1.at[0:31])
     for number, (r, steps) in enumerate(zip(x_blocks, X_ORDER)):
+        if number == 3:
+            with jax.named_scope("wait_mix_step3"):
+                mix_step(3)
         with jax.named_scope(f"wait_gather1_{number}"):
             gather_x[number].arrive()
         total = jnp.zeros((64, 512), F32)
@@ -327,10 +322,10 @@
                     scatter1.send(part1.at[peer], got1.at[x * NZ + z], (peer, t))
     got1[x * NZ + z] = part1[kv]
 
-    with jax.named_scope("wait_mix_step"):
-        mix_step(3)
+    up_along_y(0)
+    with jax.named_scope("wait_mix_step4"):
+        mix_step(4)
     up_along_z(1)
-    up_along_y(0)
 
     with jax.named_scope("wait_scatter1"):
         scatter1.arrive()
@@ -365,8 +360,6 @@
     gather2 = Exchange(mix.at[0:3])
     for d, peer in ring_x:
         gather2.send(mix.at[x], mix.at[x], peer)
-    with jax.named_scope("wait_mix_step"):
-        mix_step(4)
     down_blocks = Exchange(down_own.at[0:7])
     for d, peer in ring_z:
         down_blocks.send(down_own.at[at_z(d)], down_all.at[t, :, lanes_z], peer)
@@ -422,7 +415,7 @@
 
     with jax.named_scope("wait_down_blocks"):
         down_blocks.arrive()
-    down_y, down_core = Exchange(down_all.at[0:3]), Exchange(down_all.at[0:4])
+    down_y, down_core = Exchange(down_all.at[0:3], DOWN), Exchange(down_all.at[0:4], DOWN)
     for d in FAR_Y:
         down_y.send(down_all.at[t], down_all.at[t], (kv, along_y(d)))
     for half in range(2):
@@ -531,7 +524,7 @@
         total += got4[j].astype(F32)
     res_own[...] = (middle[z].astype(F32) + total).astype(BF16)
     res_all[t] = res_own[...]
-    gather4 = Exchange(res_all.at[0:7])
+    gather4 = Exchange(res_all.at[0:7], LAST)
     for d, peer in ring_t:
         gather4.send(res_own, res_all.at[t], peer)
     with jax.named_scope("wait_gather4"):
@@ -548,8 +541,9 @@
     )
     result[...] = jnp.transpose(rows, (1, 0))[0:64].astype(BF16)
     with jax.named_scope("wait_sends"):
-        for exchange in unsent:
-            exchange.leave()
+        everything = (state.at[0:15, 0:80], up_all, up_all.at[0], res_all.at[0:7])
+        for group, size in enumerate(everything):
+            pltpu.make_async_copy(size, size, send_sems.at[group]).wait()
 
 
 def finish(result_in, state_in, result_out, state_out, sems):
@@ -641,7 +635,7 @@
             pltpu.VMEM((NZ, 32, 128), BF16),
             pltpu.VMEM((32, 128), BF16),
             pltpu.VMEM((NT, 32, 128), BF16),
-            pltpu.SemaphoreType.DMA((COPIES,)),
+            pltpu.SemaphoreType.DMA((4,)),
             pltpu.SemaphoreType.DMA((COPIES,)),
             pltpu.SemaphoreType.DMA((8,)),
         ],

time: 59.2 us -> 59.2 us (level)
  no operation moved by 1% of the time
where the time goes in v9:
time: 59.2 us; the launch traced here: 59.1 us
  Pallas kernels  58.4 us (99%)
  between operations  0.64 us (1%)
    pallas_call x1, Pallas kernels, body(): pl.pallas_call(kernel, out_shape=(pltpu.VMEM((64, 512), BF16), pltpu.VMEM...  57.1 us
    pallas_call x1, Pallas kernels, body(): pl.pallas_call(finish, out_shape=(jax.ShapeDtypeStruct((64, 512), BF16),...  1.34 us

profile of v9, /device:TPU:1, one launch (start us, length us, event | category | flops | bytes accessed | tf_op | source)
XLA Modules:
  0.0 59.1 jit_solution(9584489468556160579)
XLA Ops:
  0.6 57.1 %shard_map.158 = (bf16[64,512]{1,0:T(8,128)(2,1)S(1)}, f32[16,128,256]{2,1,0:T(8,128)S(1)}) custom-call(bf16[64,512]{1,0:T(8,128)(2,1)} %bitcast.13, bf16[1,64]{1,0:T(2,128)(2,1)} %bitcast.16, bf16[64,128]{1,0:T(8,128)(2,1)} %refs_2_.1, bf16[64,128]{1,0:T(8,128)(2,1)} %refs_3_.1, bf16[64,256]{1,0:T(8,128)(2,1)} %refs_4_.1, bf16[64,256]{1,0:T(8,128)(2,1)} %refs_5_.1, ...), custom_call_target="tpu_custom_call" | custom-call | tf_op jit(solution)/shard_map/pallas_call | solution.py:598
  57.7 1.3 %shard_map.159 = (bf16[64,512]{1,0:T(8,128)(2,1)}, f32[16,128,256]{2,1,0:T(8,128)}) custom-call(bf16[64,512]{1,0:T(8,128)(2,1)S(1)} %get-tuple-element.6.result_in, f32[16,128,256]{2,1,0:T(8,128)S(1)} %get-tuple-element.7.state_in), custom_call_target="tpu_custom_call" | custom-call | tf_op jit(solution)/shard_map/pallas_call | solution.py:646

commit v10 on v9

--- a/solution.py
+++ b/solution.py
@@ -292,9 +292,6 @@
     has_sums = x == NX - 1
     scatter1 = Exchange(got1.at[0:31])
     for number, (r, steps) in enumerate(zip(x_blocks, X_ORDER)):
-        if number == 3:
-            with jax.named_scope("wait_mix_step3"):
-                mix_step(3)
         with jax.named_scope(f"wait_gather1_{number}"):
             gather_x[number].arrive()
         total = jnp.zeros((64, 512), F32)
@@ -322,6 +319,8 @@
                     scatter1.send(part1.at[peer], got1.at[x * NZ + z], (peer, t))
     got1[x * NZ + z] = part1[kv]
 
+    with jax.named_scope("wait_mix_step3"):
+        mix_step(3)
     up_along_y(0)
     with jax.named_scope("wait_mix_step4"):
         mix_step(4)

time: 59.2 us -> 57.6 us (0.973)
  Pallas kernels: 58.4 us -> 56.9 us
    pallas_call x1, Pallas kernels: 57.1 us -> 55.5 us  [body(): pl.pallas_call(kernel, out_shape=(pltpu.VMEM((64, 512), BF16), pltpu.VMEM...]
where the time goes in v10:
time: 57.6 us; the launch traced here: 57.5 us
  Pallas kernels  56.9 us (99%)
  between operations  0.64 us (1%)
    pallas_call x1, Pallas kernels, body(): pl.pallas_call(kernel, out_shape=(pltpu.VMEM((64, 512), BF16), pltpu.VMEM...  55.5 us
    pallas_call x1, Pallas kernels, body(): pl.pallas_call(finish, out_shape=(jax.ShapeDtypeStruct((64, 512), BF16),...  1.34 us

profile of v10, /device:TPU:1, one launch (start us, length us, event | category | flops | bytes accessed | tf_op | source)
XLA Modules:
  0.0 57.5 jit_solution(380784114297700616)
XLA Ops:
  0.6 55.5 %shard_map.158 = (bf16[64,512]{1,0:T(8,128)(2,1)S(1)}, f32[16,128,256]{2,1,0:T(8,128)S(1)}) custom-call(bf16[64,512]{1,0:T(8,128)(2,1)} %bitcast.13, bf16[1,64]{1,0:T(2,128)(2,1)} %bitcast.16, bf16[64,128]{1,0:T(8,128)(2,1)} %refs_2_.1, bf16[64,128]{1,0:T(8,128)(2,1)} %refs_3_.1, bf16[64,256]{1,0:T(8,128)(2,1)} %refs_4_.1, bf16[64,256]{1,0:T(8,128)(2,1)} %refs_5_.1, ...), custom_call_target="tpu_custom_call" | custom-call | tf_op jit(solution)/shard_map/pallas_call | solution.py:597
  56.2 1.3 %shard_map.159 = (bf16[64,512]{1,0:T(8,128)(2,1)}, f32[16,128,256]{2,1,0:T(8,128)}) custom-call(bf16[64,512]{1,0:T(8,128)(2,1)S(1)} %get-tuple-element.6.result_in, f32[16,128,256]{2,1,0:T(8,128)S(1)} %get-tuple-element.7.state_in), custom_call_target="tpu_custom_call" | custom-call | tf_op jit(solution)/shard_map/pallas_call | solution.py:645

commit v11 on v10

--- a/solution.py
+++ b/solution.py
@@ -19,7 +19,8 @@
 
 NX, NY, NZ = 4, 4, 8
 NT = 2 * NY
-COPIES = 32
+COPIES = 35
+PARTS = (32, 16)
 SMALL, UP, DOWN, LAST = range(4)
 FAR_X = [2, 1, 3]
 FAR_Y = [2, 1, 3]
@@ -95,15 +96,20 @@
         tok_own,
         tok_all,
         middle,
-        up_own,
-        up_all,
-        down_own,
-        down_all,
+        up_own0,
+        up_own1,
+        up_all0,
+        up_all1,
+        down_own0,
+        down_own1,
+        down_all0,
+        down_all1,
         part3a,
         got3a,
         part3b,
         got3b,
-        hid,
+        hid0,
+        hid1,
         part4,
         got4,
         res_own,
@@ -232,7 +238,7 @@
     mix_step(1)
 
     with jax.named_scope("wait_later"):
-        loaded(2, up_all.at[0, 0:3])
+        loaded(2, new_state.at[0:9, 0:32])
         loaded(4, mixer_gain)
         loaded(5, log_decay)
         loaded(6, out_gain)
@@ -244,17 +250,22 @@
     down = w_down[...].astype(F32)
     down = jnp.concatenate([down, pltpu.roll(down, 768 - 48, 1)], axis=0)
     down = jnp.transpose(down, (1, 0)).astype(BF16)
+    up_own, up_all = (up_own0, up_own1), (up_all0, up_all1)
+    down_own, down_all = (down_own0, down_own1), (down_all0, down_all1)
     for j in range(NZ):
-        up_own[0, j] = units[96 * j : 96 * j + 48]
-        up_own[1, j] = units[96 * j + 48 : 96 * j + 96]
-        down_own[j] = down[96 * j : 96 * j + 48]
+        for part, skip in ((0, 0), (1, 32)):
+            count = PARTS[part]
+            low, high = 96 * j + skip, 96 * j + 48 + skip
+            up_own[part][j, 0] = units[low : low + count]
+            up_own[part][j, 1] = units[high : high + count]
+            down_own[part][j] = down[low : low + count]
     lanes_z = lanes_of(z)
-    for half in range(2):
-        up_all[half, t, :, lanes_z] = up_own[half, z]
-    down_all[t, :, lanes_z] = down_own[z]
-    up_blocks = [Exchange(up_own.at[half, 0:7]) for half in range(2)]
-    up_y = [Exchange(up_all.at[half, 0:3], UP) for half in range(2)]
-    up_core = [Exchange(up_all.at[half, 0:4], UP) for half in range(2)]
+    for part in range(2):
+        up_all[part][:, t, :, lanes_z] = up_own[part][z]
+        down_all[part][t, :, lanes_z] = down_own[part][z]
+    up_blocks = [Exchange(up_own[part].at[0:7]) for part in range(2)]
+    up_y = [Exchange(up_all[part].at[:, 0:3], UP) for part in range(2)]
+    up_core = [Exchange(up_all[part].at[:, 0:4], UP) for part in range(2)]
     partner = (kv, t + 1 - 2 * core)
 
     def along_y(d):
@@ -263,15 +274,15 @@
     def up_along_z(half):
         for d, peer in ring_z:
             up_blocks[half].send(
-                up_own.at[half, at_z(d)], up_all.at[half, t, :, lanes_z], peer
+                up_own[half].at[at_z(d)], up_all[half].at[:, t, :, lanes_z], peer
             )
 
     def up_along_y(half):
         with jax.named_scope(f"wait_up_blocks_{half}"):
             up_blocks[half].arrive()
         for d in FAR_Y:
-            up_y[half].send(up_all.at[half, t], up_all.at[half, t], (kv, along_y(d)))
-        up_core[half].send(up_all.at[half, t], up_all.at[half, t], partner)
+            up_y[half].send(up_all[half].at[:, t], up_all[half].at[:, t], (kv, along_y(d)))
+        up_core[half].send(up_all[half].at[:, t], up_all[half].at[:, t], partner)
 
     up_along_z(0)
     lane32 = lax.broadcasted_iota(jnp.int32, (32, 128), 1)
@@ -359,9 +370,12 @@
     gather2 = Exchange(mix.at[0:3])
     for d, peer in ring_x:
         gather2.send(mix.at[x], mix.at[x], peer)
-    down_blocks = Exchange(down_own.at[0:7])
-    for d, peer in ring_z:
-        down_blocks.send(down_own.at[at_z(d)], down_all.at[t, :, lanes_z], peer)
+    down_blocks = [Exchange(down_own[part].at[0:7]) for part in range(2)]
+    for part in range(2):
+        for d, peer in ring_z:
+            down_blocks[part].send(
+                down_own[part].at[at_z(d)], down_all[part].at[t, :, lanes_z], peer
+            )
     tok_blocks = Exchange(tok_all.at[0:7])
     for d, peer in ring_z:
         tok_blocks.send(tok_own, tok_all.at[z], peer)
@@ -413,17 +427,24 @@
         spread.send(attn_own, attn_all.at[z], peer)
 
     with jax.named_scope("wait_down_blocks"):
-        down_blocks.arrive()
-    down_y, down_core = Exchange(down_all.at[0:3], DOWN), Exchange(down_all.at[0:4], DOWN)
+        for exchange in down_blocks:
+            exchange.arrive()
+    down_y = [Exchange(down_all[part].at[0:3], DOWN) for part in range(2)]
+    down_core = [Exchange(down_all[part].at[0:4], DOWN) for part in range(2)]
+
+    def down_send(exchanges, block, peer):
+        for exchange, ref in zip(exchanges, down_all):
+            exchange.send(ref.at[block], ref.at[block], peer)
+
     for d in FAR_Y:
-        down_y.send(down_all.at[t], down_all.at[t], (kv, along_y(d)))
+        down_send(down_y, t, (kv, along_y(d)))
     for half in range(2):
         with jax.named_scope(f"wait_up_y_{half}"):
             up_y[half].arrive()
         for d in range(1, NY):
             other = along_y(d)
-            up_core[half].send(up_all.at[half, other], up_all.at[half, other], partner)
-    down_core.send(down_all.at[t], down_all.at[t], partner)
+            up_core[half].send(up_all[half].at[:, other], up_all[half].at[:, other], partner)
+    down_send(down_core, t, partner)
 
     with jax.named_scope("wait_tok_blocks"):
         tok_blocks.arrive()
@@ -463,16 +484,17 @@
             up_core[half].arrive()
         terms = lax.dot_general(
             left,
-            up_all[half].reshape(384, 1024),
+            up_all[half][...].reshape(16 * PARTS[half], 1024),
             (((1,), (1,)), ((), ())),
             preferred_element_type=F32,
         )
         for j in range(NX):
             rows = slice(16 * j, 16 * j + 16)
-            part3[j, :, 0:384] = terms[rows].astype(BF16)
-            part3[j, :, 384:768] = terms[64 + 16 * j : 80 + 16 * j].astype(BF16)
+            width = 16 * PARTS[half]
+            part3[j, :, 0:width] = terms[rows].astype(BF16)
+            part3[j, :, width : 2 * width] = terms[64 + 16 * j : 80 + 16 * j].astype(BF16)
             if half == 0:
-                part3[j, :, 768:896] = squares[rows]
+                part3[j, :, 2 * width : 2 * width + 128] = squares[rows]
         got3[x] = part3[x]
         for d, peer in ring_x:
             scatter3[half].send(part3.at[at_x(d)], got3.at[x], peer)
@@ -481,11 +503,12 @@
         middle[2 * p] = jnp.where(lane32 < 64, wide[0:32], turned[32:64]).astype(BF16)
         middle[2 * p + 1] = jnp.where(lane32 < 64, turned[0:32], wide[32:64]).astype(BF16)
     with jax.named_scope("wait_down_y"):
-        down_y.arrive()
+        for exchange in down_y:
+            exchange.arrive()
     for d in range(1, NY):
-        other = along_y(d)
-        down_core.send(down_all.at[other], down_all.at[other], partner)
-    gather3 = [Exchange(hid.at[half, 0:3]) for half in range(2)]
+        down_send(down_core, along_y(d), partner)
+    hid = (hid0, hid1)
+    gather3 = [Exchange(ref.at[0:3]) for ref in hid]
     inv = None
     for half, got3 in enumerate(gots3):
         with jax.named_scope(f"wait_scatter3_{half}"):
@@ -493,23 +516,27 @@
         total = got3[0].astype(F32)
         for j in range(1, NX):
             total += got3[j].astype(F32)
+        width = 16 * PARTS[half]
         if half == 0:
-            inv = lax.rsqrt(of_pair(total[:, 768:896]) / D + EPS)
-        gate = total[:, 0:384] * inv
-        hid[half, x] = (gate * sigmoid(gate) * (total[:, 384:768] * inv)).astype(BF16)
+            inv = lax.rsqrt(of_pair(total[:, 2 * width : 2 * width + 128]) / D + EPS)
+        gate = total[:, 0:width] * inv
+        hid[half][x] = (gate * sigmoid(gate) * (total[:, width : 2 * width] * inv)).astype(BF16)
         for d, peer in ring_x:
-            gather3[half].send(hid.at[half, x], hid.at[half, x], peer)
+            gather3[half].send(hid[half].at[x], hid[half].at[x], peer)
     with jax.named_scope("wait_down_core"):
-        down_core.arrive()
-
-    weights = down_all[...].reshape(NT * 48, 1024)
-    products = []
+        for exchange in down_core:
+            exchange.arrive()
+
+    total = jnp.zeros((128, 1024), F32)
     for half in range(2):
         with jax.named_scope(f"wait_gather3_{half}"):
             gather3[half].arrive()
-        products.append(
-            jnp.dot(hid[half].reshape(64, 384), weights, preferred_element_type=F32)
-        )
+        width = 8 * PARTS[half]
+        hidden = hid[half][...].reshape(64, 2 * width)
+        stacked = jnp.concatenate([hidden[:, 0:width], hidden[:, width:]], axis=0)
+        weights = down_all[half][...].reshape(width, 1024)
+        total += jnp.dot(stacked, weights, preferred_element_type=F32)
+    products = (total[0:64], total[64:128])
     for j, block in enumerate(packed_products(*products, lane32)):
         part4[j] = block.astype(BF16)
     got4[z] = part4[z]
@@ -540,7 +567,7 @@
     )
     result[...] = jnp.transpose(rows, (1, 0))[0:64].astype(BF16)
     with jax.named_scope("wait_sends"):
-        everything = (state.at[0:15, 0:80], up_all, up_all.at[0], res_all.at[0:7])
+        everything = (state.at[0:15, 0:80], state.at[0:12], state.at[0:6], res_all.at[0:7])
         for group, size in enumerate(everything):
             pltpu.make_async_copy(size, size, send_sems.at[group]).wait()
 
@@ -621,15 +648,16 @@
             pltpu.VMEM((32, 128), BF16),
             pltpu.VMEM((NZ, 32, 128), BF16),
             pltpu.VMEM((NZ, 32, 128), BF16),
-            pltpu.VMEM((2, NZ, 48, 128), BF16),
-            pltpu.VMEM((2, NT, 48, 1024), BF16),
-            pltpu.VMEM((NZ, 48, 128), BF16),
-            pltpu.VMEM((NT, 48, 1024), BF16),
-            pltpu.VMEM((NX, 16, 896), BF16),
-            pltpu.VMEM((NX, 16, 896), BF16),
-            pltpu.VMEM((NX, 16, 768), BF16),
-            pltpu.VMEM((NX, 16, 768), BF16),
-            pltpu.VMEM((2, NX, 16, 384), BF16),
+            *(pltpu.VMEM((NZ, 2, units, 128), BF16) for units in PARTS),
+            *(pltpu.VMEM((2, NT, units, 1024), BF16) for units in PARTS),
+            *(pltpu.VMEM((NZ, units, 128), BF16) for units in PARTS),
+            *(pltpu.VMEM((NT, units, 1024), BF16) for units in PARTS),
+            pltpu.VMEM((NX, 16, 1152), BF16),
+            pltpu.VMEM((NX, 16, 1152), BF16),
+            pltpu.VMEM((NX, 16, 512), BF16),
+            pltpu.VMEM((NX, 16, 512), BF16),
+            pltpu.VMEM((NX, 16, 512), BF16),
+            pltpu.VMEM((NX, 16, 256), BF16),
             pltpu.VMEM((NZ, 32, 128), BF16),
             pltpu.VMEM((NZ, 32, 128), BF16),
             pltpu.VMEM((32, 128), BF16),

time: 57.6 us -> 57.8 us (level)
  no operation moved by 1% of the time
where the time goes in v11:
time: 57.8 us; the launch traced here: 57.7 us
  Pallas kernels  57.1 us (99%)
  between operations  0.64 us (1%)
    pallas_call x1, Pallas kernels, body(): pl.pallas_call(kernel, out_shape=(pltpu.VMEM((64, 512), BF16), pltpu.VMEM...  55.7 us
    pallas_call x1, Pallas kernels, body(): pl.pallas_call(finish, out_shape=(jax.ShapeDtypeStruct((64, 512), BF16),...  1.34 us

profile of v11, /device:TPU:1, one launch (start us, length us, event | category | flops | bytes accessed | tf_op | source)
XLA Modules:
  0.0 57.7 jit_solution(12304667638294991332)
XLA Ops:
  0.6 55.7 %shard_map.158 = (bf16[64,512]{1,0:T(8,128)(2,1)S(1)}, f32[16,128,256]{2,1,0:T(8,128)S(1)}) custom-call(bf16[64,512]{1,0:T(8,128)(2,1)} %bitcast.13, bf16[1,64]{1,0:T(2,128)(2,1)} %bitcast.16, bf16[64,128]{1,0:T(8,128)(2,1)} %refs_2_.1, bf16[64,128]{1,0:T(8,128)(2,1)} %refs_3_.1, bf16[64,256]{1,0:T(8,128)(2,1)} %refs_4_.1, bf16[64,256]{1,0:T(8,128)(2,1)} %refs_5_.1, ...), custom_call_target="tpu_custom_call" | custom-call | tf_op jit(solution)/shard_map/pallas_call | solution.py:624
  56.4 1.3 %shard_map.159 = (bf16[64,512]{1,0:T(8,128)(2,1)}, f32[16,128,256]{2,1,0:T(8,128)}) custom-call(bf16[64,512]{1,0:T(8,128)(2,1)S(1)} %get-tuple-element.6.result_in, f32[16,128,256]{2,1,0:T(8,128)S(1)} %get-tuple-element.7.state_in), custom_call_target="tpu_custom_call" | custom-call | tf_op jit(solution)/shard_map/pallas_call | solution.py:673

commit v12 on v10

--- a/solution.py
+++ b/solution.py
@@ -24,7 +24,7 @@
 FAR_X = [2, 1, 3]
 FAR_Y = [2, 1, 3]
 FAR_Z = [4, 3, 5, 2, 6, 1, 7]
-FAR_T = [4, 5, 2, 3, 6, 7, 1]
+FAR_T = [(dy, dc) for dy in FAR_Y + [0] for dc in range(2) if (dy, dc) != (0, 0)]
 X_ORDER = [(0, 4), (2, 6), (3, 7), (1, 5)]
 PLANE = [(dz, dx) for dz in FAR_Z + [0] for dx in FAR_X + [0] if (dz, dx) != (0, 0)]
 LOADS = [(0, 0), (1, 1), (2, 0), (3, 0), (4, 0), (5, 0), (6, 0)]
@@ -123,9 +123,6 @@
     def at_z(d):
         return lax.rem(z + d, NZ)
 
-    def at_t(d):
-        return lax.rem(t + d, NT)
-
     counter = [0]
 
     class Exchange:
@@ -156,8 +153,8 @@
 
     for dz, dx in PLANE:
         greet((at_z(dz) * NX + at_x(dx), t))
-    for d in FAR_T:
-        greet((kv, at_t(d)))
+    for dy, dc in FAR_T:
+        greet((kv, lax.rem(y + dy, NY) * 2 + (core if dc == 0 else 1 - core)))
     def loaded(sem, size):
         pltpu.make_async_copy(size, size, local_sems.at[sem]).wait()
 
@@ -198,7 +195,9 @@
 
     ring_x = [(d, (z * NX + at_x(d), t)) for d in FAR_X]
     ring_z = [(d, (at_z(d) * NX + x, t)) for d in FAR_Z]
-    ring_t = [(d, (kv, at_t(d))) for d in FAR_T]
+    ring_t = [
+        lax.rem(y + dy, NY) * 2 + (core if dc == 0 else 1 - core) for dy, dc in FAR_T
+    ]
     gather_w = Exchange(w_all.at[0:3], DOWN)
     gather_x = [Exchange(x_all.at[0:3, 0], UP) for _ in X_ORDER]
     x_blocks = [lax.rem(z + steps[0], 4) for steps in X_ORDER]
@@ -397,8 +396,8 @@
         part2[j] = jnp.concatenate([pair[rows] for pair in pairs], axis=0).astype(BF16)
     got2[t] = part2[t]
     scatter2 = Exchange(got2.at[0:7])
-    for d, peer in ring_t:
-        scatter2.send(part2.at[at_t(d)], got2.at[t], peer)
+    for other in ring_t:
+        scatter2.send(part2.at[other], got2.at[t], (kv, other))
     up_along_y(1)
     with jax.named_scope("wait_scatter2"):
         scatter2.arrive()
@@ -524,8 +523,8 @@
     res_own[...] = (middle[z].astype(F32) + total).astype(BF16)
     res_all[t] = res_own[...]
     gather4 = Exchange(res_all.at[0:7], LAST)
-    for d, peer in ring_t:
-        gather4.send(res_own, res_all.at[t], peer)
+    for other in ring_t:
+        gather4.send(res_own, res_all.at[t], (kv, other))
     with jax.named_scope("wait_gather4"):
         gather4.arrive()
     blocks = [res_all[j].astype(F32) for j in range(NT)]

time: 57.6 us -> 57.6 us (level)
  no operation moved by 1% of the time
where the time goes in v12:
time: 57.6 us; the launch traced here: 57.5 us
  Pallas kernels  56.9 us (99%)
  between operations  0.64 us (1%)
    pallas_call x1, Pallas kernels, body(): pl.pallas_call(kernel, out_shape=(pltpu.VMEM((64, 512), BF16), pltpu.VMEM...  55.5 us
    pallas_call x1, Pallas kernels, body(): pl.pallas_call(finish, out_shape=(jax.ShapeDtypeStruct((64, 512), BF16),...  1.34 us

profile of v12, /device:TPU:1, one launch (start us, length us, event | category | flops | bytes accessed | tf_op | source)
XLA Modules:
  0.0 57.5 jit_solution(13252422165824752115)
XLA Ops:
  0.6 55.5 %shard_map.158 = (bf16[64,512]{1,0:T(8,128)(2,1)S(1)}, f32[16,128,256]{2,1,0:T(8,128)S(1)}) custom-call(bf16[64,512]{1,0:T(8,128)(2,1)} %bitcast.13, bf16[1,64]{1,0:T(2,128)(2,1)} %bitcast.16, bf16[64,128]{1,0:T(8,128)(2,1)} %refs_2_.1, bf16[64,128]{1,0:T(8,128)(2,1)} %refs_3_.1, bf16[64,256]{1,0:T(8,128)(2,1)} %refs_4_.1, bf16[64,256]{1,0:T(8,128)(2,1)} %refs_5_.1, ...), custom_call_target="tpu_custom_call" | custom-call | tf_op jit(solution)/shard_map/pallas_call | solution.py:596
  56.1 1.3 %shard_map.159 = (bf16[64,512]{1,0:T(8,128)(2,1)}, f32[16,128,256]{2,1,0:T(8,128)}) custom-call(bf16[64,512]{1,0:T(8,128)(2,1)S(1)} %get-tuple-element.6.result_in, f32[16,128,256]{2,1,0:T(8,128)S(1)} %get-tuple-element.7.state_in), custom_call_target="tpu_custom_call" | custom-call | tf_op jit(solution)/shard_map/pallas_call | solution.py:644

commit v13 on v10

--- a/solution.py
+++ b/solution.py
@@ -146,9 +146,6 @@
         def arrive(self):
             pltpu.make_async_copy(self.size, self.size, recv_sems.at[self.number]).wait()
 
-    for i, sem in LOADS:
-        pltpu.make_async_copy(inputs[i], held[i], local_sems.at[sem]).start()
-
     barrier = pltpu.get_barrier_semaphore()
 
     def greet(peer):
@@ -158,6 +155,9 @@
         greet((at_z(dz) * NX + at_x(dx), t))
     for d in FAR_T:
         greet((kv, at_t(d)))
+    for i, sem in LOADS:
+        pltpu.make_async_copy(inputs[i], held[i], local_sems.at[sem]).start()
+
     def loaded(sem, size):
         pltpu.make_async_copy(size, size, local_sems.at[sem]).wait()
 

time: 57.6 us -> 57.6 us (level)
  no operation moved by 1% of the time
where the time goes in v13:
time: 57.6 us; the launch traced here: 57.5 us
  Pallas kernels  56.9 us (99%)
  between operations  0.64 us (1%)
    pallas_call x1, Pallas kernels, body(): pl.pallas_call(kernel, out_shape=(pltpu.VMEM((64, 512), BF16), pltpu.VMEM...  55.5 us
    pallas_call x1, Pallas kernels, body(): pl.pallas_call(finish, out_shape=(jax.ShapeDtypeStruct((64, 512), BF16),...  1.34 us

profile of v13, /device:TPU:1, one launch (start us, length us, event | category | flops | bytes accessed | tf_op | source)
XLA Modules:
  0.0 57.5 jit_solution(11979079082754405719)
XLA Ops:
  0.6 55.5 %shard_map.158 = (bf16[64,512]{1,0:T(8,128)(2,1)S(1)}, f32[16,128,256]{2,1,0:T(8,128)S(1)}) custom-call(bf16[64,512]{1,0:T(8,128)(2,1)} %bitcast.13, bf16[1,64]{1,0:T(2,128)(2,1)} %bitcast.16, bf16[64,128]{1,0:T(8,128)(2,1)} %refs_2_.1, bf16[64,128]{1,0:T(8,128)(2,1)} %refs_3_.1, bf16[64,256]{1,0:T(8,128)(2,1)} %refs_4_.1, bf16[64,256]{1,0:T(8,128)(2,1)} %refs_5_.1, ...), custom_call_target="tpu_custom_call" | custom-call | tf_op jit(solution)/shard_map/pallas_call | solution.py:597
  56.2 1.3 %shard_map.159 = (bf16[64,512]{1,0:T(8,128)(2,1)}, f32[16,128,256]{2,1,0:T(8,128)}) custom-call(bf16[64,512]{1,0:T(8,128)(2,1)S(1)} %get-tuple-element.6.result_in, f32[16,128,256]{2,1,0:T(8,128)S(1)} %get-tuple-element.7.state_in), custom_call_target="tpu_custom_call" | custom-call | tf_op jit(solution)/shard_map/pallas_call | solution.py:645
